TPU v7x, 256 devices: a whole 4x4x8 slice. The times are simulated.
256 devices in a mesh: fs: 16 (over y, x), tp: 16 (over z, core).
Axes of the slice: x: 4, y: 4, z: 8, core: 2. Of those that a mesh axis runs over, the one named last changes fastest.
Arguments:
- tokens: bfloat16 [32768, 2048], P(('fs', 'tp')), may hold values from -6 to 6
- norm_gain: float32 [2048], replicated, may hold values from 0.1 to 1.9
- gate_weight: bfloat16 [2048, 5632], P('fs', 'tp'), may hold values from -0.125 to 0.125
- up_weight: bfloat16 [2048, 5632], P('fs', 'tp'), may hold values from -0.125 to 0.125
- down_weight: bfloat16 [5632, 2048], P('tp', 'fs'), may hold values from -0.078125 to 0.078125
Outputs:
- mixed: bfloat16 [32768, 2048], P(('fs', 'tp'))
All inputs are finite; a program needn't handle non-finite values.
Results may differ from a plain program's by a relative error of at most 0.0065.
Values may be sent and summed in bfloat16 or wider, within the bound.
No kernel may reach another device: no remote copies, remote signals or barrier semaphores. Data moves between devices by JAX's collectives and lax.ppermute only.
A program may use at most 128 MiB of HBM per device.

v0:
```python
import functools

import jax
import jax.numpy as jnp
from jax import lax
from jax.experimental import pallas as pl
from jax.experimental.pallas import tpu as pltpu
from jax.sharding import Mesh, PartitionSpec as P


eps_floor = 0.05
X, Y, Z = 4, 4, 8
AXES = ("y", "x", "z", "c")
LANES = 128
f32, bf16 = jnp.float32, jnp.bfloat16


def place(y, x, z, c):
    return ((y * X + x) * Z + z) * 2 + c


def rows_and_columns():
    along_x = lambda c: [[place(y, x, z, c) for x in range(X)] for y in range(Y) for z in range(Z)]
    along_y = lambda c: [[place(y, x, z, c) for y in range(Y)] for x in range(X) for z in range(Z)]
    return along_x(0) + along_y(1), along_y(0) + along_x(1)


FIRST, SECOND = rows_and_columns()
WHOLE = pl.BlockSpec(memory_space=pltpu.VMEM)
SMALL = pltpu.CompilerParams(vmem_limit_bytes=12 << 20)


def onward(x, by):
    pairs = [(2 * z + c, 2 * ((z + (by if c == 0 else -by)) % Z) + c) for z in range(Z) for c in range(2)]
    return lax.ppermute(x, ("z", "c"), pairs)


def swap(x):
    return lax.ppermute(x, "c", [(0, 1), (1, 0)])


def from_four(copies, groups):
    return lax.all_to_all(copies, AXES, 0, 0, axis_index_groups=groups, tiled=True)


def norm_body(tokens, gain, out):
    values = tokens[...].astype(f32)
    factor = lax.rsqrt(jnp.mean(values * values, axis=-1, keepdims=True) + eps_floor)
    out[...] = (values * factor * gain[...]).T.astype(bf16)


def norm(tokens, gain):
    return pl.pallas_call(
        norm_body,
        out_shape=jax.ShapeDtypeStruct(tokens.shape[::-1], bf16),
        in_specs=[WHOLE, WHOLE],
        out_specs=WHOLE,
        compiler_params=SMALL,
        name="norm",
    )(tokens, gain[None])


def spread_body(units, packed, gate_up, down):
    for k in range(packed.shape[0]):
        gate_up[0, :, LANES * k : LANES * (k + 1)] = packed[k, : 2 * units]
        down[0, LANES * k : LANES * (k + 1), :units] = packed[k, 2 * units :].T
        down[0, LANES * k : LANES * (k + 1), units:] = jnp.zeros((LANES, down.shape[2] - units), bf16)


def spread(packed):
    n, units = packed.shape[0], packed.shape[1] // 3
    shapes = [(n, 2 * units, n * LANES), (n, n * LANES, pl.cdiv(units, LANES) * LANES)]
    return pl.pallas_call(
        functools.partial(spread_body, units),
        grid=(n,),
        out_shape=[jax.ShapeDtypeStruct(s, bf16) for s in shapes],
        in_specs=[pl.BlockSpec(packed.shape, lambda i: (0, 0, 0))],
        out_specs=[pl.BlockSpec((1, *s[1:]), lambda i: (i, 0, 0)) for s in shapes],
        compiler_params=SMALL,
        name="spread",
    )(packed)


def share_body(n, units, core_ref, *refs):
    pieces, weights, outs, turned = refs[:n], refs[n : n + 4], refs[n + 4 : 2 * n + 4], refs[2 * n + 4]
    depth, m = weights[0].shape[2], pieces[0].shape[1]
    blocks = turned.shape[0] // LANES
    core = core_ref[0]

    def order(b, w):
        return jnp.where(core == w, b, (b % 4) * 4 + b // 4)

    hidden = []
    for w in (0, 1):
        for b in range(blocks):
            at = pl.ds(pl.multiple_of(order(b, w) * LANES, LANES), LANES)
            for i in range(n):
                turned[LANES * b : LANES * (b + 1), m * i : m * (i + 1)] = pieces[i][at, :]
        both = jnp.dot(weights[2 * w][0], turned[:depth], preferred_element_type=f32)
        for k in range(1, 4):
            both += jnp.dot(weights[2 * w][k], turned[depth * k : depth * (k + 1)], preferred_element_type=f32)
        gate, upper = both[:units], both[units:]
        hidden.append((gate / (1.0 + jnp.exp(-gate)) * upper).astype(bf16))
    for b in range(blocks):
        part = 0.0
        for w in (0, 1):
            at = order(b, w)
            rows = weights[2 * w + 1][at // 4, pl.ds(pl.multiple_of(at % 4 * LANES, LANES), LANES), :units]
            part += jnp.dot(rows, hidden[w], preferred_element_type=f32)
        for i in range(n):
            outs[i][LANES * b : LANES * (b + 1), :] = part[:, m * i : m * (i + 1)].astype(outs[i].dtype)


def share(core, pieces, weights, dtype):
    n, units = len(pieces), weights[0].shape[1] // 2
    shape = pieces[0].shape
    return pl.pallas_call(
        functools.partial(share_body, n, units),
        out_shape=[jax.ShapeDtypeStruct(shape, dtype)] * n,
        in_specs=[pl.BlockSpec(memory_space=pltpu.SMEM)] + [WHOLE] * (n + 4),
        out_specs=[WHOLE] * n,
        scratch_shapes=[pltpu.VMEM((shape[0], n * shape[1]), bf16)],
        compiler_params=pltpu.CompilerParams(vmem_limit_bytes=24 << 20),
        name="share",
    )(core, *pieces, *weights)


def close_body(own, first, second, out):
    out[...] = (own[...] + first[...].astype(f32) + second[...].astype(f32)).T.astype(bf16)


def close(own, first, second):
    return pl.pallas_call(
        close_body,
        out_shape=jax.ShapeDtypeStruct(own.shape[::-1], bf16),
        in_specs=[WHOLE] * 3,
        out_specs=WHOLE,
        compiler_params=SMALL,
        name="close",
    )(own, first, second)


def local(tokens, norm_gain, gate_weight, up_weight, down_weight):
    core = lax.axis_index("c").astype(jnp.int32)[None]
    normed = norm(tokens, norm_gain)

    own, mate = {0: normed}, {0: swap(normed)}
    for d in (1, 2, 3, 4):
        own[d] = onward(own[d - 1], 1)
        if d < 4:
            mate[d] = onward(mate[d - 1], 1)

    packed = jnp.concatenate([gate_weight.T, up_weight.T, down_weight], axis=0)
    copies = jnp.broadcast_to(packed[None], (4, *packed.shape))
    rows = from_four(copies, FIRST)
    gate_up, down = spread(rows)
    gate_up = from_four(gate_up, SECOND)
    down = from_four(down, SECOND)
    gate_up_mate = swap(gate_up)
    down_mate = swap(down)
    weights = (gate_up, down, gate_up_mate, down_mate)

    own4, mate3 = share(core, [own[4], mate[3]], weights, bf16)
    own3, mate2 = share(core, [own[3], mate[2]], weights, f32)
    own2, mate1 = share(core, [own[2], mate[1]], weights, f32)
    own1, own0 = share(core, [own[1], own[0]], weights, f32)

    def send(x):
        return onward(x.astype(bf16), -1)

    got_own = send(own4)
    got_mate = send(mate3)
    got_own = send(got_own.astype(f32) + own3)
    got_mate = send(got_mate.astype(f32) + mate2)
    got_own = send(got_own.astype(f32) + own2)
    got_mate = send(got_mate.astype(f32) + mate1)
    got_own = send(got_own.astype(f32) + own1)
    return close(own0, got_own, swap(got_mate))


def solution(mesh):
    fine = Mesh(mesh.devices.reshape(Y, X, Z, 2), AXES)
    fs, tp = ("y", "x"), ("z", "c")

    return jax.shard_map(
        local,
        mesh=fine,
        in_specs=(P(fs + tp, None), P(), P(fs, tp), P(fs, tp), P(tp, fs)),
        out_specs=P(fs + tp, None),
        check_vma=False,
    )
```

profile of v0, /device:TPU:2, one launch (start us, length us, event | category | flops | bytes accessed | tf_op | source)
XLA Modules:
  0.0 155.1 jit_solution(12737951259077362822)
XLA Ops:
  0.0 1.0 pad_maximum_fusion
  1.0 0.1 broadcast_in_dim.14
  1.1 14.2 %all_to_all.15.packed = bf16[4,1056,128]{2,1,0:T(8,128)(2,1)S(1)} all-to-all(bf16[4,1056,128]{2,1,0:T(8,128)(2,1)S(1)} %broadcast_in_dim.14), channel_id=1, replica_groups={{0,16,32,48},{2,18,34,50},{4,20,36,52},{6,22,38,54},{8,24,40,56},{10,26..., dimensions={0} | all-to-all | bytes 2162688 | tf_op jit(solution)/shard_map/all_to_all | solution.py:43
  15.4 0.8 spread.1
  16.2 1.2 copy-done
  17.3 25.0 %all_to_all.16.refs_2_ = bf16[4,704,512]{2,1,0:T(8,128)(2,1)S(1)} all-to-all(bf16[4,704,512]{2,1,0:T(8,128)(2,1)S(1)} %get-tuple-element.15), channel_id=1, replica_groups={{0,64,128,192},{2,66,130,194},{4,68,132,196},{6,70,134,198},{8,72,136,2..., dimensions={0} | all-to-all | bytes 5767168 | tf_op jit(solution)/shard_map/all_to_all | solution.py:43
  42.3 0.0 collective-permute-start.1
  42.3 4.5 %all-to-all-start.2 = ((bf16[4,512,384]{2,1,0:T(8,128)(2,1)}), bf16[4,512,384]{2,1,0:T(8,128)(2,1)}, u32[]{:S(2)}, u32[]{:S(2)}) async-start(bf16[4,512,384]{2,1,0:T(8,128)(2,1)} %copy-done), calls=%async_computation.2 | async-start | bytes 3145728 | tf_op jit(solution)/shard_map/all_to_all | solution.py:43
  46.8 0.0 copy-start.1
  46.8 1.0 copy-done.1
  47.8 0.4 norm.1.refs_1_
  48.2 2.0 %collective-permute-start = (bf16[2048,128]{1,0:T(8,128)(2,1)S(1)}, bf16[2048,128]{1,0:T(8,128)(2,1)}, u32[]{:S(2)}, u32[]{:S(2)}) collective-permute-start(bf16[2048,128]{1,0:T(8,128)(2,1)S(1)} %norm.1.refs_1_), channel_id=1, source_target_pairs={{0,2},{1,15},{2,4},{3,1},{4,6},{5,3},{6,8},{7,5},{8,10},{9,7},{10,... | collective-permute-start | bytes 1572872 | tf_op jit(solution)/shard_map/ppermute | solution.py:35
  50.2 5.3 %collective-permute-start.6 = (bf16[2048,128]{1,0:T(8,128)(2,1)S(1)}, bf16[2048,128]{1,0:T(8,128)(2,1)}, u32[]{:S(2)}, u32[]{:S(2)}) collective-permute-start(bf16[2048,128]{1,0:T(8,128)(2,1)S(1)} %norm.1.refs_1_), channel_id=1, source_target_pairs={{0,1},{1,0},{2,3},{3,2},{4,5},{5,4},{6,7},{7,6},{8,9},{9,8},{10,11... | collective-permute-start | bytes 1572872 | tf_op jit(solution)/shard_map/ppermute | solution.py:39
  55.5 5.9 %collective-permute-done.refs_0_ = bf16[2048,128]{1,0:T(8,128)(2,1)} collective-permute-done((bf16[2048,128]{1,0:T(8,128)(2,1)S(1)}, bf16[2048,128]{1,0:T(8,128)(2,1)}, u32[]{:S(2)}, u32[]{:S(2)}) %collective-permute-start) | collective-permute-done | bytes 524320 | tf_op jit(solution)/shard_map/ppermute | solution.py:35
  61.4 0.0 collective-permute-start.7
  61.4 3.8 %collective-permute-start.2 = (bf16[4,512,384]{2,1,0:T(8,128)(2,1)}, bf16[4,512,384]{2,1,0:T(8,128)(2,1)}, u32[]{:S(2)}, u32[]{:S(2)}) collective-permute-start(bf16[4,512,384]{2,1,0:T(8,128)(2,1)} %all-to-all-done.2.refs_3_), channel_id=1, source_target_pairs={{0,1},{1,0},{2,3},{3,2},{4,5},{5,4},{6,7},{7,6},{8,9},{9,8},{10,11... | collective-permute-start | bytes 4718600 | tf_op jit(solution)/shard_map/ppermute | solution.py:39
  65.2 6.9 %collective-permute-done.3.refs_0_ = bf16[2048,128]{1,0:T(8,128)(2,1)} collective-permute-done((bf16[2048,128]{1,0:T(8,128)(2,1)}, bf16[2048,128]{1,0:T(8,128)(2,1)}, u32[]{:S(2)}, u32[]{:S(2)}) %collective-permute-start.3) | collective-permute-done | bytes 524320 | tf_op jit(solution)/shard_map/ppermute | solution.py:35
  72.1 0.0 collective-permute-start.4
  72.1 5.6 %collective-permute-done.7.refs_1_ = bf16[2048,128]{1,0:T(8,128)(2,1)} collective-permute-done((bf16[2048,128]{1,0:T(8,128)(2,1)}, bf16[2048,128]{1,0:T(8,128)(2,1)}, u32[]{:S(2)}, u32[]{:S(2)}) %collective-permute-start.7) | collective-permute-done | bytes 524320 | tf_op jit(solution)/shard_map/ppermute | solution.py:35
  77.7 0.0 collective-permute-start.8
  77.7 5.6 %collective-permute-done.4.refs_0_ = bf16[2048,128]{1,0:T(8,128)(2,1)} collective-permute-done((bf16[2048,128]{1,0:T(8,128)(2,1)}, bf16[2048,128]{1,0:T(8,128)(2,1)}, u32[]{:S(2)}, u32[]{:S(2)}) %collective-permute-start.4) | collective-permute-done | bytes 524320 | tf_op jit(solution)/shard_map/ppermute | solution.py:35
  83.4 5.6 %collective-permute-done.8.refs_1_ = bf16[2048,128]{1,0:T(8,128)(2,1)} collective-permute-done((bf16[2048,128]{1,0:T(8,128)(2,1)}, bf16[2048,128]{1,0:T(8,128)(2,1)}, u32[]{:S(2)}, u32[]{:S(2)}) %collective-permute-start.8) | collective-permute-done | bytes 524320 | tf_op jit(solution)/shard_map/ppermute | solution.py:35
  89.0 0.0 collective-permute-start.9
  89.0 5.6 %collective-permute-done.5.refs_0_ = bf16[2048,128]{1,0:T(8,128)(2,1)} collective-permute-done((bf16[2048,128]{1,0:T(8,128)(2,1)}, bf16[2048,128]{1,0:T(8,128)(2,1)}, u32[]{:S(2)}, u32[]{:S(2)}) %collective-permute-start.5) | collective-permute-done | bytes 524320 | tf_op jit(solution)/shard_map/ppermute | solution.py:35
  94.6 5.6 %collective-permute-done.9.refs_1_ = bf16[2048,128]{1,0:T(8,128)(2,1)} collective-permute-done((bf16[2048,128]{1,0:T(8,128)(2,1)}, bf16[2048,128]{1,0:T(8,128)(2,1)}, u32[]{:S(2)}, u32[]{:S(2)}) %collective-permute-start.9) | collective-permute-done | bytes 524320 | tf_op jit(solution)/shard_map/ppermute | solution.py:35
  100.2 6.1 %share.5 = (bf16[2048,128]{1,0:T(8,128)(2,1)S(1)}, bf16[2048,128]{1,0:T(8,128)(2,1)S(1)}) custom-call(s32[1]{0:T(128)} %bitcast.core_ref, bf16[2048,128]{1,0:T(8,128)(2,1)} %collective-permute-done.5.refs_0_, bf16[2048,128]{1,0:T(8,128)(2,1)} %collective-permute-done.9.refs_1_, bf16[4,704,512]{2,1,0:T(8,128)(2,1)S(1)} %all_to_all.16.refs_2_, ...), custom_call_target="tpu_custom_call" | custom-call | tf_op jit(solution)/shard_map/share/pallas_call | solution.py:117
  106.4 0.9 collective-permute-start.14
  107.2 1.0 collective-permute-start.10
  108.3 6.1 %share.6 = (f32[2048,128]{1,0:T(8,128)S(1)}, f32[2048,128]{1,0:T(8,128)S(1)}) custom-call(s32[1]{0:T(128)} %bitcast.core_ref, bf16[2048,128]{1,0:T(8,128)(2,1)} %collective-permute-done.4.refs_0_, bf16[2048,128]{1,0:T(8,128)(2,1)} %collective-permute-done.8.refs_1_, bf16[4,704,512]{2,1,0:T(8,128)(2,1)S(1)} %all_to_all.16.refs_2_, ...), custom_call_target="tpu_custom_call" | custom-call | tf_op jit(solution)/shard_map/share/pallas_call | solution.py:117
  114.4 1.2 collective-permute-done.14
  115.6 0.1 add_convert_fusion.1
  115.8 2.1 %collective-permute-start.15 = (bf16[2048,128]{1,0:T(8,128)(2,1)S(1)}, bf16[2048,128]{1,0:T(8,128)(2,1)S(1)}, u32[]{:S(2)}, u32[]{:S(2)}) collective-permute-start(bf16[2048,128]{1,0:T(8,128)(2,1)S(1)} %add_convert_fusion.1), channel_id=1, source_target_pairs={{0,14},{1,3},{2,0},{3,5},{4,2},{5,7},{6,4},{7,9},{8,6},{9,11},{10,... | collective-permute-start | bytes 1572872 | tf_op jit(solution)/shard_map/ppermute | solution.py:35
  117.9 3.4 %collective-permute-done.10 = bf16[2048,128]{1,0:T(8,128)(2,1)S(1)} collective-permute-done((bf16[2048,128]{1,0:T(8,128)(2,1)S(1)}, bf16[2048,128]{1,0:T(8,128)(2,1)S(1)}, u32[]{:S(2)}, u32[]{:S(2)}) %collective-permute-start.10) | collective-permute-done | bytes 524320 | tf_op jit(solution)/shard_map/ppermute | solution.py:35
  121.2 0.1 add_convert_fusion.4
  121.4 2.1 %collective-permute-start.11 = (bf16[2048,128]{1,0:T(8,128)(2,1)S(1)}, bf16[2048,128]{1,0:T(8,128)(2,1)S(1)}, u32[]{:S(2)}, u32[]{:S(2)}) collective-permute-start(bf16[2048,128]{1,0:T(8,128)(2,1)S(1)} %add_convert_fusion.4), channel_id=1, source_target_pairs={{0,14},{1,3},{2,0},{3,5},{4,2},{5,7},{6,4},{7,9},{8,6},{9,11},{10,... | collective-permute-start | bytes 1572872 | tf_op jit(solution)/shard_map/ppermute | solution.py:35
  123.5 6.1 %share.7 = (f32[2048,128]{1,0:T(8,128)S(1)}, f32[2048,128]{1,0:T(8,128)S(1)}) custom-call(s32[1]{0:T(128)} %bitcast.core_ref, bf16[2048,128]{1,0:T(8,128)(2,1)} %collective-permute-done.3.refs_0_, bf16[2048,128]{1,0:T(8,128)(2,1)} %collective-permute-done.7.refs_1_, bf16[4,704,512]{2,1,0:T(8,128)(2,1)S(1)} %all_to_all.16.refs_2_, ...), custom_call_target="tpu_custom_call" | custom-call | tf_op jit(solution)/shard_map/share/pallas_call | solution.py:117
  129.6 0.1 add_convert_fusion
  129.8 0.1 collective-permute-start.16
  129.8 2.6 %collective-permute-done.11 = bf16[2048,128]{1,0:T(8,128)(2,1)S(1)} collective-permute-done((bf16[2048,128]{1,0:T(8,128)(2,1)S(1)}, bf16[2048,128]{1,0:T(8,128)(2,1)S(1)}, u32[]{:S(2)}, u32[]{:S(2)}) %collective-permute-start.11) | collective-permute-done | bytes 524320 | tf_op jit(solution)/shard_map/ppermute | solution.py:35
  132.5 0.1 add_convert_fusion.3
  132.6 2.1 %collective-permute-start.12 = (bf16[2048,128]{1,0:T(8,128)(2,1)S(1)}, bf16[2048,128]{1,0:T(8,128)(2,1)S(1)}, u32[]{:S(2)}, u32[]{:S(2)}) collective-permute-start(bf16[2048,128]{1,0:T(8,128)(2,1)S(1)} %add_convert_fusion.3), channel_id=1, source_target_pairs={{0,14},{1,3},{2,0},{3,5},{4,2},{5,7},{6,4},{7,9},{8,6},{9,11},{10,... | collective-permute-start | bytes 1572872 | tf_op jit(solution)/shard_map/ppermute | solution.py:35
  134.7 6.0 %share.4 = (f32[2048,128]{1,0:T(8,128)S(1)}, f32[2048,128]{1,0:T(8,128)S(1)}) custom-call(s32[1]{0:T(128)} %bitcast.core_ref, bf16[2048,128]{1,0:T(8,128)(2,1)} %collective-permute-done.refs_0_, bf16[2048,128]{1,0:T(8,128)(2,1)S(1)} %norm.1.refs_1_, bf16[4,704,512]{2,1,0:T(8,128)(2,1)S(1)} %all_to_all.16.refs_2_, ...), custom_call_target="tpu_custom_call" | custom-call | tf_op jit(solution)/shard_map/share/pallas_call | solution.py:117
  140.7 0.1 collective-permute-start.17
  140.8 3.8 %collective-permute-done.12 = bf16[2048,128]{1,0:T(8,128)(2,1)S(1)} collective-permute-done((bf16[2048,128]{1,0:T(8,128)(2,1)S(1)}, bf16[2048,128]{1,0:T(8,128)(2,1)S(1)}, u32[]{:S(2)}, u32[]{:S(2)}) %collective-permute-start.12) | collective-permute-done | bytes 524320 | tf_op jit(solution)/shard_map/ppermute | solution.py:35
  144.6 0.1 add_convert_fusion.2
  144.8 1.3 collective-permute-start.13
  146.1 8.0 %collective-permute-done.13.first = bf16[2048,128]{1,0:T(8,128)(2,1)S(1)} collective-permute-done((bf16[2048,128]{1,0:T(8,128)(2,1)S(1)}, bf16[2048,128]{1,0:T(8,128)(2,1)S(1)}, u32[]{:S(2)}, u32[]{:S(2)}) %collective-permute-start.13) | collective-permute-done | bytes 524320 | tf_op jit(solution)/shard_map/ppermute | solution.py:35
  154.0 1.0 close.1
  (12 shorter events, 0.0 us)
Async XLA Ops:
  16.2 1.2 copy-start
  42.3 57.9 %collective-permute-start.1 = (bf16[4,704,512]{2,1,0:T(8,128)(2,1)S(1)}, bf16[4,704,512]{2,1,0:T(8,128)(2,1)}, u32[]{:S(2)}, u32[]{:S(2)}) collective-permute-start(bf16[4,704,512]{2,1,0:T(8,128)(2,1)S(1)} %all_to_all.16.refs_2_), channel_id=1, source_target_pairs={{0,1},{1,0},{2,3},{3,2},{4,5},{5,4},{6,7},{7,6},{8,9},{9,8},{10,11... | collective-permute-start | bytes 8650760 | tf_op jit(solution)/shard_map/ppermute | solution.py:39
  42.3 4.5 %copy-start.2 = (f32[2048]{0:T(1024)S(1)}, f32[2048]{0:T(1024)}, u32[]{:S(2)}) copy-start(f32[2048]{0:T(1024)} %param.6) | copy-start | bytes 24580
  42.3 19.1 %all-to-all-start.2 = ((bf16[4,512,384]{2,1,0:T(8,128)(2,1)}), bf16[4,512,384]{2,1,0:T(8,128)(2,1)}, u32[]{:S(2)}, u32[]{:S(2)}) async-start(bf16[4,512,384]{2,1,0:T(8,128)(2,1)} %copy-done), calls=%async_computation.2 | async-start | bytes 3145728 | tf_op jit(solution)/shard_map/all_to_all | solution.py:43
  46.8 1.0 copy-start.1
  48.2 13.2 %collective-permute-start = (bf16[2048,128]{1,0:T(8,128)(2,1)S(1)}, bf16[2048,128]{1,0:T(8,128)(2,1)}, u32[]{:S(2)}, u32[]{:S(2)}) collective-permute-start(bf16[2048,128]{1,0:T(8,128)(2,1)S(1)} %norm.1.refs_1_), channel_id=1, source_target_pairs={{0,2},{1,15},{2,4},{3,1},{4,6},{5,3},{6,8},{7,5},{8,10},{9,7},{10,... | collective-permute-start | bytes 1572872 | tf_op jit(solution)/shard_map/ppermute | solution.py:35
  50.2 11.2 %collective-permute-start.6 = (bf16[2048,128]{1,0:T(8,128)(2,1)S(1)}, bf16[2048,128]{1,0:T(8,128)(2,1)}, u32[]{:S(2)}, u32[]{:S(2)}) collective-permute-start(bf16[2048,128]{1,0:T(8,128)(2,1)S(1)} %norm.1.refs_1_), channel_id=1, source_target_pairs={{0,1},{1,0},{2,3},{3,2},{4,5},{5,4},{6,7},{7,6},{8,9},{9,8},{10,11... | collective-permute-start | bytes 1572872 | tf_op jit(solution)/shard_map/ppermute | solution.py:39
  61.4 10.7 %collective-permute-start.3 = (bf16[2048,128]{1,0:T(8,128)(2,1)}, bf16[2048,128]{1,0:T(8,128)(2,1)}, u32[]{:S(2)}, u32[]{:S(2)}) collective-permute-start(bf16[2048,128]{1,0:T(8,128)(2,1)} %collective-permute-done.refs_0_), channel_id=1, source_target_pairs={{0,2},{1,15},{2,4},{3,1},{4,6},{5,3},{6,8},{7,5},{8,10},{9,7},{10,... | collective-permute-start | bytes 1572872 | tf_op jit(solution)/shard_map/ppermute | solution.py:35
  61.4 16.3 %collective-permute-start.7 = (bf16[2048,128]{1,0:T(8,128)(2,1)}, bf16[2048,128]{1,0:T(8,128)(2,1)}, u32[]{:S(2)}, u32[]{:S(2)}) collective-permute-start(bf16[2048,128]{1,0:T(8,128)(2,1)} %collective-permute-done.6), channel_id=1, source_target_pairs={{0,2},{1,15},{2,4},{3,1},{4,6},{5,3},{6,8},{7,5},{8,10},{9,7},{10,... | collective-permute-start | bytes 1572872 | tf_op jit(solution)/shard_map/ppermute | solution.py:35
  61.4 38.8 %collective-permute-start.2 = (bf16[4,512,384]{2,1,0:T(8,128)(2,1)}, bf16[4,512,384]{2,1,0:T(8,128)(2,1)}, u32[]{:S(2)}, u32[]{:S(2)}) collective-permute-start(bf16[4,512,384]{2,1,0:T(8,128)(2,1)} %all-to-all-done.2.refs_3_), channel_id=1, source_target_pairs={{0,1},{1,0},{2,3},{3,2},{4,5},{5,4},{6,7},{7,6},{8,9},{9,8},{10,11... | collective-permute-start | bytes 4718600 | tf_op jit(solution)/shard_map/ppermute | solution.py:39
  72.1 11.2 %collective-permute-start.4 = (bf16[2048,128]{1,0:T(8,128)(2,1)}, bf16[2048,128]{1,0:T(8,128)(2,1)}, u32[]{:S(2)}, u32[]{:S(2)}) collective-permute-start(bf16[2048,128]{1,0:T(8,128)(2,1)} %collective-permute-done.3.refs_0_), channel_id=1, source_target_pairs={{0,2},{1,15},{2,4},{3,1},{4,6},{5,3},{6,8},{7,5},{8,10},{9,7},{10,... | collective-permute-start | bytes 1572872 | tf_op jit(solution)/shard_map/ppermute | solution.py:35
  77.7 11.2 %collective-permute-start.8 = (bf16[2048,128]{1,0:T(8,128)(2,1)}, bf16[2048,128]{1,0:T(8,128)(2,1)}, u32[]{:S(2)}, u32[]{:S(2)}) collective-permute-start(bf16[2048,128]{1,0:T(8,128)(2,1)} %collective-permute-done.7.refs_1_), channel_id=1, source_target_pairs={{0,2},{1,15},{2,4},{3,1},{4,6},{5,3},{6,8},{7,5},{8,10},{9,7},{10,... | collective-permute-start | bytes 1572872 | tf_op jit(solution)/shard_map/ppermute | solution.py:35
  83.4 11.2 %collective-permute-start.5 = (bf16[2048,128]{1,0:T(8,128)(2,1)}, bf16[2048,128]{1,0:T(8,128)(2,1)}, u32[]{:S(2)}, u32[]{:S(2)}) collective-permute-start(bf16[2048,128]{1,0:T(8,128)(2,1)} %collective-permute-done.4.refs_0_), channel_id=1, source_target_pairs={{0,2},{1,15},{2,4},{3,1},{4,6},{5,3},{6,8},{7,5},{8,10},{9,7},{10,... | collective-permute-start | bytes 1572872 | tf_op jit(solution)/shard_map/ppermute | solution.py:35
  89.0 11.2 %collective-permute-start.9 = (bf16[2048,128]{1,0:T(8,128)(2,1)}, bf16[2048,128]{1,0:T(8,128)(2,1)}, u32[]{:S(2)}, u32[]{:S(2)}) collective-permute-start(bf16[2048,128]{1,0:T(8,128)(2,1)} %collective-permute-done.8.refs_1_), channel_id=1, source_target_pairs={{0,2},{1,15},{2,4},{3,1},{4,6},{5,3},{6,8},{7,5},{8,10},{9,7},{10,... | collective-permute-start | bytes 1572872 | tf_op jit(solution)/shard_map/ppermute | solution.py:35
  106.4 9.3 %collective-permute-start.14 = (bf16[2048,128]{1,0:T(8,128)(2,1)S(1)}, bf16[2048,128]{1,0:T(8,128)(2,1)S(1)}, u32[]{:S(2)}, u32[]{:S(2)}) collective-permute-start(bf16[2048,128]{1,0:T(8,128)(2,1)S(1)} %get-tuple-element.22), channel_id=1, source_target_pairs={{0,14},{1,3},{2,0},{3,5},{4,2},{5,7},{6,4},{7,9},{8,6},{9,11},{10,... | collective-permute-start | bytes 1572872 | tf_op jit(solution)/shard_map/ppermute | solution.py:35
  107.2 14.0 %collective-permute-start.10 = (bf16[2048,128]{1,0:T(8,128)(2,1)S(1)}, bf16[2048,128]{1,0:T(8,128)(2,1)S(1)}, u32[]{:S(2)}, u32[]{:S(2)}) collective-permute-start(bf16[2048,128]{1,0:T(8,128)(2,1)S(1)} %get-tuple-element.18), channel_id=1, source_target_pairs={{0,14},{1,3},{2,0},{3,5},{4,2},{5,7},{6,4},{7,9},{8,6},{9,11},{10,... | collective-permute-start | bytes 1572872 | tf_op jit(solution)/shard_map/ppermute | solution.py:35
  115.8 13.8 %collective-permute-start.15 = (bf16[2048,128]{1,0:T(8,128)(2,1)S(1)}, bf16[2048,128]{1,0:T(8,128)(2,1)S(1)}, u32[]{:S(2)}, u32[]{:S(2)}) collective-permute-start(bf16[2048,128]{1,0:T(8,128)(2,1)S(1)} %add_convert_fusion.1), channel_id=1, source_target_pairs={{0,14},{1,3},{2,0},{3,5},{4,2},{5,7},{6,4},{7,9},{8,6},{9,11},{10,... | collective-permute-start | bytes 1572872 | tf_op jit(solution)/shard_map/ppermute | solution.py:35
  121.4 11.1 %collective-permute-start.11 = (bf16[2048,128]{1,0:T(8,128)(2,1)S(1)}, bf16[2048,128]{1,0:T(8,128)(2,1)S(1)}, u32[]{:S(2)}, u32[]{:S(2)}) collective-permute-start(bf16[2048,128]{1,0:T(8,128)(2,1)S(1)} %add_convert_fusion.4), channel_id=1, source_target_pairs={{0,14},{1,3},{2,0},{3,5},{4,2},{5,7},{6,4},{7,9},{8,6},{9,11},{10,... | collective-permute-start | bytes 1572872 | tf_op jit(solution)/shard_map/ppermute | solution.py:35
  129.8 10.9 %collective-permute-start.16 = (bf16[2048,128]{1,0:T(8,128)(2,1)S(1)}, bf16[2048,128]{1,0:T(8,128)(2,1)S(1)}, u32[]{:S(2)}, u32[]{:S(2)}) collective-permute-start(bf16[2048,128]{1,0:T(8,128)(2,1)S(1)} %add_convert_fusion), channel_id=1, source_target_pairs={{0,14},{1,3},{2,0},{3,5},{4,2},{5,7},{6,4},{7,9},{8,6},{9,11},{10,... | collective-permute-start | bytes 1572872 | tf_op jit(solution)/shard_map/ppermute | solution.py:35
  132.6 12.0 %collective-permute-start.12 = (bf16[2048,128]{1,0:T(8,128)(2,1)S(1)}, bf16[2048,128]{1,0:T(8,128)(2,1)S(1)}, u32[]{:S(2)}, u32[]{:S(2)}) collective-permute-start(bf16[2048,128]{1,0:T(8,128)(2,1)S(1)} %add_convert_fusion.3), channel_id=1, source_target_pairs={{0,14},{1,3},{2,0},{3,5},{4,2},{5,7},{6,4},{7,9},{8,6},{9,11},{10,... | collective-permute-start | bytes 1572872 | tf_op jit(solution)/shard_map/ppermute | solution.py:35
  140.7 5.4 %collective-permute-start.17 = (bf16[2048,128]{1,0:T(8,128)(2,1)S(1)}, bf16[2048,128]{1,0:T(8,128)(2,1)S(1)}, u32[]{:S(2)}, u32[]{:S(2)}) collective-permute-start(bf16[2048,128]{1,0:T(8,128)(2,1)S(1)} %collective-permute-done.16), channel_id=1, source_target_pairs={{0,1},{1,0},{2,3},{3,2},{4,5},{5,4},{6,7},{7,6},{8,9},{9,8},{10,11... | collective-permute-start | bytes 1572872 | tf_op jit(solution)/shard_map/ppermute | solution.py:39
  144.8 9.3 %collective-permute-start.13 = (bf16[2048,128]{1,0:T(8,128)(2,1)S(1)}, bf16[2048,128]{1,0:T(8,128)(2,1)S(1)}, u32[]{:S(2)}, u32[]{:S(2)}) collective-permute-start(bf16[2048,128]{1,0:T(8,128)(2,1)S(1)} %add_convert_fusion.2), channel_id=1, source_target_pairs={{0,14},{1,3},{2,0},{3,5},{4,2},{5,7},{6,4},{7,9},{8,6},{9,11},{10,... | collective-permute-start | bytes 1572872 | tf_op jit(solution)/shard_map/ppermute | solution.py:35
where the time goes:
time: 157 us; the launch traced here: 155 us
  waiting for transfers between devices  59.9 us (38%)
  blocking collectives  39.2 us (25%)
  Pallas kernels  26.5 us (17%)
  starting transfers between devices  25.2 us (16%)
  local copies, waits for them, and re-layouts  2.34 us (1%)
  other arithmetic  1.67 us (1%)
    ppermute x14, waiting for transfers between devices, onward(): return lax.ppermute(x, ('z', 'c'), pairs)  59.9 us
    all_to_all x2, blocking collectives, from_four(): lax.all_to_all(copies, AXES, 0, 0, axis_index_groups=groups, tiled=True)  39.2 us
    pallas_call x4, Pallas kernels, share(): pl.pallas_call(functools.partial(share_body, n, units), out_shape=[jax.Sh...  24.4 us
    ppermute x14, starting transfers between devices, onward(): return lax.ppermute(x, ('z', 'c'), pairs)  11.6 us
    ppermute x4, starting transfers between devices, swap(): return lax.ppermute(x, 'c', [(0, 1), (1, 0)])  9.17 us
    all_to_all x1, starting transfers between devices, from_four(): lax.all_to_all(copies, AXES, 0, 0, axis_index_groups=groups, tiled=True)  4.48 us
  transfers between devices with their start and end apart: 19, of which 12 were waited for; matrix products, arithmetic and copies ran while one was open for 0% of the time, Pallas kernels for 12%

commit v1 on v0

v1 whole, which is shorter than its diff:
```python
import functools

import jax
import jax.numpy as jnp
from jax import lax
from jax.experimental import pallas as pl
from jax.experimental.pallas import tpu as pltpu
from jax.sharding import Mesh, PartitionSpec as P


eps_floor = 0.05
X, Y, Z = 4, 4, 8
AXES = ("y", "x", "z", "c")
LANES = 128
f32, bf16 = jnp.float32, jnp.bfloat16


def place(y, x, z, c):
    return ((y * X + x) * Z + z) * 2 + c


def rows_and_columns():
    along_x = lambda c: [[place(y, x, z, c) for x in range(X)] for y in range(Y) for z in range(Z)]
    along_y = lambda c: [[place(y, x, z, c) for y in range(Y)] for x in range(X) for z in range(Z)]
    return along_x(0) + along_y(1), along_y(0) + along_x(1)


FIRST, SECOND = rows_and_columns()
WHOLE = pl.BlockSpec(memory_space=pltpu.VMEM)
LARGE = pltpu.CompilerParams(vmem_limit_bytes=60 << 20)
SMALL = pltpu.CompilerParams(vmem_limit_bytes=12 << 20)


def onward(x, by):
    pairs = [(2 * z + c, 2 * ((z + (by if c == 0 else -by)) % Z) + c) for z in range(Z) for c in range(2)]
    return lax.ppermute(x, ("z", "c"), pairs)


def swap(x):
    return lax.ppermute(x, "c", [(0, 1), (1, 0)])


def from_four(copies, groups):
    return lax.all_to_all(copies, AXES, 0, 0, axis_index_groups=groups, tiled=True)


def norm_body(tokens, gain, out):
    values = tokens[...].astype(f32)
    factor = lax.rsqrt(jnp.mean(values * values, axis=-1, keepdims=True) + eps_floor)
    out[...] = (values * factor * gain[...]).T.astype(bf16)


def norm(tokens, gain):
    return pl.pallas_call(
        norm_body,
        out_shape=jax.ShapeDtypeStruct(tokens.shape[::-1], bf16),
        in_specs=[WHOLE, WHOLE],
        out_specs=WHOLE,
        compiler_params=SMALL,
        name="norm",
    )(tokens, gain[None])


def repeat(packed, out, sems):
    copies = [pltpu.make_async_copy(packed, out.at[k], sems.at[k]) for k in range(4)]
    for c in copies:
        c.start()
    for c in copies:
        c.wait()


def repeated(body, shape, *operands, room=SMALL):
    return pl.pallas_call(
        body,
        out_shape=jax.ShapeDtypeStruct((4, *shape), bf16),
        in_specs=[WHOLE] * len(operands),
        out_specs=pl.BlockSpec(memory_space=pltpu.HBM),
        scratch_shapes=[pltpu.VMEM(shape, bf16), pltpu.SemaphoreType.DMA((4,))],
        compiler_params=room,
    )(*operands)


def pack_body(gate, upper, down, out, packed, sems):
    units = gate.shape[0]
    packed[:units] = gate[...]
    packed[units : 2 * units] = upper[...]
    for at in range(0, units, LANES):
        n = min(LANES, units - at)
        rows = slice(2 * units + at, 2 * units + at + LANES)
        packed[rows, :n] = down[at : at + n].T
        if n < LANES:
            packed[rows, n:] = jnp.zeros((LANES, LANES - n), bf16)
    repeat(packed, out, sems)


def pack(gate, upper, down):
    rows = 2 * gate.shape[0] + pl.cdiv(gate.shape[0], LANES) * LANES
    return repeated(pack_body, (rows, LANES), gate, upper, down)


def spread_body(blocks, out, packed, sems):
    for k in range(4):
        packed[:, LANES * k : LANES * (k + 1)] = blocks[k]
    repeat(packed, out, sems)


def spread(blocks):
    return repeated(spread_body, (blocks.shape[1], 4 * LANES), blocks, room=LARGE)


def hold_body(source, out, sem):
    copy = pltpu.make_async_copy(source, out, sem)
    copy.start()
    copy.wait()


def hold(x):
    return pl.pallas_call(
        hold_body,
        out_shape=jax.ShapeDtypeStruct(x.shape, x.dtype),
        in_specs=[pl.BlockSpec(memory_space=pltpu.HBM)],
        out_specs=WHOLE,
        scratch_shapes=[pltpu.SemaphoreType.DMA],
        compiler_params=SMALL,
        name="hold",
    )(x)


def order(core, b, w):
    return jnp.where(core == w, b, (b % 4) * 4 + b // 4)


def half_hidden(core, w, units, pieces, weights, turned):
    m, depth = pieces[0].shape[1], weights.shape[2]
    for b in range(turned.shape[0] // LANES):
        at = pl.ds(pl.multiple_of(order(core, b, w) * LANES, LANES), LANES)
        for i, piece in enumerate(pieces):
            turned[LANES * b : LANES * (b + 1), m * i : m * (i + 1)] = piece[at, :]
    both = jnp.dot(weights[0, : 2 * units], turned[:depth], preferred_element_type=f32)
    for k in range(1, 4):
        both += jnp.dot(weights[k, : 2 * units], turned[depth * k : depth * (k + 1)], preferred_element_type=f32)
    gate, upper = both[:units], both[units:]
    return (gate / (1.0 + jnp.exp(-gate)) * upper).astype(bf16)


def begin_body(n, units, core_ref, *refs):
    pieces, weights, out, turned = refs[:n], refs[n], refs[n + 1], refs[n + 2]
    out[...] = half_hidden(core_ref[0], 0, units, pieces, weights, turned)


def finish_body(n, units, core_ref, *refs):
    pieces, weights, first, outs, turned = refs[:n], refs[n : n + 2], refs[n + 2], refs[n + 3 : 2 * n + 3], refs[2 * n + 3]
    core, m = core_ref[0], pieces[0].shape[1]
    hidden = first[...], half_hidden(core, 1, units, pieces, weights[1], turned)
    for b in range(turned.shape[0] // LANES):
        part = 0.0
        for w in (0, 1):
            at = order(core, b, w)
            lanes = pl.ds(pl.multiple_of(at % 4 * LANES, LANES), LANES)
            tiles = [weights[w][at // 4, r : r + LANES, lanes] for r in range(2 * units, weights[w].shape[1], LANES)]
            part += jnp.dot(jnp.concatenate(tiles, axis=1)[:, :units], hidden[w], preferred_element_type=f32)
        for i in range(n):
            outs[i][LANES * b : LANES * (b + 1), :] = part[:, m * i : m * (i + 1)].astype(outs[i].dtype)


def call(body, units, core, pieces, rest, out_shape):
    n, (features, m) = len(pieces), pieces[0].shape
    return pl.pallas_call(
        functools.partial(body, n, units),
        out_shape=out_shape,
        in_specs=[pl.BlockSpec(memory_space=pltpu.SMEM)] + [WHOLE] * (n + len(rest)),
        out_specs=jax.tree.map(lambda _: WHOLE, out_shape),
        scratch_shapes=[pltpu.VMEM((features, n * m), bf16)],
        compiler_params=pltpu.CompilerParams(vmem_limit_bytes=18 << 20),
    )(core, *pieces, *rest)


def begin(units, core, pieces, weights):
    n, m = len(pieces), pieces[0].shape[1]
    return call(begin_body, units, core, pieces, [weights], jax.ShapeDtypeStruct((units, n * m), bf16))


def finish(units, core, pieces, weights, first, dtype):
    out_shape = [jax.ShapeDtypeStruct(p.shape, dtype) for p in pieces]
    return call(finish_body, units, core, pieces, [*weights, first], out_shape)


def close_body(own, first, second, out):
    out[...] = (own[...] + first[...].astype(f32) + second[...].astype(f32)).T.astype(bf16)


def close(own, first, second):
    return pl.pallas_call(
        close_body,
        out_shape=jax.ShapeDtypeStruct(own.shape[::-1], bf16),
        in_specs=[WHOLE] * 3,
        out_specs=WHOLE,
        compiler_params=SMALL,
        name="close",
    )(own, first, second)


def local(tokens, norm_gain, gate_weight, up_weight, down_weight):
    core = lax.axis_index("c").astype(jnp.int32)[None]
    normed = norm(tokens, norm_gain)

    own, mate = {0: normed}, {0: swap(normed)}
    for d in (1, 2, 3, 4):
        own[d] = onward(own[d - 1], 1)
        if d < 4:
            mate[d] = onward(mate[d - 1], 1)

    rows = from_four(pack(gate_weight.T, up_weight.T, down_weight), FIRST)
    columns = from_four(spread(rows), SECOND)
    other = swap(columns)
    columns = hold(columns)
    weights = columns, hold(other)

    units = down_weight.shape[0]
    groups = [(own[4], mate[3]), (own[3], mate[2]), (own[2], mate[1]), (own[1], own[0])]
    firsts = []
    for g in groups:
        firsts.append(begin(units, core, g, columns))
    dtypes = [bf16, f32, f32, f32]
    shares = [finish(units, core, g, weights, f, t) for g, f, t in zip(groups, firsts, dtypes)]
    (own4, mate3), (own3, mate2), (own2, mate1), (own1, own0) = shares

    def send(x):
        return onward(x.astype(bf16), -1)

    got_own = send(own4)
    got_mate = send(mate3)
    got_own = send(got_own.astype(f32) + own3)
    got_mate = send(got_mate.astype(f32) + mate2)
    got_own = send(got_own.astype(f32) + own2)
    got_mate = send(got_mate.astype(f32) + mate1)
    got_own = send(got_own.astype(f32) + own1)
    return close(own0, got_own, swap(got_mate))


def solution(mesh):
    fine = Mesh(mesh.devices.reshape(Y, X, Z, 2), AXES)
    fs, tp = ("y", "x"), ("z", "c")

    return jax.shard_map(
        local,
        mesh=fine,
        in_specs=(P(fs + tp, None), P(), P(fs, tp), P(fs, tp), P(tp, fs)),
        out_specs=P(fs + tp, None),
        check_vma=False,
    )
```

time: 157 us -> 163 us (1.038)
  blocking collectives: 39.2 us -> 50.4 us
  starting transfers between devices: 25.2 us -> 15.6 us
  Pallas kernels: 26.5 us -> 30.3 us
  waiting for transfers between devices: 59.9 us -> 61.9 us
    all_to_all x2, blocking collectives: 39.2 us -> 50.4 us  [from_four(): lax.all_to_all(copies, AXES, 0, 0, axis_index_groups=groups, tiled=True)]
    ppermute x4 -> x3, starting transfers between devices: 9.17 us -> 4.17 us  [swap(): return lax.ppermute(x, 'c', [(0, 1), (1, 0)])]
    all_to_all x1 -> x0, starting transfers between devices: 4.48 us -> none  [from_four(): lax.all_to_all(copies, AXES, 0, 0, axis_index_groups=groups, tiled=True)]
    pallas_call x5 -> x12, Pallas kernels: 25.1 us -> 28.9 us  [the longest x8 20.6 us: call(): pl.pallas_call(functools.partial(body, n, units), out_shape=out_shape, in...]
    ppermute x14, waiting for transfers between devices: 59.9 us -> 61.8 us  [onward(): return lax.ppermute(x, ('z', 'c'), pairs)]
  transfers between devices with their start and end apart: 19 -> 17, of which waited for: 12 -> 12; matrix products, arithmetic and copies ran while one was open for 0% -> 0% of each run, Pallas kernels for 12% -> 11%
where the time goes in v1:
time: 163 us; the launch traced here: 162 us
  waiting for transfers between devices  61.9 us (38%)
  blocking collectives  50.4 us (31%)
  Pallas kernels  30.3 us (19%)
  starting transfers between devices  15.6 us (10%)
  local copies, waits for them, and re-layouts  2.68 us (2%)
    ppermute x14, waiting for transfers between devices, onward(): return lax.ppermute(x, ('z', 'c'), pairs)  61.8 us
    all_to_all x2, blocking collectives, from_four(): lax.all_to_all(copies, AXES, 0, 0, axis_index_groups=groups, tiled=True)  50.4 us
    pallas_call x8, Pallas kernels, call(): pl.pallas_call(functools.partial(body, n, units), out_shape=out_shape, in...  20.6 us
    ppermute x14, starting transfers between devices, onward(): return lax.ppermute(x, ('z', 'c'), pairs)  11.4 us
    pallas_call x2, Pallas kernels, hold(): pl.pallas_call(hold_body, out_shape=jax.ShapeDtypeStruct(x.shape, x.dtype...  4.54 us
    ppermute x3, starting transfers between devices, swap(): return lax.ppermute(x, 'c', [(0, 1), (1, 0)])  4.17 us
    pallas_call x2, Pallas kernels, repeated(): pl.pallas_call(body, out_shape=jax.ShapeDtypeStruct((4, *shape), bf16), i...  3.83 us
  transfers between devices with their start and end apart: 17, of which 12 were waited for; matrix products, arithmetic and copies ran while one was open for 0% of the time, Pallas kernels for 11%

profile of v1, /device:TPU:2, one launch (start us, length us, event | category | flops | bytes accessed | tf_op | source)
XLA Modules:
  0.0 161.6 jit_solution(6895499029153102748)
XLA Ops:
  0.0 0.9 copy-done.1
  0.9 0.9 copy-done.2
  1.8 0.9 copy-done.3
  2.7 0.3 shard_map.55
  3.0 15.2 %all_to_all.10.blocks = bf16[4,1088,128]{2,1,0:T(8,128)(2,1)} all-to-all(bf16[4,1088,128]{2,1,0:T(8,128)(2,1)S(1)} %shard_map.55), channel_id=1, replica_groups={{0,16,32,48},{2,18,34,50},{4,20,36,52},{6,22,38,54},{8,24,40,56},{10,26..., dimensions={0} | all-to-all | bytes 2228224 | tf_op jit(solution)/shard_map/all_to_all | solution.py:44
  18.1 3.5 %shard_map.56 = bf16[4,1088,512]{2,1,0:T(8,128)(2,1)} custom-call(bf16[4,1088,128]{2,1,0:T(8,128)(2,1)} %all_to_all.10.blocks), custom_call_target="tpu_custom_call" | custom-call | tf_op jit(solution)/shard_map/pallas_call | solution.py:73
  21.7 0.0 copy-start
  21.7 0.0 copy-start.4
  21.7 35.2 %all_to_all.11.source = bf16[4,1088,512]{2,1,0:T(8,128)(2,1)} all-to-all(bf16[4,1088,512]{2,1,0:T(8,128)(2,1)} %shard_map.56), channel_id=1, replica_groups={{0,64,128,192},{2,66,130,194},{4,68,132,196},{6,70,134,198},{8,72,136,2..., dimensions={0} | all-to-all | bytes 8912896 | tf_op jit(solution)/shard_map/all_to_all | solution.py:44
  57.0 0.4 norm.1.refs_1_
  57.3 1.3 collective-permute-start
  58.7 4.2 %collective-permute-start.5 = (bf16[2048,128]{1,0:T(8,128)(2,1)S(1)}, bf16[2048,128]{1,0:T(8,128)(2,1)S(1)}, u32[]{:S(2)}, u32[]{:S(2)}) collective-permute-start(bf16[2048,128]{1,0:T(8,128)(2,1)S(1)} %norm.1.refs_1_), channel_id=1, source_target_pairs={{0,1},{1,0},{2,3},{3,2},{4,5},{5,4},{6,7},{7,6},{8,9},{9,8},{10,11... | collective-permute-start | bytes 1572872 | tf_op jit(solution)/shard_map/ppermute | solution.py:40
  62.8 6.9 %collective-permute-done.refs_0_ = bf16[2048,128]{1,0:T(8,128)(2,1)S(1)} collective-permute-done((bf16[2048,128]{1,0:T(8,128)(2,1)S(1)}, bf16[2048,128]{1,0:T(8,128)(2,1)S(1)}, u32[]{:S(2)}, u32[]{:S(2)}) %collective-permute-start) | collective-permute-done | bytes 524320 | tf_op jit(solution)/shard_map/ppermute | solution.py:36
  69.8 0.0 collective-permute-start.2
  69.8 10.4 %collective-permute-done.2.refs_0_ = bf16[2048,128]{1,0:T(8,128)(2,1)S(1)} collective-permute-done((bf16[2048,128]{1,0:T(8,128)(2,1)S(1)}, bf16[2048,128]{1,0:T(8,128)(2,1)S(1)}, u32[]{:S(2)}, u32[]{:S(2)}) %collective-permute-start.2) | collective-permute-done | bytes 524320 | tf_op jit(solution)/shard_map/ppermute | solution.py:36
  80.2 5.6 %collective-permute-done.6.refs_1_ = bf16[2048,128]{1,0:T(8,128)(2,1)S(1)} collective-permute-done((bf16[2048,128]{1,0:T(8,128)(2,1)S(1)}, bf16[2048,128]{1,0:T(8,128)(2,1)S(1)}, u32[]{:S(2)}, u32[]{:S(2)}) %collective-permute-start.6) | collective-permute-done | bytes 524320 | tf_op jit(solution)/shard_map/ppermute | solution.py:36
  85.8 5.6 %collective-permute-done.3.refs_0_ = bf16[2048,128]{1,0:T(8,128)(2,1)S(1)} collective-permute-done((bf16[2048,128]{1,0:T(8,128)(2,1)S(1)}, bf16[2048,128]{1,0:T(8,128)(2,1)S(1)}, u32[]{:S(2)}, u32[]{:S(2)}) %collective-permute-start.3) | collective-permute-done | bytes 524320 | tf_op jit(solution)/shard_map/ppermute | solution.py:36
  91.4 5.6 %collective-permute-done.7.refs_1_ = bf16[2048,128]{1,0:T(8,128)(2,1)S(1)} collective-permute-done((bf16[2048,128]{1,0:T(8,128)(2,1)S(1)}, bf16[2048,128]{1,0:T(8,128)(2,1)S(1)}, u32[]{:S(2)}, u32[]{:S(2)}) %collective-permute-start.7) | collective-permute-done | bytes 524320 | tf_op jit(solution)/shard_map/ppermute | solution.py:36
  97.0 2.3 %hold.2.refs_2_ = bf16[4,1088,512]{2,1,0:T(8,128)(2,1)S(1)} custom-call(bf16[4,1088,512]{2,1,0:T(8,128)(2,1)} %all_to_all.11.source), custom_call_target="tpu_custom_call" | custom-call | tf_op jit(solution)/shard_map/hold/pallas_call | solution.py:118
  99.3 3.4 %collective-permute-done.4.refs_0_ = bf16[2048,128]{1,0:T(8,128)(2,1)} collective-permute-done((bf16[2048,128]{1,0:T(8,128)(2,1)S(1)}, bf16[2048,128]{1,0:T(8,128)(2,1)}, u32[]{:S(2)}, u32[]{:S(2)}) %collective-permute-start.4) | collective-permute-done | bytes 524320 | tf_op jit(solution)/shard_map/ppermute | solution.py:36
  102.7 5.6 %collective-permute-done.8.refs_1_ = bf16[2048,128]{1,0:T(8,128)(2,1)} collective-permute-done((bf16[2048,128]{1,0:T(8,128)(2,1)S(1)}, bf16[2048,128]{1,0:T(8,128)(2,1)}, u32[]{:S(2)}, u32[]{:S(2)}) %collective-permute-start.8) | collective-permute-done | bytes 524320 | tf_op jit(solution)/shard_map/ppermute | solution.py:36
  108.3 2.2 %shard_map.59.refs_4_ = bf16[352,256]{1,0:T(8,128)(2,1)S(1)} custom-call(s32[1]{0:T(128)} %bitcast.core_ref, bf16[2048,128]{1,0:T(8,128)(2,1)} %collective-permute-done.4.refs_0_, bf16[2048,128]{1,0:T(8,128)(2,1)} %collective-permute-done.8.refs_1_, bf16[4,1088,512]{2,1,0:T(8,128)(2,1)S(1)} %hold.2.refs_2_), custom_call_target="tpu_custom_call" | custom-call | tf_op jit(solution)/shard_map/pallas_call | solution.py:168
  110.6 2.3 %hold.3.refs_3_ = bf16[4,1088,512]{2,1,0:T(8,128)(2,1)S(1)} custom-call(bf16[4,1088,512]{2,1,0:T(8,128)(2,1)} %collective-permute-done.1.source), custom_call_target="tpu_custom_call" | custom-call | tf_op jit(solution)/shard_map/hold/pallas_call | solution.py:118
  112.8 4.7 %shard_map.60 = (bf16[2048,128]{1,0:T(8,128)(2,1)S(1)}, bf16[2048,128]{1,0:T(8,128)(2,1)S(1)}) custom-call(s32[1]{0:T(128)} %bitcast.core_ref, bf16[2048,128]{1,0:T(8,128)(2,1)} %collective-permute-done.4.refs_0_, bf16[2048,128]{1,0:T(8,128)(2,1)} %collective-permute-done.8.refs_1_, bf16[4,1088,512]{2,1,0:T(8,128)(2,1)S(1)} %hold.2.refs_2_, ...), custom_call_target="tpu_custom_call" | custom-call | tf_op jit(solution)/shard_map/pallas_call | solution.py:168
  117.6 0.9 collective-permute-start.9
  118.5 1.0 collective-permute-start.13
  119.5 1.0 shard_map.61.refs_4_
  120.5 3.5 %shard_map.62 = (f32[2048,128]{1,0:T(8,128)S(1)}, f32[2048,128]{1,0:T(8,128)S(1)}) custom-call(s32[1]{0:T(128)} %bitcast.core_ref, bf16[2048,128]{1,0:T(8,128)(2,1)S(1)} %collective-permute-done.3.refs_0_, bf16[2048,128]{1,0:T(8,128)(2,1)S(1)} %collective-permute-done.7.refs_1_, bf16[4,1088,512]{2,1,0:T(8,128)(2,1)S(1)} %hold.2.refs_2_, ...), custom_call_target="tpu_custom_call" | custom-call | tf_op jit(solution)/shard_map/pallas_call | solution.py:168
  124.1 2.8 %collective-permute-done.9 = bf16[2048,128]{1,0:T(8,128)(2,1)S(1)} collective-permute-done((bf16[2048,128]{1,0:T(8,128)(2,1)S(1)}, bf16[2048,128]{1,0:T(8,128)(2,1)S(1)}, u32[]{:S(2)}, u32[]{:S(2)}) %collective-permute-start.9) | collective-permute-done | bytes 524320 | tf_op jit(solution)/shard_map/ppermute | solution.py:36
  126.8 0.1 add_convert_fusion.4
  127.0 2.1 %collective-permute-start.10 = (bf16[2048,128]{1,0:T(8,128)(2,1)S(1)}, bf16[2048,128]{1,0:T(8,128)(2,1)S(1)}, u32[]{:S(2)}, u32[]{:S(2)}) collective-permute-start(bf16[2048,128]{1,0:T(8,128)(2,1)S(1)} %add_convert_fusion.4), channel_id=1, source_target_pairs={{0,14},{1,3},{2,0},{3,5},{4,2},{5,7},{6,4},{7,9},{8,6},{9,11},{10,... | collective-permute-start | bytes 1572872 | tf_op jit(solution)/shard_map/ppermute | solution.py:36
  129.0 3.4 %collective-permute-done.13 = bf16[2048,128]{1,0:T(8,128)(2,1)S(1)} collective-permute-done((bf16[2048,128]{1,0:T(8,128)(2,1)S(1)}, bf16[2048,128]{1,0:T(8,128)(2,1)S(1)}, u32[]{:S(2)}, u32[]{:S(2)}) %collective-permute-start.13) | collective-permute-done | bytes 524320 | tf_op jit(solution)/shard_map/ppermute | solution.py:36
  132.5 0.1 add_convert_fusion.1
  132.6 2.1 %collective-permute-start.14 = (bf16[2048,128]{1,0:T(8,128)(2,1)S(1)}, bf16[2048,128]{1,0:T(8,128)(2,1)S(1)}, u32[]{:S(2)}, u32[]{:S(2)}) collective-permute-start(bf16[2048,128]{1,0:T(8,128)(2,1)S(1)} %add_convert_fusion.1), channel_id=1, source_target_pairs={{0,14},{1,3},{2,0},{3,5},{4,2},{5,7},{6,4},{7,9},{8,6},{9,11},{10,... | collective-permute-start | bytes 1572872 | tf_op jit(solution)/shard_map/ppermute | solution.py:36
  134.7 1.0 shard_map.63.refs_4_
  135.7 3.5 %shard_map.64 = (f32[2048,128]{1,0:T(8,128)S(1)}, f32[2048,128]{1,0:T(8,128)S(1)}) custom-call(s32[1]{0:T(128)} %bitcast.core_ref, bf16[2048,128]{1,0:T(8,128)(2,1)S(1)} %collective-permute-done.2.refs_0_, bf16[2048,128]{1,0:T(8,128)(2,1)S(1)} %collective-permute-done.6.refs_1_, bf16[4,1088,512]{2,1,0:T(8,128)(2,1)S(1)} %hold.2.refs_2_, ...), custom_call_target="tpu_custom_call" | custom-call | tf_op jit(solution)/shard_map/pallas_call | solution.py:168
  139.2 0.1 add_convert_fusion.3
  139.3 0.9 collective-permute-start.11
  140.3 3.4 %collective-permute-done.14 = bf16[2048,128]{1,0:T(8,128)(2,1)S(1)} collective-permute-done((bf16[2048,128]{1,0:T(8,128)(2,1)S(1)}, bf16[2048,128]{1,0:T(8,128)(2,1)S(1)}, u32[]{:S(2)}, u32[]{:S(2)}) %collective-permute-start.14) | collective-permute-done | bytes 524320 | tf_op jit(solution)/shard_map/ppermute | solution.py:36
  143.7 0.1 add_convert_fusion
  143.8 2.3 %collective-permute-start.15 = (bf16[2048,128]{1,0:T(8,128)(2,1)S(1)}, bf16[2048,128]{1,0:T(8,128)(2,1)S(1)}, u32[]{:S(2)}, u32[]{:S(2)}) collective-permute-start(bf16[2048,128]{1,0:T(8,128)(2,1)S(1)} %add_convert_fusion), channel_id=1, source_target_pairs={{0,14},{1,3},{2,0},{3,5},{4,2},{5,7},{6,4},{7,9},{8,6},{9,11},{10,... | collective-permute-start | bytes 1572872 | tf_op jit(solution)/shard_map/ppermute | solution.py:36
  146.1 1.0 shard_map.57.refs_4_
  147.1 3.6 %shard_map.58 = (f32[2048,128]{1,0:T(8,128)S(1)}, f32[2048,128]{1,0:T(8,128)S(1)}) custom-call(s32[1]{0:T(128)} %bitcast.core_ref, bf16[2048,128]{1,0:T(8,128)(2,1)S(1)} %collective-permute-done.refs_0_, bf16[2048,128]{1,0:T(8,128)(2,1)S(1)} %norm.1.refs_1_, bf16[4,1088,512]{2,1,0:T(8,128)(2,1)S(1)} %hold.2.refs_2_, bf16[4,1088,512]{2,1,0:T(8,128)(2,1)S(1)} %hold.3.refs_3_, ...), custom_call_target="tpu_custom_call" | custom-call | tf_op jit(solution)/shard_map/pallas_call | solution.py:168
  150.7 0.1 add_convert_fusion.2
  150.8 0.7 collective-permute-start.12
  151.5 3.4 %collective-permute-done.15 = bf16[2048,128]{1,0:T(8,128)(2,1)S(1)} collective-permute-done((bf16[2048,128]{1,0:T(8,128)(2,1)S(1)}, bf16[2048,128]{1,0:T(8,128)(2,1)S(1)}, u32[]{:S(2)}, u32[]{:S(2)}) %collective-permute-start.15) | collective-permute-done | bytes 524320 | tf_op jit(solution)/shard_map/ppermute | solution.py:36
  154.9 5.6 %collective-permute-done.12.first = bf16[2048,128]{1,0:T(8,128)(2,1)S(1)} collective-permute-done((bf16[2048,128]{1,0:T(8,128)(2,1)S(1)}, bf16[2048,128]{1,0:T(8,128)(2,1)S(1)}, u32[]{:S(2)}, u32[]{:S(2)}) %collective-permute-start.12) | collective-permute-done | bytes 524320 | tf_op jit(solution)/shard_map/ppermute | solution.py:36
  160.6 1.0 close.1
  (17 shorter events, 0.0 us)
Async XLA Ops:
  0.0 0.9 copy-start.1
  0.9 0.9 copy-start.2
  1.8 0.9 copy-start.3
  21.7 35.3 %copy-start = (bf16[128,2048]{1,0:T(8,128)(2,1)S(1)}, bf16[128,2048]{1,0:T(8,128)(2,1)}, u32[]{:S(2)}) copy-start(bf16[128,2048]{1,0:T(8,128)(2,1)} %tokens.1) | copy-start | bytes 1572868
  21.7 35.2 %copy-start.4 = (f32[2048]{0:T(1024)S(1)}, f32[2048]{0:T(1024)}, u32[]{:S(2)}) copy-start(f32[2048]{0:T(1024)} %param.6) | copy-start | bytes 24580
  56.9 53.6 %collective-permute-start.1 = (bf16[4,1088,512]{2,1,0:T(8,128)(2,1)}, bf16[4,1088,512]{2,1,0:T(8,128)(2,1)}, u32[]{:S(2)}, u32[]{:S(2)}) collective-permute-start(bf16[4,1088,512]{2,1,0:T(8,128)(2,1)} %all_to_all.11.source), channel_id=1, source_target_pairs={{0,1},{1,0},{2,3},{3,2},{4,5},{5,4},{6,7},{7,6},{8,9},{9,8},{10,11... | collective-permute-start | bytes 13369352 | tf_op jit(solution)/shard_map/ppermute | solution.py:40
  57.3 12.4 %collective-permute-start = (bf16[2048,128]{1,0:T(8,128)(2,1)S(1)}, bf16[2048,128]{1,0:T(8,128)(2,1)S(1)}, u32[]{:S(2)}, u32[]{:S(2)}) collective-permute-start(bf16[2048,128]{1,0:T(8,128)(2,1)S(1)} %norm.1.refs_1_), channel_id=1, source_target_pairs={{0,2},{1,15},{2,4},{3,1},{4,6},{5,3},{6,8},{7,5},{8,10},{9,7},{10,... | collective-permute-start | bytes 1572872 | tf_op jit(solution)/shard_map/ppermute | solution.py:36
  58.7 11.1 %collective-permute-start.5 = (bf16[2048,128]{1,0:T(8,128)(2,1)S(1)}, bf16[2048,128]{1,0:T(8,128)(2,1)S(1)}, u32[]{:S(2)}, u32[]{:S(2)}) collective-permute-start(bf16[2048,128]{1,0:T(8,128)(2,1)S(1)} %norm.1.refs_1_), channel_id=1, source_target_pairs={{0,1},{1,0},{2,3},{3,2},{4,5},{5,4},{6,7},{7,6},{8,9},{9,8},{10,11... | collective-permute-start | bytes 1572872 | tf_op jit(solution)/shard_map/ppermute | solution.py:40
  69.8 10.4 %collective-permute-start.2 = (bf16[2048,128]{1,0:T(8,128)(2,1)S(1)}, bf16[2048,128]{1,0:T(8,128)(2,1)S(1)}, u32[]{:S(2)}, u32[]{:S(2)}) collective-permute-start(bf16[2048,128]{1,0:T(8,128)(2,1)S(1)} %collective-permute-done.refs_0_), channel_id=1, source_target_pairs={{0,2},{1,15},{2,4},{3,1},{4,6},{5,3},{6,8},{7,5},{8,10},{9,7},{10,... | collective-permute-start | bytes 1572872 | tf_op jit(solution)/shard_map/ppermute | solution.py:36
  69.8 16.0 %collective-permute-start.6 = (bf16[2048,128]{1,0:T(8,128)(2,1)S(1)}, bf16[2048,128]{1,0:T(8,128)(2,1)S(1)}, u32[]{:S(2)}, u32[]{:S(2)}) collective-permute-start(bf16[2048,128]{1,0:T(8,128)(2,1)S(1)} %collective-permute-done.5), channel_id=1, source_target_pairs={{0,2},{1,15},{2,4},{3,1},{4,6},{5,3},{6,8},{7,5},{8,10},{9,7},{10,... | collective-permute-start | bytes 1572872 | tf_op jit(solution)/shard_map/ppermute | solution.py:36
  80.2 11.2 %collective-permute-start.3 = (bf16[2048,128]{1,0:T(8,128)(2,1)S(1)}, bf16[2048,128]{1,0:T(8,128)(2,1)S(1)}, u32[]{:S(2)}, u32[]{:S(2)}) collective-permute-start(bf16[2048,128]{1,0:T(8,128)(2,1)S(1)} %collective-permute-done.2.refs_0_), channel_id=1, source_target_pairs={{0,2},{1,15},{2,4},{3,1},{4,6},{5,3},{6,8},{7,5},{8,10},{9,7},{10,... | collective-permute-start | bytes 1572872 | tf_op jit(solution)/shard_map/ppermute | solution.py:36
  85.8 11.2 %collective-permute-start.7 = (bf16[2048,128]{1,0:T(8,128)(2,1)S(1)}, bf16[2048,128]{1,0:T(8,128)(2,1)S(1)}, u32[]{:S(2)}, u32[]{:S(2)}) collective-permute-start(bf16[2048,128]{1,0:T(8,128)(2,1)S(1)} %collective-permute-done.6.refs_1_), channel_id=1, source_target_pairs={{0,2},{1,15},{2,4},{3,1},{4,6},{5,3},{6,8},{7,5},{8,10},{9,7},{10,... | collective-permute-start | bytes 1572872 | tf_op jit(solution)/shard_map/ppermute | solution.py:36
  91.4 11.3 %collective-permute-start.4 = (bf16[2048,128]{1,0:T(8,128)(2,1)S(1)}, bf16[2048,128]{1,0:T(8,128)(2,1)}, u32[]{:S(2)}, u32[]{:S(2)}) collective-permute-start(bf16[2048,128]{1,0:T(8,128)(2,1)S(1)} %collective-permute-done.3.refs_0_), channel_id=1, source_target_pairs={{0,2},{1,15},{2,4},{3,1},{4,6},{5,3},{6,8},{7,5},{8,10},{9,7},{10,... | collective-permute-start | bytes 1572872 | tf_op jit(solution)/shard_map/ppermute | solution.py:36
  97.0 11.3 %collective-permute-start.8 = (bf16[2048,128]{1,0:T(8,128)(2,1)S(1)}, bf16[2048,128]{1,0:T(8,128)(2,1)}, u32[]{:S(2)}, u32[]{:S(2)}) collective-permute-start(bf16[2048,128]{1,0:T(8,128)(2,1)S(1)} %collective-permute-done.7.refs_1_), channel_id=1, source_target_pairs={{0,2},{1,15},{2,4},{3,1},{4,6},{5,3},{6,8},{7,5},{8,10},{9,7},{10,... | collective-permute-start | bytes 1572872 | tf_op jit(solution)/shard_map/ppermute | solution.py:36
  117.6 9.3 %collective-permute-start.9 = (bf16[2048,128]{1,0:T(8,128)(2,1)S(1)}, bf16[2048,128]{1,0:T(8,128)(2,1)S(1)}, u32[]{:S(2)}, u32[]{:S(2)}) collective-permute-start(bf16[2048,128]{1,0:T(8,128)(2,1)S(1)} %get-tuple-element.14), channel_id=1, source_target_pairs={{0,14},{1,3},{2,0},{3,5},{4,2},{5,7},{6,4},{7,9},{8,6},{9,11},{10,... | collective-permute-start | bytes 1572872 | tf_op jit(solution)/shard_map/ppermute | solution.py:36
  118.5 14.0 %collective-permute-start.13 = (bf16[2048,128]{1,0:T(8,128)(2,1)S(1)}, bf16[2048,128]{1,0:T(8,128)(2,1)S(1)}, u32[]{:S(2)}, u32[]{:S(2)}) collective-permute-start(bf16[2048,128]{1,0:T(8,128)(2,1)S(1)} %get-tuple-element.18), channel_id=1, source_target_pairs={{0,14},{1,3},{2,0},{3,5},{4,2},{5,7},{6,4},{7,9},{8,6},{9,11},{10,... | collective-permute-start | bytes 1572872 | tf_op jit(solution)/shard_map/ppermute | solution.py:36
  127.0 12.3 %collective-permute-start.10 = (bf16[2048,128]{1,0:T(8,128)(2,1)S(1)}, bf16[2048,128]{1,0:T(8,128)(2,1)S(1)}, u32[]{:S(2)}, u32[]{:S(2)}) collective-permute-start(bf16[2048,128]{1,0:T(8,128)(2,1)S(1)} %add_convert_fusion.4), channel_id=1, source_target_pairs={{0,14},{1,3},{2,0},{3,5},{4,2},{5,7},{6,4},{7,9},{8,6},{9,11},{10,... | collective-permute-start | bytes 1572872 | tf_op jit(solution)/shard_map/ppermute | solution.py:36
  132.6 11.1 %collective-permute-start.14 = (bf16[2048,128]{1,0:T(8,128)(2,1)S(1)}, bf16[2048,128]{1,0:T(8,128)(2,1)S(1)}, u32[]{:S(2)}, u32[]{:S(2)}) collective-permute-start(bf16[2048,128]{1,0:T(8,128)(2,1)S(1)} %add_convert_fusion.1), channel_id=1, source_target_pairs={{0,14},{1,3},{2,0},{3,5},{4,2},{5,7},{6,4},{7,9},{8,6},{9,11},{10,... | collective-permute-start | bytes 1572872 | tf_op jit(solution)/shard_map/ppermute | solution.py:36
  139.3 11.3 %collective-permute-start.11 = (bf16[2048,128]{1,0:T(8,128)(2,1)S(1)}, bf16[2048,128]{1,0:T(8,128)(2,1)S(1)}, u32[]{:S(2)}, u32[]{:S(2)}) collective-permute-start(bf16[2048,128]{1,0:T(8,128)(2,1)S(1)} %add_convert_fusion.3), channel_id=1, source_target_pairs={{0,14},{1,3},{2,0},{3,5},{4,2},{5,7},{6,4},{7,9},{8,6},{9,11},{10,... | collective-permute-start | bytes 1572872 | tf_op jit(solution)/shard_map/ppermute | solution.py:36
  143.8 11.1 %collective-permute-start.15 = (bf16[2048,128]{1,0:T(8,128)(2,1)S(1)}, bf16[2048,128]{1,0:T(8,128)(2,1)S(1)}, u32[]{:S(2)}, u32[]{:S(2)}) collective-permute-start(bf16[2048,128]{1,0:T(8,128)(2,1)S(1)} %add_convert_fusion), channel_id=1, source_target_pairs={{0,14},{1,3},{2,0},{3,5},{4,2},{5,7},{6,4},{7,9},{8,6},{9,11},{10,... | collective-permute-start | bytes 1572872 | tf_op jit(solution)/shard_map/ppermute | solution.py:36
  150.8 9.7 %collective-permute-start.12 = (bf16[2048,128]{1,0:T(8,128)(2,1)S(1)}, bf16[2048,128]{1,0:T(8,128)(2,1)S(1)}, u32[]{:S(2)}, u32[]{:S(2)}) collective-permute-start(bf16[2048,128]{1,0:T(8,128)(2,1)S(1)} %add_convert_fusion.2), channel_id=1, source_target_pairs={{0,14},{1,3},{2,0},{3,5},{4,2},{5,7},{6,4},{7,9},{8,6},{9,11},{10,... | collective-permute-start | bytes 1572872 | tf_op jit(solution)/shard_map/ppermute | solution.py:36
  154.9 5.6 %collective-permute-start.16 = (bf16[2048,128]{1,0:T(8,128)(2,1)S(1)}, bf16[2048,128]{1,0:T(8,128)(2,1)S(1)}, u32[]{:S(2)}, u32[]{:S(2)}) collective-permute-start(bf16[2048,128]{1,0:T(8,128)(2,1)S(1)} %collective-permute-done.15), channel_id=1, source_target_pairs={{0,1},{1,0},{2,3},{3,2},{4,5},{5,4},{6,7},{7,6},{8,9},{9,8},{10,11... | collective-permute-start | bytes 1572872 | tf_op jit(solution)/shard_map/ppermute | solution.py:40

commit v2 on v1

--- a/solution.py
+++ b/solution.py
@@ -19,21 +19,22 @@
     return ((y * X + x) * Z + z) * 2 + c
 
 
-def rows_and_columns():
-    along_x = lambda c: [[place(y, x, z, c) for x in range(X)] for y in range(Y) for z in range(Z)]
-    along_y = lambda c: [[place(y, x, z, c) for y in range(Y)] for x in range(X) for z in range(Z)]
-    return along_x(0) + along_y(1), along_y(0) + along_x(1)
-
-
-FIRST, SECOND = rows_and_columns()
+ROWS = [[place(y, x, z, 0) for x in range(X)] for y in range(Y) for z in range(Z)]
+ROWS += [[place(y, x, z, 1) for y in range(Y)] for x in range(X) for z in range(Z)]
 WHOLE = pl.BlockSpec(memory_space=pltpu.VMEM)
-LARGE = pltpu.CompilerParams(vmem_limit_bytes=60 << 20)
 SMALL = pltpu.CompilerParams(vmem_limit_bytes=12 << 20)
 
 
 def onward(x, by):
     pairs = [(2 * z + c, 2 * ((z + (by if c == 0 else -by)) % Z) + c) for z in range(Z) for c in range(2)]
     return lax.ppermute(x, ("z", "c"), pairs)
+
+
+def along_column(x, by):
+    flat = lambda y, x, c: (y % Y * X + x % X) * 2 + c
+    pairs = [(flat(j, i, 0), flat(j + by, i, 0)) for j in range(Y) for i in range(X)]
+    pairs += [(flat(j, i, 1), flat(j, i + by, 1)) for j in range(Y) for i in range(X)]
+    return lax.ppermute(x, ("y", "x", "c"), pairs)
 
 
 def swap(x):
@@ -69,14 +70,14 @@
         c.wait()
 
 
-def repeated(body, shape, *operands, room=SMALL):
+def repeated(body, shape, *operands):
     return pl.pallas_call(
         body,
         out_shape=jax.ShapeDtypeStruct((4, *shape), bf16),
         in_specs=[WHOLE] * len(operands),
         out_specs=pl.BlockSpec(memory_space=pltpu.HBM),
         scratch_shapes=[pltpu.VMEM(shape, bf16), pltpu.SemaphoreType.DMA((4,))],
-        compiler_params=room,
+        compiler_params=SMALL,
     )(*operands)
 
 
@@ -98,32 +99,48 @@
     return repeated(pack_body, (rows, LANES), gate, upper, down)
 
 
-def spread_body(blocks, out, packed, sems):
+def spread_body(blocks, out):
     for k in range(4):
-        packed[:, LANES * k : LANES * (k + 1)] = blocks[k]
-    repeat(packed, out, sems)
+        out[:, LANES * k : LANES * (k + 1)] = blocks[k]
 
 
 def spread(blocks):
-    return repeated(spread_body, (blocks.shape[1], 4 * LANES), blocks, room=LARGE)
-
-
-def hold_body(source, out, sem):
-    copy = pltpu.make_async_copy(source, out, sem)
-    copy.start()
-    copy.wait()
-
-
-def hold(x):
+    return pl.pallas_call(
+        spread_body,
+        out_shape=jax.ShapeDtypeStruct((blocks.shape[1], 4 * LANES), bf16),
+        in_specs=[WHOLE],
+        out_specs=WHOLE,
+        compiler_params=SMALL,
+        name="spread",
+    )(blocks)
+
+
+def hold_body(place_ref, here, before, after, top, bottom, out, sems):
+    at, half = place_ref[0], top.shape[0]
+    ends = [
+        (here, out.at[at]),
+        (before, out.at[(at + 3) % 4]),
+        (after, out.at[(at + 1) % 4]),
+        (top, out.at[(at + 2) % 4, :half]),
+        (bottom, out.at[(at + 2) % 4, half:]),
+    ]
+    copies = [pltpu.make_async_copy(*e, sems.at[i]) for i, e in enumerate(ends)]
+    for c in copies:
+        c.start()
+    for c in copies:
+        c.wait()
+
+
+def hold(place, blocks):
     return pl.pallas_call(
         hold_body,
-        out_shape=jax.ShapeDtypeStruct(x.shape, x.dtype),
-        in_specs=[pl.BlockSpec(memory_space=pltpu.HBM)],
-        out_specs=WHOLE,
-        scratch_shapes=[pltpu.SemaphoreType.DMA],
+        out_shape=jax.ShapeDtypeStruct((4, *blocks[0].shape), bf16),
+        in_specs=[pl.BlockSpec(memory_space=pltpu.SMEM)] + [pl.BlockSpec(memory_space=pltpu.HBM)] * 5,
+        out_specs=WHOLE,
+        scratch_shapes=[pltpu.SemaphoreType.DMA((5,))],
         compiler_params=SMALL,
         name="hold",
-    )(x)
+    )(place, *blocks)
 
 
 def order(core, b, w):
@@ -210,11 +227,21 @@
         if d < 4:
             mate[d] = onward(mate[d - 1], 1)
 
-    rows = from_four(pack(gate_weight.T, up_weight.T, down_weight), FIRST)
-    columns = from_four(spread(rows), SECOND)
-    other = swap(columns)
-    columns = hold(columns)
-    weights = columns, hold(other)
+    rows = from_four(pack(gate_weight.T, up_weight.T, down_weight), ROWS)
+    here = spread(rows)
+    half = here.shape[0] // 2
+    before = along_column(here, 1)
+    after = along_column(here, -1)
+    top = along_column(before[:half], 1)
+    bottom = along_column(after[half:], -1)
+    blocks = here, before, after, top, bottom
+    others = []
+    for b in blocks:
+        others.append(swap(b))
+    row, column = lax.axis_index("y").astype(jnp.int32)[None], lax.axis_index("x").astype(jnp.int32)[None]
+    first = core == 0
+    columns = hold(jnp.where(first, row, column), blocks)
+    weights = columns, hold(jnp.where(first, column, row), others)
 
     units = down_weight.shape[0]
     groups = [(own[4], mate[3]), (own[3], mate[2]), (own[2], mate[1]), (own[1], own[0])]

time: 163 us -> 121 us (0.74)
  blocking collectives: 50.4 us -> 0 us
  starting transfers between devices: 15.6 us -> 26.3 us
  Pallas kernels: 30.3 us -> 27.6 us
  local copies, waits for them, and re-layouts: 2.68 us -> 4.53 us
  waiting for transfers between devices: 61.9 us -> 60.1 us
    all_to_all x2 -> x0, blocking collectives: 50.4 us -> none  [from_four(): lax.all_to_all(copies, AXES, 0, 0, axis_index_groups=groups, tiled=True)]
    ppermute x14, waiting for transfers between devices: 61.8 us -> 44.7 us  [onward(): return lax.ppermute(x, ('z', 'c'), pairs)]
    all_to_all x0 -> x1, waiting for transfers between devices: none -> 8.17 us  [from_four(): lax.all_to_all(copies, AXES, 0, 0, axis_index_groups=groups, tiled=True)]
    ppermute x0 -> x4, waiting for transfers between devices: none -> 7.3 us  [along_column(): return lax.ppermute(x, ('y', 'x', 'c'), pairs)]
    ppermute x0 -> x4, starting transfers between devices: none -> 7.1 us  [along_column(): return lax.ppermute(x, ('y', 'x', 'c'), pairs)]
    all_to_all x0 -> x1, starting transfers between devices: none -> 4.84 us  [from_four(): lax.all_to_all(copies, AXES, 0, 0, axis_index_groups=groups, tiled=True)]
    pallas_call x2 -> x1, Pallas kernels: 3.83 us -> 1.15 us  [repeated(): pl.pallas_call(body, out_shape=jax.ShapeDtypeStruct((4, *shape), bf16), i...]
    unnamed x10 -> x26, local copies, waits for them, and re-layouts: 2.68 us -> 3.4 us
  transfers between devices with their start and end apart: 17 -> 26, of which waited for: 12 -> 14; matrix products, arithmetic and copies ran while one was open for 0% -> 1% of each run, Pallas kernels for 11% -> 17%
where the time goes in v2:
time: 121 us; the launch traced here: 119 us
  waiting for transfers between devices  60.1 us (50%)
  Pallas kernels  27.6 us (23%)
  starting transfers between devices  26.3 us (22%)
  local copies, waits for them, and re-layouts  4.53 us (4%)
    ppermute x14, waiting for transfers between devices, onward(): return lax.ppermute(x, ('z', 'c'), pairs)  44.7 us
    pallas_call x8, Pallas kernels, call(): pl.pallas_call(functools.partial(body, n, units), out_shape=out_shape, in...  20.7 us
    ppermute x14, starting transfers between devices, onward(): return lax.ppermute(x, ('z', 'c'), pairs)  10.8 us
    all_to_all x1, waiting for transfers between devices, from_four(): lax.all_to_all(copies, AXES, 0, 0, axis_index_groups=groups, tiled=True)  8.17 us
    ppermute x4, waiting for transfers between devices, along_column(): return lax.ppermute(x, ('y', 'x', 'c'), pairs)  7.3 us
    ppermute x4, starting transfers between devices, along_column(): return lax.ppermute(x, ('y', 'x', 'c'), pairs)  7.1 us
    all_to_all x1, starting transfers between devices, from_four(): lax.all_to_all(copies, AXES, 0, 0, axis_index_groups=groups, tiled=True)  4.84 us
    pallas_call x2, Pallas kernels, hold(): pl.pallas_call(hold_body, out_shape=jax.ShapeDtypeStruct((4, *blocks[0].s...  4.2 us
  transfers between devices with their start and end apart: 26, of which 14 were waited for; matrix products, arithmetic and copies ran while one was open for 1% of the time, Pallas kernels for 17%

profile of v2, /device:TPU:2, one launch (start us, length us, event | category | flops | bytes accessed | tf_op | source)
XLA Modules:
  0.0 119.5 jit_solution(13844955491644726848)
XLA Ops:
  0.0 1.0 copy-done.8
  1.0 0.7 copy-done.12
  1.7 0.4 norm.1.refs_1_
  2.1 2.0 %collective-permute-start = (bf16[2048,128]{1,0:T(8,128)(2,1)S(1)}, bf16[2048,128]{1,0:T(8,128)(2,1)S(1)}, u32[]{:S(2)}, u32[]{:S(2)}) collective-permute-start(bf16[2048,128]{1,0:T(8,128)(2,1)S(1)} %norm.1.refs_1_), channel_id=1, source_target_pairs={{0,2},{1,15},{2,4},{3,1},{4,6},{5,3},{6,8},{7,5},{8,10},{9,7},{10,... | collective-permute-start | bytes 1572872 | tf_op jit(solution)/shard_map/ppermute | solution.py:30
  4.1 3.5 %collective-permute-start.13 = (bf16[2048,128]{1,0:T(8,128)(2,1)S(1)}, bf16[2048,128]{1,0:T(8,128)(2,1)}, u32[]{:S(2)}, u32[]{:S(2)}) collective-permute-start(bf16[2048,128]{1,0:T(8,128)(2,1)S(1)} %norm.1.refs_1_), channel_id=1, source_target_pairs={{0,1},{1,0},{2,3},{3,2},{4,5},{5,4},{6,7},{7,6},{8,9},{9,8},{10,11... | collective-permute-start | bytes 1572872 | tf_op jit(solution)/shard_map/ppermute | solution.py:41
  7.6 1.2 shard_map.55
  8.8 4.8 %all-to-all-start = ((bf16[4,1088,128]{2,1,0:T(8,128)(2,1)}), bf16[4,1088,128]{2,1,0:T(8,128)(2,1)S(1)}, u32[]{:S(2)}, u32[]{:S(2)}) async-start(bf16[4,1088,128]{2,1,0:T(8,128)(2,1)} %shard_map.55), calls=%async_computation | async-start | bytes 2228224 | tf_op jit(solution)/shard_map/all_to_all | solution.py:45
  13.6 1.6 %collective-permute-done.refs_0_ = bf16[2048,128]{1,0:T(8,128)(2,1)S(1)} collective-permute-done((bf16[2048,128]{1,0:T(8,128)(2,1)S(1)}, bf16[2048,128]{1,0:T(8,128)(2,1)S(1)}, u32[]{:S(2)}, u32[]{:S(2)}) %collective-permute-start) | collective-permute-done | bytes 524320 | tf_op jit(solution)/shard_map/ppermute | solution.py:30
  15.2 8.2 %all-to-all-done.blocks = bf16[4,1088,128]{2,1,0:T(8,128)(2,1)S(1)} async-done(((bf16[4,1088,128]{2,1,0:T(8,128)(2,1)}), bf16[4,1088,128]{2,1,0:T(8,128)(2,1)S(1)}, u32[]{:S(2)}, u32[]{:S(2)}) %all-to-all-start) | async-done | bytes 1114144 | tf_op jit(solution)/shard_map/all_to_all | solution.py:45
  23.4 0.2 spread.1.here
  23.6 1.7 %collective-permute-start.1 = (bf16[1088,512]{1,0:T(8,128)(2,1)S(1)}, bf16[1088,512]{1,0:T(8,128)(2,1)S(1)}, u32[]{:S(2)}, u32[]{:S(2)}) collective-permute-start(bf16[1088,512]{1,0:T(8,128)(2,1)S(1)} %spread.1.here), channel_id=1, source_target_pairs={{0,64},{16,80},{32,96},{48,112},{64,128},{80,144},{96,160},{112,17... | collective-permute-start | bytes 3342344 | tf_op jit(solution)/shard_map/ppermute | solution.py:37
  25.2 1.7 %collective-permute-start.2 = (bf16[1088,512]{1,0:T(8,128)(2,1)S(1)}, bf16[1088,512]{1,0:T(8,128)(2,1)}, u32[]{:S(2)}, u32[]{:S(2)}) collective-permute-start(bf16[1088,512]{1,0:T(8,128)(2,1)S(1)} %spread.1.here), channel_id=1, source_target_pairs={{0,192},{16,208},{32,224},{48,240},{64,0},{80,16},{96,32},{112,48}... | collective-permute-start | bytes 3342344 | tf_op jit(solution)/shard_map/ppermute | solution.py:37
  26.9 4.4 %collective-permute-done.14.refs_1_ = bf16[2048,128]{1,0:T(8,128)(2,1)} collective-permute-done((bf16[2048,128]{1,0:T(8,128)(2,1)}, bf16[2048,128]{1,0:T(8,128)(2,1)}, u32[]{:S(2)}, u32[]{:S(2)}) %collective-permute-start.14) | collective-permute-done | bytes 524320 | tf_op jit(solution)/shard_map/ppermute | solution.py:30
  31.3 6.2 %collective-permute-done.11.refs_0_ = bf16[2048,128]{1,0:T(8,128)(2,1)S(1)} collective-permute-done((bf16[2048,128]{1,0:T(8,128)(2,1)}, bf16[2048,128]{1,0:T(8,128)(2,1)S(1)}, u32[]{:S(2)}, u32[]{:S(2)}) %collective-permute-start.11) | collective-permute-done | bytes 524320 | tf_op jit(solution)/shard_map/ppermute | solution.py:30
  37.5 5.6 %collective-permute-done.15.refs_1_ = bf16[2048,128]{1,0:T(8,128)(2,1)S(1)} collective-permute-done((bf16[2048,128]{1,0:T(8,128)(2,1)}, bf16[2048,128]{1,0:T(8,128)(2,1)S(1)}, u32[]{:S(2)}, u32[]{:S(2)}) %collective-permute-start.15) | collective-permute-done | bytes 524320 | tf_op jit(solution)/shard_map/ppermute | solution.py:30
  43.2 1.4 %collective-permute-start.3 = (bf16[544,512]{1,0:T(8,128)(2,1)S(1)}, bf16[544,512]{1,0:T(8,128)(2,1)}, u32[]{:S(2)}, u32[]{:S(2)}) collective-permute-start(bf16[544,512]{1,0:T(8,128)(2,1)S(1)} %slice.8), channel_id=1, source_target_pairs={{0,64},{16,80},{32,96},{48,112},{64,128},{80,144},{96,160},{112,17... | collective-permute-start | bytes 1671176 | tf_op jit(solution)/shard_map/ppermute | solution.py:37
  44.6 1.1 slice.9
  45.8 3.0 %collective-permute-done.12.refs_0_ = bf16[2048,128]{1,0:T(8,128)(2,1)S(1)} collective-permute-done((bf16[2048,128]{1,0:T(8,128)(2,1)S(1)}, bf16[2048,128]{1,0:T(8,128)(2,1)S(1)}, u32[]{:S(2)}, u32[]{:S(2)}) %collective-permute-start.12) | collective-permute-done | bytes 524320 | tf_op jit(solution)/shard_map/ppermute | solution.py:30
  48.7 0.8 copy-done.4
  49.6 4.8 %collective-permute-done.16.refs_1_ = bf16[2048,128]{1,0:T(8,128)(2,1)S(1)} collective-permute-done((bf16[2048,128]{1,0:T(8,128)(2,1)S(1)}, bf16[2048,128]{1,0:T(8,128)(2,1)S(1)}, u32[]{:S(2)}, u32[]{:S(2)}) %collective-permute-start.16) | collective-permute-done | bytes 524320 | tf_op jit(solution)/shard_map/ppermute | solution.py:30
  54.4 0.8 copy-done.6
  55.1 2.3 %collective-permute-start.4 = (bf16[544,512]{1,0:T(8,128)(2,1)S(1)}, bf16[544,512]{1,0:T(8,128)(2,1)}, u32[]{:S(2)}, u32[]{:S(2)}) collective-permute-start(bf16[544,512]{1,0:T(8,128)(2,1)S(1)} %slice.9), channel_id=1, source_target_pairs={{0,192},{16,208},{32,224},{48,240},{64,0},{80,16},{96,32},{112,48}... | collective-permute-start | bytes 1671176 | tf_op jit(solution)/shard_map/ppermute | solution.py:37
  57.5 7.3 %collective-permute-done.4.bottom = bf16[544,512]{1,0:T(8,128)(2,1)} collective-permute-done((bf16[544,512]{1,0:T(8,128)(2,1)S(1)}, bf16[544,512]{1,0:T(8,128)(2,1)}, u32[]{:S(2)}, u32[]{:S(2)}) %collective-permute-start.4) | collective-permute-done | bytes 557088 | tf_op jit(solution)/shard_map/ppermute | solution.py:37
  64.8 1.9 %hold.2.refs_2_ = bf16[4,1088,512]{2,1,0:T(8,128)(2,1)S(1)} custom-call(s32[1]{0:T(128)S(6)} %select_n.7.place_ref, bf16[1088,512]{1,0:T(8,128)(2,1)S(1)} %spread.1.here, bf16[1088,512]{1,0:T(8,128)(2,1)S(1)} %collective-permute-done.1.before, bf16[1088,512]{1,0:T(8,128)(2,1)} %collective-permute-done.2.after, bf16[544,512]{1,0:T(8,128)(2,1)} %collective-permute-done.3.top, ...), custom_call_target="tpu_custom_call" | custom-call | tf_op jit(solution)/shard_map/hold/pallas_call | solution.py:135
  66.7 1.0 shard_map.58.refs_4_
  67.8 2.3 %hold.3.refs_3_ = bf16[4,1088,512]{2,1,0:T(8,128)(2,1)S(1)} custom-call(s32[1]{0:T(128)S(6)} %select_n.8.place_ref, bf16[1088,512]{1,0:T(8,128)(2,1)} %collective-permute-done.5.here, bf16[1088,512]{1,0:T(8,128)(2,1)} %collective-permute-done.6.before, bf16[1088,512]{1,0:T(8,128)(2,1)} %collective-permute-done.7.after, ...), custom_call_target="tpu_custom_call" | custom-call | tf_op jit(solution)/shard_map/hold/pallas_call | solution.py:135
  70.1 3.6 %shard_map.59 = (bf16[2048,128]{1,0:T(8,128)(2,1)S(1)}, bf16[2048,128]{1,0:T(8,128)(2,1)S(1)}) custom-call(s32[1]{0:T(128)} %bitcast.core_ref, bf16[2048,128]{1,0:T(8,128)(2,1)S(1)} %copy-done.5, bf16[2048,128]{1,0:T(8,128)(2,1)S(1)} %copy-done.7, bf16[4,1088,512]{2,1,0:T(8,128)(2,1)S(1)} %hold.2.refs_2_, bf16[4,1088,512]{2,1,0:T(8,128)(2,1)S(1)} %hold.3.refs_3_, ...), custom_call_target="tpu_custom_call" | custom-call | tf_op jit(solution)/shard_map/pallas_call | solution.py:185
  73.7 0.6 collective-permute-start.17
  74.3 1.0 collective-permute-start.21
  75.3 1.0 shard_map.60.refs_4_
  76.4 3.5 %shard_map.61 = (f32[2048,128]{1,0:T(8,128)S(1)}, f32[2048,128]{1,0:T(8,128)S(1)}) custom-call(s32[1]{0:T(128)} %bitcast.core_ref, bf16[2048,128]{1,0:T(8,128)(2,1)S(1)} %copy-done.1, bf16[2048,128]{1,0:T(8,128)(2,1)S(1)} %copy-done.3, bf16[4,1088,512]{2,1,0:T(8,128)(2,1)S(1)} %hold.2.refs_2_, bf16[4,1088,512]{2,1,0:T(8,128)(2,1)S(1)} %hold.3.refs_3_, ...), custom_call_target="tpu_custom_call" | custom-call | tf_op jit(solution)/shard_map/pallas_call | solution.py:185
  79.9 3.0 %collective-permute-done.17 = bf16[2048,128]{1,0:T(8,128)(2,1)S(1)} collective-permute-done((bf16[2048,128]{1,0:T(8,128)(2,1)S(1)}, bf16[2048,128]{1,0:T(8,128)(2,1)S(1)}, u32[]{:S(2)}, u32[]{:S(2)}) %collective-permute-start.17) | collective-permute-done | bytes 524320 | tf_op jit(solution)/shard_map/ppermute | solution.py:30
  83.1 1.9 %collective-permute-start.18 = (bf16[2048,128]{1,0:T(8,128)(2,1)S(1)}, bf16[2048,128]{1,0:T(8,128)(2,1)S(1)}, u32[]{:S(2)}, u32[]{:S(2)}) collective-permute-start(bf16[2048,128]{1,0:T(8,128)(2,1)S(1)} %add_convert_fusion.4), channel_id=1, source_target_pairs={{0,14},{1,3},{2,0},{3,5},{4,2},{5,7},{6,4},{7,9},{8,6},{9,11},{10,... | collective-permute-start | bytes 1572872 | tf_op jit(solution)/shard_map/ppermute | solution.py:30
  84.9 3.7 %collective-permute-done.21 = bf16[2048,128]{1,0:T(8,128)(2,1)S(1)} collective-permute-done((bf16[2048,128]{1,0:T(8,128)(2,1)S(1)}, bf16[2048,128]{1,0:T(8,128)(2,1)S(1)}, u32[]{:S(2)}, u32[]{:S(2)}) %collective-permute-start.21) | collective-permute-done | bytes 524320 | tf_op jit(solution)/shard_map/ppermute | solution.py:30
  88.7 2.1 %collective-permute-start.22 = (bf16[2048,128]{1,0:T(8,128)(2,1)S(1)}, bf16[2048,128]{1,0:T(8,128)(2,1)S(1)}, u32[]{:S(2)}, u32[]{:S(2)}) collective-permute-start(bf16[2048,128]{1,0:T(8,128)(2,1)S(1)} %add_convert_fusion.1), channel_id=1, source_target_pairs={{0,14},{1,3},{2,0},{3,5},{4,2},{5,7},{6,4},{7,9},{8,6},{9,11},{10,... | collective-permute-start | bytes 1572872 | tf_op jit(solution)/shard_map/ppermute | solution.py:30
  90.8 2.2 %shard_map.62.refs_4_ = bf16[352,256]{1,0:T(8,128)(2,1)S(1)} custom-call(s32[1]{0:T(128)} %bitcast.core_ref, bf16[2048,128]{1,0:T(8,128)(2,1)} %collective-permute-done.10.refs_0_, bf16[2048,128]{1,0:T(8,128)(2,1)} %collective-permute-done.14.refs_1_, bf16[4,1088,512]{2,1,0:T(8,128)(2,1)S(1)} %hold.2.refs_2_), custom_call_target="tpu_custom_call" | custom-call | tf_op jit(solution)/shard_map/pallas_call | solution.py:185
  93.0 4.7 %shard_map.63 = (f32[2048,128]{1,0:T(8,128)S(1)}, f32[2048,128]{1,0:T(8,128)S(1)}) custom-call(s32[1]{0:T(128)} %bitcast.core_ref, bf16[2048,128]{1,0:T(8,128)(2,1)} %collective-permute-done.10.refs_0_, bf16[2048,128]{1,0:T(8,128)(2,1)} %collective-permute-done.14.refs_1_, bf16[4,1088,512]{2,1,0:T(8,128)(2,1)S(1)} %hold.2.refs_2_, ...), custom_call_target="tpu_custom_call" | custom-call | tf_op jit(solution)/shard_map/pallas_call | solution.py:185
  97.7 0.1 add_convert_fusion.3
  98.0 1.8 %collective-permute-done.22 = bf16[2048,128]{1,0:T(8,128)(2,1)S(1)} collective-permute-done((bf16[2048,128]{1,0:T(8,128)(2,1)S(1)}, bf16[2048,128]{1,0:T(8,128)(2,1)S(1)}, u32[]{:S(2)}, u32[]{:S(2)}) %collective-permute-start.22) | collective-permute-done | bytes 524320 | tf_op jit(solution)/shard_map/ppermute | solution.py:30
  99.9 1.9 %collective-permute-start.23 = (bf16[2048,128]{1,0:T(8,128)(2,1)S(1)}, bf16[2048,128]{1,0:T(8,128)(2,1)S(1)}, u32[]{:S(2)}, u32[]{:S(2)}) collective-permute-start(bf16[2048,128]{1,0:T(8,128)(2,1)S(1)} %add_convert_fusion), channel_id=1, source_target_pairs={{0,14},{1,3},{2,0},{3,5},{4,2},{5,7},{6,4},{7,9},{8,6},{9,11},{10,... | collective-permute-start | bytes 1572872 | tf_op jit(solution)/shard_map/ppermute | solution.py:30
  101.8 1.0 shard_map.56.refs_4_
  102.8 3.6 %shard_map.57 = (f32[2048,128]{1,0:T(8,128)S(1)}, f32[2048,128]{1,0:T(8,128)S(1)}) custom-call(s32[1]{0:T(128)} %bitcast.core_ref, bf16[2048,128]{1,0:T(8,128)(2,1)S(1)} %collective-permute-done.refs_0_, bf16[2048,128]{1,0:T(8,128)(2,1)S(1)} %norm.1.refs_1_, bf16[4,1088,512]{2,1,0:T(8,128)(2,1)S(1)} %hold.2.refs_2_, bf16[4,1088,512]{2,1,0:T(8,128)(2,1)S(1)} %hold.3.refs_3_, ...), custom_call_target="tpu_custom_call" | custom-call | tf_op jit(solution)/shard_map/pallas_call | solution.py:185
  106.4 0.8 collective-permute-done.19
  107.1 0.1 add_convert_fusion.2
  107.3 1.3 %collective-permute-start.20 = (bf16[2048,128]{1,0:T(8,128)(2,1)S(1)}, bf16[2048,128]{1,0:T(8,128)(2,1)S(1)}, u32[]{:S(2)}, u32[]{:S(2)}) collective-permute-start(bf16[2048,128]{1,0:T(8,128)(2,1)S(1)} %add_convert_fusion.2), channel_id=1, source_target_pairs={{0,14},{1,3},{2,0},{3,5},{4,2},{5,7},{6,4},{7,9},{8,6},{9,11},{10,... | collective-permute-start | bytes 1572872 | tf_op jit(solution)/shard_map/ppermute | solution.py:30
  108.6 4.2 %collective-permute-done.23 = bf16[2048,128]{1,0:T(8,128)(2,1)S(1)} collective-permute-done((bf16[2048,128]{1,0:T(8,128)(2,1)S(1)}, bf16[2048,128]{1,0:T(8,128)(2,1)S(1)}, u32[]{:S(2)}, u32[]{:S(2)}) %collective-permute-start.23) | collective-permute-done | bytes 524320 | tf_op jit(solution)/shard_map/ppermute | solution.py:30
  112.8 5.6 %collective-permute-done.20.first = bf16[2048,128]{1,0:T(8,128)(2,1)S(1)} collective-permute-done((bf16[2048,128]{1,0:T(8,128)(2,1)S(1)}, bf16[2048,128]{1,0:T(8,128)(2,1)S(1)}, u32[]{:S(2)}, u32[]{:S(2)}) %collective-permute-start.20) | collective-permute-done | bytes 524320 | tf_op jit(solution)/shard_map/ppermute | solution.py:30
  118.4 1.1 close.1
  (51 shorter events, 0.6 us)
Async XLA Ops:
  0.0 1.0 copy-start.8
  1.0 0.7 copy-start.12
  1.7 5.9 %copy-start.9 = (bf16[128,352]{0,1:T(8,128)(2,1)S(1)}, bf16[128,352]{0,1:T(8,128)(2,1)}, u32[]{:S(2)}) copy-start(bf16[128,352]{0,1:T(8,128)(2,1)} %param.7) | copy-start | bytes 270340
  1.7 5.9 %copy-start.10 = (bf16[128,352]{0,1:T(8,128)(2,1)S(1)}, bf16[128,352]{0,1:T(8,128)(2,1)}, u32[]{:S(2)}) copy-start(bf16[128,352]{0,1:T(8,128)(2,1)} %param.8) | copy-start | bytes 270340
  1.7 5.9 %copy-start.11 = (bf16[352,128]{1,0:T(8,128)(2,1)S(1)}, bf16[352,128]{1,0:T(8,128)(2,1)}, u32[]{:S(2)}) copy-start(bf16[352,128]{1,0:T(8,128)(2,1)} %down.1) | copy-start | bytes 270340
  2.1 13.1 %collective-permute-start = (bf16[2048,128]{1,0:T(8,128)(2,1)S(1)}, bf16[2048,128]{1,0:T(8,128)(2,1)S(1)}, u32[]{:S(2)}, u32[]{:S(2)}) collective-permute-start(bf16[2048,128]{1,0:T(8,128)(2,1)S(1)} %norm.1.refs_1_), channel_id=1, source_target_pairs={{0,2},{1,15},{2,4},{3,1},{4,6},{5,3},{6,8},{7,5},{8,10},{9,7},{10,... | collective-permute-start | bytes 1572872 | tf_op jit(solution)/shard_map/ppermute | solution.py:30
  4.1 11.1 %collective-permute-start.13 = (bf16[2048,128]{1,0:T(8,128)(2,1)S(1)}, bf16[2048,128]{1,0:T(8,128)(2,1)}, u32[]{:S(2)}, u32[]{:S(2)}) collective-permute-start(bf16[2048,128]{1,0:T(8,128)(2,1)S(1)} %norm.1.refs_1_), channel_id=1, source_target_pairs={{0,1},{1,0},{2,3},{3,2},{4,5},{5,4},{6,7},{7,6},{8,9},{9,8},{10,11... | collective-permute-start | bytes 1572872 | tf_op jit(solution)/shard_map/ppermute | solution.py:41
  8.8 14.6 %all-to-all-start = ((bf16[4,1088,128]{2,1,0:T(8,128)(2,1)}), bf16[4,1088,128]{2,1,0:T(8,128)(2,1)S(1)}, u32[]{:S(2)}, u32[]{:S(2)}) async-start(bf16[4,1088,128]{2,1,0:T(8,128)(2,1)} %shard_map.55), calls=%async_computation | async-start | bytes 2228224 | tf_op jit(solution)/shard_map/all_to_all | solution.py:45
  15.2 11.7 %collective-permute-start.10 = (bf16[2048,128]{1,0:T(8,128)(2,1)S(1)}, bf16[2048,128]{1,0:T(8,128)(2,1)}, u32[]{:S(2)}, u32[]{:S(2)}) collective-permute-start(bf16[2048,128]{1,0:T(8,128)(2,1)S(1)} %collective-permute-done.refs_0_), channel_id=1, source_target_pairs={{0,2},{1,15},{2,4},{3,1},{4,6},{5,3},{6,8},{7,5},{8,10},{9,7},{10,... | collective-permute-start | bytes 1572872 | tf_op jit(solution)/shard_map/ppermute | solution.py:30
  15.2 16.1 %collective-permute-start.14 = (bf16[2048,128]{1,0:T(8,128)(2,1)}, bf16[2048,128]{1,0:T(8,128)(2,1)}, u32[]{:S(2)}, u32[]{:S(2)}) collective-permute-start(bf16[2048,128]{1,0:T(8,128)(2,1)} %collective-permute-done.13), channel_id=1, source_target_pairs={{0,2},{1,15},{2,4},{3,1},{4,6},{5,3},{6,8},{7,5},{8,10},{9,7},{10,... | collective-permute-start | bytes 1572872 | tf_op jit(solution)/shard_map/ppermute | solution.py:30
  23.6 19.6 %collective-permute-start.1 = (bf16[1088,512]{1,0:T(8,128)(2,1)S(1)}, bf16[1088,512]{1,0:T(8,128)(2,1)S(1)}, u32[]{:S(2)}, u32[]{:S(2)}) collective-permute-start(bf16[1088,512]{1,0:T(8,128)(2,1)S(1)} %spread.1.here), channel_id=1, source_target_pairs={{0,64},{16,80},{32,96},{48,112},{64,128},{80,144},{96,160},{112,17... | collective-permute-start | bytes 3342344 | tf_op jit(solution)/shard_map/ppermute | solution.py:37
  25.2 19.4 %collective-permute-start.2 = (bf16[1088,512]{1,0:T(8,128)(2,1)S(1)}, bf16[1088,512]{1,0:T(8,128)(2,1)}, u32[]{:S(2)}, u32[]{:S(2)}) collective-permute-start(bf16[1088,512]{1,0:T(8,128)(2,1)S(1)} %spread.1.here), channel_id=1, source_target_pairs={{0,192},{16,208},{32,224},{48,240},{64,0},{80,16},{96,32},{112,48}... | collective-permute-start | bytes 3342344 | tf_op jit(solution)/shard_map/ppermute | solution.py:37
  26.9 10.6 %collective-permute-start.11 = (bf16[2048,128]{1,0:T(8,128)(2,1)}, bf16[2048,128]{1,0:T(8,128)(2,1)S(1)}, u32[]{:S(2)}, u32[]{:S(2)}) collective-permute-start(bf16[2048,128]{1,0:T(8,128)(2,1)} %collective-permute-done.10.refs_0_), channel_id=1, source_target_pairs={{0,2},{1,15},{2,4},{3,1},{4,6},{5,3},{6,8},{7,5},{8,10},{9,7},{10,... | collective-permute-start | bytes 1572872 | tf_op jit(solution)/shard_map/ppermute | solution.py:30
  31.3 11.8 %collective-permute-start.15 = (bf16[2048,128]{1,0:T(8,128)(2,1)}, bf16[2048,128]{1,0:T(8,128)(2,1)S(1)}, u32[]{:S(2)}, u32[]{:S(2)}) collective-permute-start(bf16[2048,128]{1,0:T(8,128)(2,1)} %collective-permute-done.14.refs_1_), channel_id=1, source_target_pairs={{0,2},{1,15},{2,4},{3,1},{4,6},{5,3},{6,8},{7,5},{8,10},{9,7},{10,... | collective-permute-start | bytes 1572872 | tf_op jit(solution)/shard_map/ppermute | solution.py:30
  37.5 8.2 %copy-start = (bf16[2048,128]{1,0:T(8,128)(2,1)}, bf16[2048,128]{1,0:T(8,128)(2,1)S(1)}, u32[]{:S(2)}) copy-start(bf16[2048,128]{1,0:T(8,128)(2,1)S(1)} %collective-permute-done.11.refs_0_) | copy-start | bytes 1572868
  37.5 11.2 %collective-permute-start.12 = (bf16[2048,128]{1,0:T(8,128)(2,1)S(1)}, bf16[2048,128]{1,0:T(8,128)(2,1)S(1)}, u32[]{:S(2)}, u32[]{:S(2)}) collective-permute-start(bf16[2048,128]{1,0:T(8,128)(2,1)S(1)} %collective-permute-done.11.refs_0_), channel_id=1, source_target_pairs={{0,2},{1,15},{2,4},{3,1},{4,6},{5,3},{6,8},{7,5},{8,10},{9,7},{10,... | collective-permute-start | bytes 1572872 | tf_op jit(solution)/shard_map/ppermute | solution.py:30
  43.1 2.6 %copy-start.2 = (bf16[2048,128]{1,0:T(8,128)(2,1)}, bf16[2048,128]{1,0:T(8,128)(2,1)S(1)}, u32[]{:S(2)}) copy-start(bf16[2048,128]{1,0:T(8,128)(2,1)S(1)} %collective-permute-done.15.refs_1_) | copy-start | bytes 1572868
  43.1 11.2 %collective-permute-start.16 = (bf16[2048,128]{1,0:T(8,128)(2,1)S(1)}, bf16[2048,128]{1,0:T(8,128)(2,1)S(1)}, u32[]{:S(2)}, u32[]{:S(2)}) collective-permute-start(bf16[2048,128]{1,0:T(8,128)(2,1)S(1)} %collective-permute-done.15.refs_1_), channel_id=1, source_target_pairs={{0,2},{1,15},{2,4},{3,1},{4,6},{5,3},{6,8},{7,5},{8,10},{9,7},{10,... | collective-permute-start | bytes 1572872 | tf_op jit(solution)/shard_map/ppermute | solution.py:30
  43.1 24.6 %collective-permute-start.5 = (bf16[1088,512]{1,0:T(8,128)(2,1)S(1)}, bf16[1088,512]{1,0:T(8,128)(2,1)}, u32[]{:S(2)}, u32[]{:S(2)}) collective-permute-start(bf16[1088,512]{1,0:T(8,128)(2,1)S(1)} %spread.1.here), channel_id=1, source_target_pairs={{0,1},{1,0},{2,3},{3,2},{4,5},{5,4},{6,7},{7,6},{8,9},{9,8},{10,11... | collective-permute-start | bytes 3342344 | tf_op jit(solution)/shard_map/ppermute | solution.py:41
  43.2 14.3 %collective-permute-start.3 = (bf16[544,512]{1,0:T(8,128)(2,1)S(1)}, bf16[544,512]{1,0:T(8,128)(2,1)}, u32[]{:S(2)}, u32[]{:S(2)}) collective-permute-start(bf16[544,512]{1,0:T(8,128)(2,1)S(1)} %slice.8), channel_id=1, source_target_pairs={{0,64},{16,80},{32,96},{48,112},{64,128},{80,144},{96,160},{112,17... | collective-permute-start | bytes 1671176 | tf_op jit(solution)/shard_map/ppermute | solution.py:37
  44.6 23.1 %collective-permute-start.6 = (bf16[1088,512]{1,0:T(8,128)(2,1)S(1)}, bf16[1088,512]{1,0:T(8,128)(2,1)}, u32[]{:S(2)}, u32[]{:S(2)}) collective-permute-start(bf16[1088,512]{1,0:T(8,128)(2,1)S(1)} %collective-permute-done.1.before), channel_id=1, source_target_pairs={{0,1},{1,0},{2,3},{3,2},{4,5},{5,4},{6,7},{7,6},{8,9},{9,8},{10,11... | collective-permute-start | bytes 3342344 | tf_op jit(solution)/shard_map/ppermute | solution.py:41
  48.7 0.8 copy-start.4
  49.6 18.2 %collective-permute-start.7 = (bf16[1088,512]{1,0:T(8,128)(2,1)}, bf16[1088,512]{1,0:T(8,128)(2,1)}, u32[]{:S(2)}, u32[]{:S(2)}) collective-permute-start(bf16[1088,512]{1,0:T(8,128)(2,1)} %collective-permute-done.2.after), channel_id=1, source_target_pairs={{0,1},{1,0},{2,3},{3,2},{4,5},{5,4},{6,7},{7,6},{8,9},{9,8},{10,11... | collective-permute-start | bytes 3342344 | tf_op jit(solution)/shard_map/ppermute | solution.py:41
  54.4 0.8 copy-start.6
  55.1 9.6 %collective-permute-start.4 = (bf16[544,512]{1,0:T(8,128)(2,1)S(1)}, bf16[544,512]{1,0:T(8,128)(2,1)}, u32[]{:S(2)}, u32[]{:S(2)}) collective-permute-start(bf16[544,512]{1,0:T(8,128)(2,1)S(1)} %slice.9), channel_id=1, source_target_pairs={{0,192},{16,208},{32,224},{48,240},{64,0},{80,16},{96,32},{112,48}... | collective-permute-start | bytes 1671176 | tf_op jit(solution)/shard_map/ppermute | solution.py:37
  57.5 10.3 %collective-permute-start.8 = (bf16[544,512]{1,0:T(8,128)(2,1)}, bf16[544,512]{1,0:T(8,128)(2,1)}, u32[]{:S(2)}, u32[]{:S(2)}) collective-permute-start(bf16[544,512]{1,0:T(8,128)(2,1)} %collective-permute-done.3.top), channel_id=1, source_target_pairs={{0,1},{1,0},{2,3},{3,2},{4,5},{5,4},{6,7},{7,6},{8,9},{9,8},{10,11... | collective-permute-start | bytes 1671176 | tf_op jit(solution)/shard_map/ppermute | solution.py:41
  64.8 3.0 %collective-permute-start.9 = (bf16[544,512]{1,0:T(8,128)(2,1)}, bf16[544,512]{1,0:T(8,128)(2,1)}, u32[]{:S(2)}, u32[]{:S(2)}) collective-permute-start(bf16[544,512]{1,0:T(8,128)(2,1)} %collective-permute-done.4.bottom), channel_id=1, source_target_pairs={{0,1},{1,0},{2,3},{3,2},{4,5},{5,4},{6,7},{7,6},{8,9},{9,8},{10,11... | collective-permute-start | bytes 1671176 | tf_op jit(solution)/shard_map/ppermute | solution.py:41
  64.8 1.9 %copy-start.5 = (bf16[2048,128]{1,0:T(8,128)(2,1)S(1)}, bf16[2048,128]{1,0:T(8,128)(2,1)}, u32[]{:S(2)}) copy-start(bf16[2048,128]{1,0:T(8,128)(2,1)} %copy-done.4) | copy-start | bytes 1572868
  64.8 2.0 %copy-start.7 = (bf16[2048,128]{1,0:T(8,128)(2,1)S(1)}, bf16[2048,128]{1,0:T(8,128)(2,1)}, u32[]{:S(2)}) copy-start(bf16[2048,128]{1,0:T(8,128)(2,1)} %copy-done.6) | copy-start | bytes 1572868
  70.1 5.2 %copy-start.1 = (bf16[2048,128]{1,0:T(8,128)(2,1)S(1)}, bf16[2048,128]{1,0:T(8,128)(2,1)}, u32[]{:S(2)}) copy-start(bf16[2048,128]{1,0:T(8,128)(2,1)} %copy-done) | copy-start | bytes 1572868
  70.1 5.2 %copy-start.3 = (bf16[2048,128]{1,0:T(8,128)(2,1)S(1)}, bf16[2048,128]{1,0:T(8,128)(2,1)}, u32[]{:S(2)}) copy-start(bf16[2048,128]{1,0:T(8,128)(2,1)} %copy-done.2) | copy-start | bytes 1572868
  73.7 9.3 %collective-permute-start.17 = (bf16[2048,128]{1,0:T(8,128)(2,1)S(1)}, bf16[2048,128]{1,0:T(8,128)(2,1)S(1)}, u32[]{:S(2)}, u32[]{:S(2)}) collective-permute-start(bf16[2048,128]{1,0:T(8,128)(2,1)S(1)} %get-tuple-element.14), channel_id=1, source_target_pairs={{0,14},{1,3},{2,0},{3,5},{4,2},{5,7},{6,4},{7,9},{8,6},{9,11},{10,... | collective-permute-start | bytes 1572872 | tf_op jit(solution)/shard_map/ppermute | solution.py:30
  74.3 14.2 %collective-permute-start.21 = (bf16[2048,128]{1,0:T(8,128)(2,1)S(1)}, bf16[2048,128]{1,0:T(8,128)(2,1)S(1)}, u32[]{:S(2)}, u32[]{:S(2)}) collective-permute-start(bf16[2048,128]{1,0:T(8,128)(2,1)S(1)} %get-tuple-element.18), channel_id=1, source_target_pairs={{0,14},{1,3},{2,0},{3,5},{4,2},{5,7},{6,4},{7,9},{8,6},{9,11},{10,... | collective-permute-start | bytes 1572872 | tf_op jit(solution)/shard_map/ppermute | solution.py:30
  83.1 14.7 %collective-permute-start.18 = (bf16[2048,128]{1,0:T(8,128)(2,1)S(1)}, bf16[2048,128]{1,0:T(8,128)(2,1)S(1)}, u32[]{:S(2)}, u32[]{:S(2)}) collective-permute-start(bf16[2048,128]{1,0:T(8,128)(2,1)S(1)} %add_convert_fusion.4), channel_id=1, source_target_pairs={{0,14},{1,3},{2,0},{3,5},{4,2},{5,7},{6,4},{7,9},{8,6},{9,11},{10,... | collective-permute-start | bytes 1572872 | tf_op jit(solution)/shard_map/ppermute | solution.py:30
  88.7 11.1 %collective-permute-start.22 = (bf16[2048,128]{1,0:T(8,128)(2,1)S(1)}, bf16[2048,128]{1,0:T(8,128)(2,1)S(1)}, u32[]{:S(2)}, u32[]{:S(2)}) collective-permute-start(bf16[2048,128]{1,0:T(8,128)(2,1)S(1)} %add_convert_fusion.1), channel_id=1, source_target_pairs={{0,14},{1,3},{2,0},{3,5},{4,2},{5,7},{6,4},{7,9},{8,6},{9,11},{10,... | collective-permute-start | bytes 1572872 | tf_op jit(solution)/shard_map/ppermute | solution.py:30
  97.9 9.3 %collective-permute-start.19 = (bf16[2048,128]{1,0:T(8,128)(2,1)S(1)}, bf16[2048,128]{1,0:T(8,128)(2,1)S(1)}, u32[]{:S(2)}, u32[]{:S(2)}) collective-permute-start(bf16[2048,128]{1,0:T(8,128)(2,1)S(1)} %add_convert_fusion.3), channel_id=1, source_target_pairs={{0,14},{1,3},{2,0},{3,5},{4,2},{5,7},{6,4},{7,9},{8,6},{9,11},{10,... | collective-permute-start | bytes 1572872 | tf_op jit(solution)/shard_map/ppermute | solution.py:30
  99.9 12.8 %collective-permute-start.23 = (bf16[2048,128]{1,0:T(8,128)(2,1)S(1)}, bf16[2048,128]{1,0:T(8,128)(2,1)S(1)}, u32[]{:S(2)}, u32[]{:S(2)}) collective-permute-start(bf16[2048,128]{1,0:T(8,128)(2,1)S(1)} %add_convert_fusion), channel_id=1, source_target_pairs={{0,14},{1,3},{2,0},{3,5},{4,2},{5,7},{6,4},{7,9},{8,6},{9,11},{10,... | collective-permute-start | bytes 1572872 | tf_op jit(solution)/shard_map/ppermute | solution.py:30
  107.3 11.1 %collective-permute-start.20 = (bf16[2048,128]{1,0:T(8,128)(2,1)S(1)}, bf16[2048,128]{1,0:T(8,128)(2,1)S(1)}, u32[]{:S(2)}, u32[]{:S(2)}) collective-permute-start(bf16[2048,128]{1,0:T(8,128)(2,1)S(1)} %add_convert_fusion.2), channel_id=1, source_target_pairs={{0,14},{1,3},{2,0},{3,5},{4,2},{5,7},{6,4},{7,9},{8,6},{9,11},{10,... | collective-permute-start | bytes 1572872 | tf_op jit(solution)/shard_map/ppermute | solution.py:30
  112.8 5.6 %collective-permute-start.24 = (bf16[2048,128]{1,0:T(8,128)(2,1)S(1)}, bf16[2048,128]{1,0:T(8,128)(2,1)S(1)}, u32[]{:S(2)}, u32[]{:S(2)}) collective-permute-start(bf16[2048,128]{1,0:T(8,128)(2,1)S(1)} %collective-permute-done.23), channel_id=1, source_target_pairs={{0,1},{1,0},{2,3},{3,2},{4,5},{5,4},{6,7},{7,6},{8,9},{9,8},{10,11... | collective-permute-start | bytes 1572872 | tf_op jit(solution)/shard_map/ppermute | solution.py:41

commit v3 on v2

--- a/solution.py
+++ b/solution.py
@@ -22,6 +22,7 @@
 ROWS = [[place(y, x, z, 0) for x in range(X)] for y in range(Y) for z in range(Z)]
 ROWS += [[place(y, x, z, 1) for y in range(Y)] for x in range(X) for z in range(Z)]
 WHOLE = pl.BlockSpec(memory_space=pltpu.VMEM)
+FULL = pltpu.CompilerParams(vmem_limit_bytes=67_000_000)
 SMALL = pltpu.CompilerParams(vmem_limit_bytes=12 << 20)
 
 
@@ -45,7 +46,12 @@
     return lax.all_to_all(copies, AXES, 0, 0, axis_index_groups=groups, tiled=True)
 
 
-def norm_body(tokens, gain, out):
+def norm_body(tokens_in, gain_in, out, tokens, gain, sems):
+    copies = [pltpu.make_async_copy(tokens_in, tokens, sems.at[0]), pltpu.make_async_copy(gain_in, gain, sems.at[1])]
+    for c in copies:
+        c.start()
+    for c in copies:
+        c.wait()
     values = tokens[...].astype(f32)
     factor = lax.rsqrt(jnp.mean(values * values, axis=-1, keepdims=True) + eps_floor)
     out[...] = (values * factor * gain[...]).T.astype(bf16)
@@ -55,76 +61,81 @@
     return pl.pallas_call(
         norm_body,
         out_shape=jax.ShapeDtypeStruct(tokens.shape[::-1], bf16),
-        in_specs=[WHOLE, WHOLE],
+        in_specs=[pl.BlockSpec(memory_space=pltpu.HBM)] * 2,
         out_specs=WHOLE,
-        compiler_params=SMALL,
+        scratch_shapes=[
+            pltpu.VMEM(tokens.shape, bf16),
+            pltpu.VMEM((1, tokens.shape[1]), f32),
+            pltpu.SemaphoreType.DMA((2,)),
+        ],
+        compiler_params=FULL,
         name="norm",
     )(tokens, gain[None])
 
 
-def repeat(packed, out, sems):
-    copies = [pltpu.make_async_copy(packed, out.at[k], sems.at[k]) for k in range(4)]
-    for c in copies:
-        c.start()
-    for c in copies:
-        c.wait()
-
-
-def repeated(body, shape, *operands):
-    return pl.pallas_call(
-        body,
-        out_shape=jax.ShapeDtypeStruct((4, *shape), bf16),
-        in_specs=[WHOLE] * len(operands),
-        out_specs=pl.BlockSpec(memory_space=pltpu.HBM),
-        scratch_shapes=[pltpu.VMEM(shape, bf16), pltpu.SemaphoreType.DMA((4,))],
-        compiler_params=SMALL,
-    )(*operands)
-
-
-def pack_body(gate, upper, down, out, packed, sems):
-    units = gate.shape[0]
-    packed[:units] = gate[...]
-    packed[units : 2 * units] = upper[...]
+def pack_body(gate_in, upper_in, down_in, out, packed, down, sems):
+    units = gate_in.shape[0]
+    into = [
+        pltpu.make_async_copy(gate_in, packed.at[:units], sems.at[0]),
+        pltpu.make_async_copy(upper_in, packed.at[units : 2 * units], sems.at[1]),
+        pltpu.make_async_copy(down_in, down, sems.at[2]),
+    ]
+    for c in into:
+        c.start()
+    for c in into:
+        c.wait()
     for at in range(0, units, LANES):
         n = min(LANES, units - at)
         rows = slice(2 * units + at, 2 * units + at + LANES)
         packed[rows, :n] = down[at : at + n].T
         if n < LANES:
             packed[rows, n:] = jnp.zeros((LANES, LANES - n), bf16)
-    repeat(packed, out, sems)
+    copies = [pltpu.make_async_copy(packed, out.at[k], sems.at[3 + k]) for k in range(4)]
+    for c in copies:
+        c.start()
+    for c in copies:
+        c.wait()
 
 
 def pack(gate, upper, down):
-    rows = 2 * gate.shape[0] + pl.cdiv(gate.shape[0], LANES) * LANES
-    return repeated(pack_body, (rows, LANES), gate, upper, down)
-
-
-def spread_body(blocks, out):
-    for k in range(4):
-        out[:, LANES * k : LANES * (k + 1)] = blocks[k]
+    units = gate.shape[0]
+    shape = (2 * units + pl.cdiv(units, LANES) * LANES, LANES)
+    return pl.pallas_call(
+        pack_body,
+        out_shape=jax.ShapeDtypeStruct((4, *shape), bf16),
+        in_specs=[pl.BlockSpec(memory_space=pltpu.HBM)] * 3,
+        out_specs=pl.BlockSpec(memory_space=pltpu.HBM),
+        scratch_shapes=[pltpu.VMEM(shape, bf16), pltpu.VMEM(down.shape, bf16), pltpu.SemaphoreType.DMA((7,))],
+        compiler_params=FULL,
+        name="pack",
+    )(gate, upper, down)
+
+
+def spread_body(blocks, *halves):
+    n = halves[0].shape[0]
+    for i, out in enumerate(halves):
+        for k in range(4):
+            out[:, LANES * k : LANES * (k + 1)] = blocks[k, n * i : n * (i + 1)]
 
 
 def spread(blocks):
     return pl.pallas_call(
         spread_body,
-        out_shape=jax.ShapeDtypeStruct((blocks.shape[1], 4 * LANES), bf16),
+        out_shape=[jax.ShapeDtypeStruct((blocks.shape[1] // 2, 4 * LANES), bf16)] * 2,
         in_specs=[WHOLE],
-        out_specs=WHOLE,
+        out_specs=[WHOLE] * 2,
         compiler_params=SMALL,
         name="spread",
     )(blocks)
 
 
-def hold_body(place_ref, here, before, after, top, bottom, out, sems):
-    at, half = place_ref[0], top.shape[0]
-    ends = [
-        (here, out.at[at]),
-        (before, out.at[(at + 3) % 4]),
-        (after, out.at[(at + 1) % 4]),
-        (top, out.at[(at + 2) % 4, :half]),
-        (bottom, out.at[(at + 2) % 4, half:]),
-    ]
-    copies = [pltpu.make_async_copy(*e, sems.at[i]) for i, e in enumerate(ends)]
+def hold_body(place_ref, *refs):
+    blocks, out, sems = refs[:8], refs[8], refs[9]
+    at, half = place_ref[0], blocks[0].shape[0]
+    copies = []
+    for i, b in enumerate(blocks):
+        end = out.at[(at + (0, 3, 1, 2)[i // 2]) % 4, half * (i % 2) : half * (i % 2 + 1)]
+        copies.append(pltpu.make_async_copy(b, end, sems.at[i]))
     for c in copies:
         c.start()
     for c in copies:
@@ -132,12 +143,13 @@
 
 
 def hold(place, blocks):
+    half, width = blocks[0].shape
     return pl.pallas_call(
         hold_body,
-        out_shape=jax.ShapeDtypeStruct((4, *blocks[0].shape), bf16),
-        in_specs=[pl.BlockSpec(memory_space=pltpu.SMEM)] + [pl.BlockSpec(memory_space=pltpu.HBM)] * 5,
+        out_shape=jax.ShapeDtypeStruct((4, 2 * half, width), bf16),
+        in_specs=[pl.BlockSpec(memory_space=pltpu.SMEM)] + [pl.BlockSpec(memory_space=pltpu.HBM)] * 8,
         out_specs=WHOLE,
-        scratch_shapes=[pltpu.SemaphoreType.DMA((5,))],
+        scratch_shapes=[pltpu.SemaphoreType.DMA((8,))],
         compiler_params=SMALL,
         name="hold",
     )(place, *blocks)
@@ -228,13 +240,14 @@
             mate[d] = onward(mate[d - 1], 1)
 
     rows = from_four(pack(gate_weight.T, up_weight.T, down_weight), ROWS)
-    here = spread(rows)
-    half = here.shape[0] // 2
-    before = along_column(here, 1)
-    after = along_column(here, -1)
-    top = along_column(before[:half], 1)
-    bottom = along_column(after[half:], -1)
-    blocks = here, before, after, top, bottom
+    top, bottom = spread(rows)
+    before_top = along_column(top, 1)
+    after_bottom = along_column(bottom, -1)
+    before_bottom = along_column(bottom, 1)
+    after_top = along_column(top, -1)
+    far_top = along_column(before_top, 1)
+    far_bottom = along_column(after_bottom, -1)
+    blocks = top, bottom, before_top, before_bottom, after_top, after_bottom, far_top, far_bottom
     others = []
     for b in blocks:
         others.append(swap(b))

time: 121 us -> 128 us (1.058)
  the two profiles are of different devices: /device:TPU:2 before, /device:TPU:1 now
where the time goes in v3:
time: 128 us
  waiting for transfers between devices  46 us (36%)
  starting transfers between devices  42.3 us (33%)
  Pallas kernels  29.1 us (23%)
  local copies, waits for them, and re-layouts  9.23 us (7%)
    ppermute x14, waiting for transfers between devices, onward(): return lax.ppermute(x, ('z', 'c'), pairs)  43.4 us
    ppermute x14, starting transfers between devices, onward(): return lax.ppermute(x, ('z', 'c'), pairs)  19.4 us
    pallas_call x8, Pallas kernels, call(): pl.pallas_call(functools.partial(body, n, units), out_shape=out_shape, in...  18.3 us
    ppermute x10, starting transfers between devices, swap(): return lax.ppermute(x, 'c', [(0, 1), (1, 0)])  9.72 us
    unnamed x30, local copies, waits for them, and re-layouts  9.23 us
    ppermute x6, starting transfers between devices, along_column(): return lax.ppermute(x, ('y', 'x', 'c'), pairs)  8.14 us
    all_to_all x1, starting transfers between devices, from_four(): lax.all_to_all(copies, AXES, 0, 0, axis_index_groups=groups, tiled=True)  5.01 us
    pallas_call x2, Pallas kernels, hold(): pl.pallas_call(hold_body, out_shape=jax.ShapeDtypeStruct((4, 2 * half, wi...  4.05 us
  transfers between devices with their start and end apart: 31, of which 15 were waited for; matrix products, arithmetic and copies ran while one was open for 1% of the time, Pallas kernels for 16%

profile of v3, /device:TPU:1, one launch (start us, length us, event | category | flops | bytes accessed | tf_op | source)
XLA Modules:
  0.0 127.6 jit_solution(16454441934313773287)
XLA Ops:
  0.0 2.1 %pack.1 = bf16[4,1088,128]{2,1,0:T(8,128)(2,1)} custom-call(bf16[352,128]{1,0:T(8,128)(2,1)} %bitcast.6, bf16[352,128]{1,0:T(8,128)(2,1)} %bitcast.7, bf16[352,128]{1,0:T(8,128)(2,1)} %down_in.1), custom_call_target="tpu_custom_call" | custom-call | tf_op jit(solution)/shard_map/pack/pallas_call | solution.py:103
  2.1 5.0 %all-to-all-start = ((bf16[4,1088,128]{2,1,0:T(8,128)(2,1)}), bf16[4,1088,128]{2,1,0:T(8,128)(2,1)}, u32[]{:S(2)}, u32[]{:S(2)}) async-start(bf16[4,1088,128]{2,1,0:T(8,128)(2,1)} %pack.1), calls=%async_computation | async-start | bytes 2228224 | tf_op jit(solution)/shard_map/all_to_all | solution.py:46
  7.2 2.2 %norm.1.refs_1_ = bf16[2048,128]{1,0:T(8,128)(2,1)} custom-call(bf16[128,2048]{1,0:T(8,128)(2,1)} %tokens_in.1, f32[1,2048]{1,0:T(1,128)} %bitcast.8), custom_call_target="tpu_custom_call" | custom-call | tf_op jit(solution)/shard_map/norm/pallas_call | solution.py:61
  9.4 5.7 %collective-permute-start = (bf16[2048,128]{1,0:T(8,128)(2,1)}, bf16[2048,128]{1,0:T(8,128)(2,1)S(1)}, u32[]{:S(2)}, u32[]{:S(2)}) collective-permute-start(bf16[2048,128]{1,0:T(8,128)(2,1)} %norm.1.refs_1_), channel_id=1, source_target_pairs={{0,2},{1,15},{2,4},{3,1},{4,6},{5,3},{6,8},{7,5},{8,10},{9,7},{10,... | collective-permute-start | bytes 1572872 | tf_op jit(solution)/shard_map/ppermute | solution.py:31
  15.1 2.5 %all-to-all-done.blocks = bf16[4,1088,128]{2,1,0:T(8,128)(2,1)} async-done(((bf16[4,1088,128]{2,1,0:T(8,128)(2,1)}), bf16[4,1088,128]{2,1,0:T(8,128)(2,1)}, u32[]{:S(2)}, u32[]{:S(2)}) %all-to-all-start) | async-done | bytes 1114144 | tf_op jit(solution)/shard_map/all_to_all | solution.py:46
  17.6 1.4 %spread.1 = (bf16[544,512]{1,0:T(8,128)(2,1)S(1)}, bf16[544,512]{1,0:T(8,128)(2,1)S(1)}) custom-call(bf16[4,1088,128]{2,1,0:T(8,128)(2,1)} %all-to-all-done.blocks), custom_call_target="tpu_custom_call" | custom-call | tf_op jit(solution)/shard_map/spread/pallas_call | solution.py:122
  19.1 1.0 collective-permute-start.1
  20.1 1.4 %collective-permute-done.refs_0_ = bf16[2048,128]{1,0:T(8,128)(2,1)S(1)} collective-permute-done((bf16[2048,128]{1,0:T(8,128)(2,1)}, bf16[2048,128]{1,0:T(8,128)(2,1)S(1)}, u32[]{:S(2)}, u32[]{:S(2)}) %collective-permute-start) | collective-permute-done | bytes 524320 | tf_op jit(solution)/shard_map/ppermute | solution.py:31
  21.6 4.1 %collective-permute-start.15 = (bf16[2048,128]{1,0:T(8,128)(2,1)S(1)}, bf16[2048,128]{1,0:T(8,128)(2,1)S(1)}, u32[]{:S(2)}, u32[]{:S(2)}) collective-permute-start(bf16[2048,128]{1,0:T(8,128)(2,1)S(1)} %collective-permute-done.refs_0_), channel_id=1, source_target_pairs={{0,2},{1,15},{2,4},{3,1},{4,6},{5,3},{6,8},{7,5},{8,10},{9,7},{10,... | collective-permute-start | bytes 1572872 | tf_op jit(solution)/shard_map/ppermute | solution.py:31
  26.4 1.2 collective-permute-start.2
  27.6 1.5 %collective-permute-start.3 = (bf16[544,512]{1,0:T(8,128)(2,1)S(1)}, bf16[544,512]{1,0:T(8,128)(2,1)}, u32[]{:S(2)}, u32[]{:S(2)}) collective-permute-start(bf16[544,512]{1,0:T(8,128)(2,1)S(1)} %get-tuple-element.15.refs_0_), channel_id=1, source_target_pairs={{0,192},{16,208},{32,224},{48,240},{64,0},{80,16},{96,32},{112,48}... | collective-permute-start | bytes 1671176 | tf_op jit(solution)/shard_map/ppermute | solution.py:38
  29.1 2.7 %collective-permute-done.15.refs_0_ = bf16[2048,128]{1,0:T(8,128)(2,1)S(1)} collective-permute-done((bf16[2048,128]{1,0:T(8,128)(2,1)S(1)}, bf16[2048,128]{1,0:T(8,128)(2,1)S(1)}, u32[]{:S(2)}, u32[]{:S(2)}) %collective-permute-start.15) | collective-permute-done | bytes 524320 | tf_op jit(solution)/shard_map/ppermute | solution.py:31
  31.8 1.8 %collective-permute-start.4 = (bf16[544,512]{1,0:T(8,128)(2,1)S(1)}, bf16[544,512]{1,0:T(8,128)(2,1)}, u32[]{:S(2)}, u32[]{:S(2)}) collective-permute-start(bf16[544,512]{1,0:T(8,128)(2,1)S(1)} %get-tuple-element.16.refs_1_), channel_id=1, source_target_pairs={{0,192},{16,208},{32,224},{48,240},{64,0},{80,16},{96,32},{112,48}... | collective-permute-start | bytes 1671176 | tf_op jit(solution)/shard_map/ppermute | solution.py:38
  33.6 3.9 %collective-permute-done.19.refs_1_ = bf16[2048,128]{1,0:T(8,128)(2,1)S(1)} collective-permute-done((bf16[2048,128]{1,0:T(8,128)(2,1)S(1)}, bf16[2048,128]{1,0:T(8,128)(2,1)S(1)}, u32[]{:S(2)}, u32[]{:S(2)}) %collective-permute-start.19) | collective-permute-done | bytes 524320 | tf_op jit(solution)/shard_map/ppermute | solution.py:31
  37.4 3.6 %collective-permute-start.7 = (bf16[544,512]{1,0:T(8,128)(2,1)S(1)}, bf16[544,512]{1,0:T(8,128)(2,1)S(1)}, u32[]{:S(2)}, u32[]{:S(2)}) collective-permute-start(bf16[544,512]{1,0:T(8,128)(2,1)S(1)} %get-tuple-element.15.refs_0_), channel_id=1, source_target_pairs={{0,1},{1,0},{2,3},{3,2},{4,5},{5,4},{6,7},{7,6},{8,9},{9,8},{10,11... | collective-permute-start | bytes 1671176 | tf_op jit(solution)/shard_map/ppermute | solution.py:42
  41.0 0.8 copy-done.3
  41.9 0.8 copy-done.5
  42.7 1.7 %collective-permute-start.16 = (bf16[2048,128]{1,0:T(8,128)(2,1)S(1)}, bf16[2048,128]{1,0:T(8,128)(2,1)S(1)}, u32[]{:S(2)}, u32[]{:S(2)}) collective-permute-start(bf16[2048,128]{1,0:T(8,128)(2,1)S(1)} %collective-permute-done.15.refs_0_), channel_id=1, source_target_pairs={{0,2},{1,15},{2,4},{3,1},{4,6},{5,3},{6,8},{7,5},{8,10},{9,7},{10,... | collective-permute-start | bytes 1572872 | tf_op jit(solution)/shard_map/ppermute | solution.py:31
  45.5 0.8 copy-done.9
  46.3 2.4 %collective-permute-start.6 = (bf16[544,512]{1,0:T(8,128)(2,1)}, bf16[544,512]{1,0:T(8,128)(2,1)}, u32[]{:S(2)}, u32[]{:S(2)}) collective-permute-start(bf16[544,512]{1,0:T(8,128)(2,1)} %collective-permute-done.4.refs_5_), channel_id=1, source_target_pairs={{0,192},{16,208},{32,224},{48,240},{64,0},{80,16},{96,32},{112,48}... | collective-permute-start | bytes 1671176 | tf_op jit(solution)/shard_map/ppermute | solution.py:38
  48.7 0.8 copy-done.11
  49.9 0.8 copy-done.7
  51.2 3.0 %collective-permute-start.17 = (bf16[2048,128]{1,0:T(8,128)(2,1)S(1)}, bf16[2048,128]{1,0:T(8,128)(2,1)S(1)}, u32[]{:S(2)}, u32[]{:S(2)}) collective-permute-start(bf16[2048,128]{1,0:T(8,128)(2,1)S(1)} %collective-permute-done.16.refs_0_), channel_id=1, source_target_pairs={{0,2},{1,15},{2,4},{3,1},{4,6},{5,3},{6,8},{7,5},{8,10},{9,7},{10,... | collective-permute-start | bytes 1572872 | tf_op jit(solution)/shard_map/ppermute | solution.py:31
  54.1 2.7 %collective-permute-done.20.refs_1_ = bf16[2048,128]{1,0:T(8,128)(2,1)S(1)} collective-permute-done((bf16[2048,128]{1,0:T(8,128)(2,1)S(1)}, bf16[2048,128]{1,0:T(8,128)(2,1)S(1)}, u32[]{:S(2)}, u32[]{:S(2)}) %collective-permute-start.20) | collective-permute-done | bytes 524320 | tf_op jit(solution)/shard_map/ppermute | solution.py:31
  56.8 2.6 %collective-permute-start.21 = (bf16[2048,128]{1,0:T(8,128)(2,1)S(1)}, bf16[2048,128]{1,0:T(8,128)(2,1)S(1)}, u32[]{:S(2)}, u32[]{:S(2)}) collective-permute-start(bf16[2048,128]{1,0:T(8,128)(2,1)S(1)} %collective-permute-done.20.refs_1_), channel_id=1, source_target_pairs={{0,2},{1,15},{2,4},{3,1},{4,6},{5,3},{6,8},{7,5},{8,10},{9,7},{10,... | collective-permute-start | bytes 1572872 | tf_op jit(solution)/shard_map/ppermute | solution.py:31
  60.7 1.5 %collective-permute-done.17.refs_0_ = bf16[2048,128]{1,0:T(8,128)(2,1)S(1)} collective-permute-done((bf16[2048,128]{1,0:T(8,128)(2,1)S(1)}, bf16[2048,128]{1,0:T(8,128)(2,1)S(1)}, u32[]{:S(2)}, u32[]{:S(2)}) %collective-permute-start.17) | collective-permute-done | bytes 524320 | tf_op jit(solution)/shard_map/ppermute | solution.py:31
  62.3 2.6 %collective-permute-start.13 = (bf16[544,512]{1,0:T(8,128)(2,1)}, bf16[544,512]{1,0:T(8,128)(2,1)}, u32[]{:S(2)}, u32[]{:S(2)}) collective-permute-start(bf16[544,512]{1,0:T(8,128)(2,1)} %collective-permute-done.5.refs_6_), channel_id=1, source_target_pairs={{0,1},{1,0},{2,3},{3,2},{4,5},{5,4},{6,7},{7,6},{8,9},{9,8},{10,11... | collective-permute-start | bytes 1671176 | tf_op jit(solution)/shard_map/ppermute | solution.py:42
  64.9 3.0 %collective-permute-done.21.refs_1_ = bf16[2048,128]{1,0:T(8,128)(2,1)S(1)} collective-permute-done((bf16[2048,128]{1,0:T(8,128)(2,1)S(1)}, bf16[2048,128]{1,0:T(8,128)(2,1)S(1)}, u32[]{:S(2)}, u32[]{:S(2)}) %collective-permute-start.21) | collective-permute-done | bytes 524320 | tf_op jit(solution)/shard_map/ppermute | solution.py:31
  68.7 2.6 %collective-permute-start.14 = (bf16[544,512]{1,0:T(8,128)(2,1)}, bf16[544,512]{1,0:T(8,128)(2,1)}, u32[]{:S(2)}, u32[]{:S(2)}) collective-permute-start(bf16[544,512]{1,0:T(8,128)(2,1)} %collective-permute-done.6.refs_7_), channel_id=1, source_target_pairs={{0,1},{1,0},{2,3},{3,2},{4,5},{5,4},{6,7},{7,6},{8,9},{9,8},{10,11... | collective-permute-start | bytes 1671176 | tf_op jit(solution)/shard_map/ppermute | solution.py:42
  71.3 1.1 copy-done.4
  72.3 1.1 copy-done.6
  73.4 1.1 copy-done.8
  74.4 2.0 %hold.2.refs_2_ = bf16[4,1088,512]{2,1,0:T(8,128)(2,1)S(1)} custom-call(s32[1]{0:T(128)S(6)} %select_n.7.place_ref, bf16[544,512]{1,0:T(8,128)(2,1)S(1)} %copy-done.4, bf16[544,512]{1,0:T(8,128)(2,1)S(1)} %copy-done.6, bf16[544,512]{1,0:T(8,128)(2,1)S(1)} %copy-done.8, bf16[544,512]{1,0:T(8,128)(2,1)} %collective-permute-done.2.refs_3_, ...), custom_call_target="tpu_custom_call" | custom-call | tf_op jit(solution)/shard_map/hold/pallas_call | solution.py:147
  76.5 1.0 shard_map.57.refs_4_
  77.9 2.0 %hold.3.refs_3_ = bf16[4,1088,512]{2,1,0:T(8,128)(2,1)S(1)} custom-call(s32[1]{0:T(128)S(6)} %select_n.8.place_ref, bf16[544,512]{1,0:T(8,128)(2,1)S(1)} %copy-done.10, bf16[544,512]{1,0:T(8,128)(2,1)S(1)} %copy-done.12, bf16[544,512]{1,0:T(8,128)(2,1)S(1)} %copy-done.14, bf16[544,512]{1,0:T(8,128)(2,1)} %collective-permute-done.10.refs_3_, ...), custom_call_target="tpu_custom_call" | custom-call | tf_op jit(solution)/shard_map/hold/pallas_call | solution.py:147
  79.9 3.6 %shard_map.58 = (bf16[2048,128]{1,0:T(8,128)(2,1)S(1)}, bf16[2048,128]{1,0:T(8,128)(2,1)S(1)}) custom-call(s32[1]{0:T(128)} %bitcast.core_ref, bf16[2048,128]{1,0:T(8,128)(2,1)S(1)} %collective-permute-done.17.refs_0_, bf16[2048,128]{1,0:T(8,128)(2,1)S(1)} %copy-done.2, bf16[4,1088,512]{2,1,0:T(8,128)(2,1)S(1)} %hold.2.refs_2_, ...), custom_call_target="tpu_custom_call" | custom-call | tf_op jit(solution)/shard_map/pallas_call | solution.py:197
  83.7 1.0 shard_map.59.refs_4_
  84.7 3.6 %shard_map.60 = (f32[2048,128]{1,0:T(8,128)S(1)}, f32[2048,128]{1,0:T(8,128)S(1)}) custom-call(s32[1]{0:T(128)} %bitcast.core_ref, bf16[2048,128]{1,0:T(8,128)(2,1)S(1)} %collective-permute-done.16.refs_0_, bf16[2048,128]{1,0:T(8,128)(2,1)S(1)} %collective-permute-done.20.refs_1_, bf16[4,1088,512]{2,1,0:T(8,128)(2,1)S(1)} %hold.2.refs_2_, ...), custom_call_target="tpu_custom_call" | custom-call | tf_op jit(solution)/shard_map/pallas_call | solution.py:197
  88.3 4.6 %collective-permute-done.22 = bf16[2048,128]{1,0:T(8,128)(2,1)S(1)} collective-permute-done((bf16[2048,128]{1,0:T(8,128)(2,1)S(1)}, bf16[2048,128]{1,0:T(8,128)(2,1)S(1)}, u32[]{:S(2)}, u32[]{:S(2)}) %collective-permute-start.22) | collective-permute-done | bytes 524320 | tf_op jit(solution)/shard_map/ppermute | solution.py:31
  93.3 5.2 %collective-permute-done.26 = bf16[2048,128]{1,0:T(8,128)(2,1)S(1)} collective-permute-done((bf16[2048,128]{1,0:T(8,128)(2,1)S(1)}, bf16[2048,128]{1,0:T(8,128)(2,1)S(1)}, u32[]{:S(2)}, u32[]{:S(2)}) %collective-permute-start.26) | collective-permute-done | bytes 524320 | tf_op jit(solution)/shard_map/ppermute | solution.py:31
  98.7 1.0 shard_map.61.refs_4_
  99.7 3.6 %shard_map.62 = (f32[2048,128]{1,0:T(8,128)S(1)}, f32[2048,128]{1,0:T(8,128)S(1)}) custom-call(s32[1]{0:T(128)} %bitcast.core_ref, bf16[2048,128]{1,0:T(8,128)(2,1)S(1)} %collective-permute-done.15.refs_0_, bf16[2048,128]{1,0:T(8,128)(2,1)S(1)} %collective-permute-done.19.refs_1_, bf16[4,1088,512]{2,1,0:T(8,128)(2,1)S(1)} %hold.2.refs_2_, ...), custom_call_target="tpu_custom_call" | custom-call | tf_op jit(solution)/shard_map/pallas_call | solution.py:197
  104.3 5.4 %collective-permute-done.27 = bf16[2048,128]{1,0:T(8,128)(2,1)S(1)} collective-permute-done((bf16[2048,128]{1,0:T(8,128)(2,1)S(1)}, bf16[2048,128]{1,0:T(8,128)(2,1)S(1)}, u32[]{:S(2)}, u32[]{:S(2)}) %collective-permute-start.27) | collective-permute-done | bytes 524320 | tf_op jit(solution)/shard_map/ppermute | solution.py:31
  109.9 1.0 shard_map.55.refs_4_
  110.9 3.6 %shard_map.56 = (f32[2048,128]{1,0:T(8,128)S(1)}, f32[2048,128]{1,0:T(8,128)S(1)}) custom-call(s32[1]{0:T(128)} %bitcast.core_ref, bf16[2048,128]{1,0:T(8,128)(2,1)S(1)} %collective-permute-done.refs_0_, bf16[2048,128]{1,0:T(8,128)(2,1)S(1)} %copy-done, bf16[4,1088,512]{2,1,0:T(8,128)(2,1)S(1)} %hold.2.refs_2_, bf16[4,1088,512]{2,1,0:T(8,128)(2,1)S(1)} %hold.3.refs_3_, ...), custom_call_target="tpu_custom_call" | custom-call | tf_op jit(solution)/shard_map/pallas_call | solution.py:197
  115.5 5.4 %collective-permute-done.28 = bf16[2048,128]{1,0:T(8,128)(2,1)S(1)} collective-permute-done((bf16[2048,128]{1,0:T(8,128)(2,1)S(1)}, bf16[2048,128]{1,0:T(8,128)(2,1)S(1)}, u32[]{:S(2)}, u32[]{:S(2)}) %collective-permute-start.28) | collective-permute-done | bytes 524320 | tf_op jit(solution)/shard_map/ppermute | solution.py:31
  120.9 5.6 %collective-permute-done.25.first = bf16[2048,128]{1,0:T(8,128)(2,1)S(1)} collective-permute-done((bf16[2048,128]{1,0:T(8,128)(2,1)S(1)}, bf16[2048,128]{1,0:T(8,128)(2,1)S(1)}, u32[]{:S(2)}, u32[]{:S(2)}) %collective-permute-start.25) | collective-permute-done | bytes 524320 | tf_op jit(solution)/shard_map/ppermute | solution.py:31
  126.5 1.0 close.1
  (63 shorter events, 8.2 us)
Async XLA Ops:
  2.1 15.5 %all-to-all-start = ((bf16[4,1088,128]{2,1,0:T(8,128)(2,1)}), bf16[4,1088,128]{2,1,0:T(8,128)(2,1)}, u32[]{:S(2)}, u32[]{:S(2)}) async-start(bf16[4,1088,128]{2,1,0:T(8,128)(2,1)} %pack.1), calls=%async_computation | async-start | bytes 2228224 | tf_op jit(solution)/shard_map/all_to_all | solution.py:46
  9.4 12.2 %collective-permute-start = (bf16[2048,128]{1,0:T(8,128)(2,1)}, bf16[2048,128]{1,0:T(8,128)(2,1)S(1)}, u32[]{:S(2)}, u32[]{:S(2)}) collective-permute-start(bf16[2048,128]{1,0:T(8,128)(2,1)} %norm.1.refs_1_), channel_id=1, source_target_pairs={{0,2},{1,15},{2,4},{3,1},{4,6},{5,3},{6,8},{7,5},{8,10},{9,7},{10,... | collective-permute-start | bytes 1572872 | tf_op jit(solution)/shard_map/ppermute | solution.py:31
  15.1 10.6 %collective-permute-start.18 = (bf16[2048,128]{1,0:T(8,128)(2,1)}, bf16[2048,128]{1,0:T(8,128)(2,1)S(1)}, u32[]{:S(2)}, u32[]{:S(2)}) collective-permute-start(bf16[2048,128]{1,0:T(8,128)(2,1)} %norm.1.refs_1_), channel_id=1, source_target_pairs={{0,1},{1,0},{2,3},{3,2},{4,5},{5,4},{6,7},{7,6},{8,9},{9,8},{10,11... | collective-permute-start | bytes 1572872 | tf_op jit(solution)/shard_map/ppermute | solution.py:42
  19.1 22.8 %collective-permute-start.1 = (bf16[544,512]{1,0:T(8,128)(2,1)S(1)}, bf16[544,512]{1,0:T(8,128)(2,1)S(1)}, u32[]{:S(2)}, u32[]{:S(2)}) collective-permute-start(bf16[544,512]{1,0:T(8,128)(2,1)S(1)} %get-tuple-element.15.refs_0_), channel_id=1, source_target_pairs={{0,64},{16,80},{32,96},{48,112},{64,128},{80,144},{96,160},{112,17... | collective-permute-start | bytes 1671176 | tf_op jit(solution)/shard_map/ppermute | solution.py:38
  21.6 10.3 %collective-permute-start.15 = (bf16[2048,128]{1,0:T(8,128)(2,1)S(1)}, bf16[2048,128]{1,0:T(8,128)(2,1)S(1)}, u32[]{:S(2)}, u32[]{:S(2)}) collective-permute-start(bf16[2048,128]{1,0:T(8,128)(2,1)S(1)} %collective-permute-done.refs_0_), channel_id=1, source_target_pairs={{0,2},{1,15},{2,4},{3,1},{4,6},{5,3},{6,8},{7,5},{8,10},{9,7},{10,... | collective-permute-start | bytes 1572872 | tf_op jit(solution)/shard_map/ppermute | solution.py:31
  25.7 11.7 %collective-permute-start.19 = (bf16[2048,128]{1,0:T(8,128)(2,1)S(1)}, bf16[2048,128]{1,0:T(8,128)(2,1)S(1)}, u32[]{:S(2)}, u32[]{:S(2)}) collective-permute-start(bf16[2048,128]{1,0:T(8,128)(2,1)S(1)} %collective-permute-done.18), channel_id=1, source_target_pairs={{0,2},{1,15},{2,4},{3,1},{4,6},{5,3},{6,8},{7,5},{8,10},{9,7},{10,... | collective-permute-start | bytes 1572872 | tf_op jit(solution)/shard_map/ppermute | solution.py:31
  26.4 16.3 %collective-permute-start.2 = (bf16[544,512]{1,0:T(8,128)(2,1)S(1)}, bf16[544,512]{1,0:T(8,128)(2,1)}, u32[]{:S(2)}, u32[]{:S(2)}) collective-permute-start(bf16[544,512]{1,0:T(8,128)(2,1)S(1)} %get-tuple-element.16.refs_1_), channel_id=1, source_target_pairs={{0,64},{16,80},{32,96},{48,112},{64,128},{80,144},{96,160},{112,17... | collective-permute-start | bytes 1671176 | tf_op jit(solution)/shard_map/ppermute | solution.py:38
  27.6 16.8 %collective-permute-start.3 = (bf16[544,512]{1,0:T(8,128)(2,1)S(1)}, bf16[544,512]{1,0:T(8,128)(2,1)}, u32[]{:S(2)}, u32[]{:S(2)}) collective-permute-start(bf16[544,512]{1,0:T(8,128)(2,1)S(1)} %get-tuple-element.15.refs_0_), channel_id=1, source_target_pairs={{0,192},{16,208},{32,224},{48,240},{64,0},{80,16},{96,32},{112,48}... | collective-permute-start | bytes 1671176 | tf_op jit(solution)/shard_map/ppermute | solution.py:38
  31.8 13.4 %collective-permute-start.4 = (bf16[544,512]{1,0:T(8,128)(2,1)S(1)}, bf16[544,512]{1,0:T(8,128)(2,1)}, u32[]{:S(2)}, u32[]{:S(2)}) collective-permute-start(bf16[544,512]{1,0:T(8,128)(2,1)S(1)} %get-tuple-element.16.refs_1_), channel_id=1, source_target_pairs={{0,192},{16,208},{32,224},{48,240},{64,0},{80,16},{96,32},{112,48}... | collective-permute-start | bytes 1671176 | tf_op jit(solution)/shard_map/ppermute | solution.py:38
  37.4 8.1 %collective-permute-start.7 = (bf16[544,512]{1,0:T(8,128)(2,1)S(1)}, bf16[544,512]{1,0:T(8,128)(2,1)S(1)}, u32[]{:S(2)}, u32[]{:S(2)}) collective-permute-start(bf16[544,512]{1,0:T(8,128)(2,1)S(1)} %get-tuple-element.15.refs_0_), channel_id=1, source_target_pairs={{0,1},{1,0},{2,3},{3,2},{4,5},{5,4},{6,7},{7,6},{8,9},{9,8},{10,11... | collective-permute-start | bytes 1671176 | tf_op jit(solution)/shard_map/ppermute | solution.py:42
  41.0 0.8 copy-start.3
  41.9 6.8 %collective-permute-start.8 = (bf16[544,512]{1,0:T(8,128)(2,1)S(1)}, bf16[544,512]{1,0:T(8,128)(2,1)S(1)}, u32[]{:S(2)}, u32[]{:S(2)}) collective-permute-start(bf16[544,512]{1,0:T(8,128)(2,1)S(1)} %get-tuple-element.16.refs_1_), channel_id=1, source_target_pairs={{0,1},{1,0},{2,3},{3,2},{4,5},{5,4},{6,7},{7,6},{8,9},{9,8},{10,11... | collective-permute-start | bytes 1671176 | tf_op jit(solution)/shard_map/ppermute | solution.py:42
  41.9 0.9 copy-start.5
  42.7 8.4 %collective-permute-start.16 = (bf16[2048,128]{1,0:T(8,128)(2,1)S(1)}, bf16[2048,128]{1,0:T(8,128)(2,1)S(1)}, u32[]{:S(2)}, u32[]{:S(2)}) collective-permute-start(bf16[2048,128]{1,0:T(8,128)(2,1)S(1)} %collective-permute-done.15.refs_0_), channel_id=1, source_target_pairs={{0,2},{1,15},{2,4},{3,1},{4,6},{5,3},{6,8},{7,5},{8,10},{9,7},{10,... | collective-permute-start | bytes 1572872 | tf_op jit(solution)/shard_map/ppermute | solution.py:31
  44.5 12.3 %collective-permute-start.20 = (bf16[2048,128]{1,0:T(8,128)(2,1)S(1)}, bf16[2048,128]{1,0:T(8,128)(2,1)S(1)}, u32[]{:S(2)}, u32[]{:S(2)}) collective-permute-start(bf16[2048,128]{1,0:T(8,128)(2,1)S(1)} %collective-permute-done.19.refs_1_), channel_id=1, source_target_pairs={{0,2},{1,15},{2,4},{3,1},{4,6},{5,3},{6,8},{7,5},{8,10},{9,7},{10,... | collective-permute-start | bytes 1572872 | tf_op jit(solution)/shard_map/ppermute | solution.py:31
  45.2 14.1 %collective-permute-start.5 = (bf16[544,512]{1,0:T(8,128)(2,1)S(1)}, bf16[544,512]{1,0:T(8,128)(2,1)}, u32[]{:S(2)}, u32[]{:S(2)}) collective-permute-start(bf16[544,512]{1,0:T(8,128)(2,1)S(1)} %collective-permute-done.1.refs_2_), channel_id=1, source_target_pairs={{0,64},{16,80},{32,96},{48,112},{64,128},{80,144},{96,160},{112,17... | collective-permute-start | bytes 1671176 | tf_op jit(solution)/shard_map/ppermute | solution.py:38
  45.5 0.8 copy-start.9
  46.3 13.0 %collective-permute-start.6 = (bf16[544,512]{1,0:T(8,128)(2,1)}, bf16[544,512]{1,0:T(8,128)(2,1)}, u32[]{:S(2)}, u32[]{:S(2)}) collective-permute-start(bf16[544,512]{1,0:T(8,128)(2,1)} %collective-permute-done.4.refs_5_), channel_id=1, source_target_pairs={{0,192},{16,208},{32,224},{48,240},{64,0},{80,16},{96,32},{112,48}... | collective-permute-start | bytes 1671176 | tf_op jit(solution)/shard_map/ppermute | solution.py:38
  48.7 0.8 copy-start.11
  49.5 10.3 %collective-permute-start.9 = (bf16[544,512]{1,0:T(8,128)(2,1)S(1)}, bf16[544,512]{1,0:T(8,128)(2,1)S(1)}, u32[]{:S(2)}, u32[]{:S(2)}) collective-permute-start(bf16[544,512]{1,0:T(8,128)(2,1)S(1)} %collective-permute-done.1.refs_2_), channel_id=1, source_target_pairs={{0,1},{1,0},{2,3},{3,2},{4,5},{5,4},{6,7},{7,6},{8,9},{9,8},{10,11... | collective-permute-start | bytes 1671176 | tf_op jit(solution)/shard_map/ppermute | solution.py:42
  49.9 0.8 copy-start.7
  51.2 11.1 %collective-permute-start.17 = (bf16[2048,128]{1,0:T(8,128)(2,1)S(1)}, bf16[2048,128]{1,0:T(8,128)(2,1)S(1)}, u32[]{:S(2)}, u32[]{:S(2)}) collective-permute-start(bf16[2048,128]{1,0:T(8,128)(2,1)S(1)} %collective-permute-done.16.refs_0_), channel_id=1, source_target_pairs={{0,2},{1,15},{2,4},{3,1},{4,6},{5,3},{6,8},{7,5},{8,10},{9,7},{10,... | collective-permute-start | bytes 1572872 | tf_op jit(solution)/shard_map/ppermute | solution.py:31
  56.8 11.1 %collective-permute-start.21 = (bf16[2048,128]{1,0:T(8,128)(2,1)S(1)}, bf16[2048,128]{1,0:T(8,128)(2,1)S(1)}, u32[]{:S(2)}, u32[]{:S(2)}) collective-permute-start(bf16[2048,128]{1,0:T(8,128)(2,1)S(1)} %collective-permute-done.20.refs_1_), channel_id=1, source_target_pairs={{0,2},{1,15},{2,4},{3,1},{4,6},{5,3},{6,8},{7,5},{8,10},{9,7},{10,... | collective-permute-start | bytes 1572872 | tf_op jit(solution)/shard_map/ppermute | solution.py:31
  59.3 18.2 %collective-permute-start.12 = (bf16[544,512]{1,0:T(8,128)(2,1)}, bf16[544,512]{1,0:T(8,128)(2,1)}, u32[]{:S(2)}, u32[]{:S(2)}) collective-permute-start(bf16[544,512]{1,0:T(8,128)(2,1)} %collective-permute-done.4.refs_5_), channel_id=1, source_target_pairs={{0,1},{1,0},{2,3},{3,2},{4,5},{5,4},{6,7},{7,6},{8,9},{9,8},{10,11... | collective-permute-start | bytes 1671176 | tf_op jit(solution)/shard_map/ppermute | solution.py:42
  59.3 18.2 %collective-permute-start.10 = (bf16[544,512]{1,0:T(8,128)(2,1)}, bf16[544,512]{1,0:T(8,128)(2,1)}, u32[]{:S(2)}, u32[]{:S(2)}) collective-permute-start(bf16[544,512]{1,0:T(8,128)(2,1)} %collective-permute-done.2.refs_3_), channel_id=1, source_target_pairs={{0,1},{1,0},{2,3},{3,2},{4,5},{5,4},{6,7},{7,6},{8,9},{9,8},{10,11... | collective-permute-start | bytes 1671176 | tf_op jit(solution)/shard_map/ppermute | solution.py:42
  59.9 0.8 copy-start.13
  60.7 16.9 %collective-permute-start.11 = (bf16[544,512]{1,0:T(8,128)(2,1)}, bf16[544,512]{1,0:T(8,128)(2,1)}, u32[]{:S(2)}, u32[]{:S(2)}) collective-permute-start(bf16[544,512]{1,0:T(8,128)(2,1)} %collective-permute-done.3.refs_4_), channel_id=1, source_target_pairs={{0,1},{1,0},{2,3},{3,2},{4,5},{5,4},{6,7},{7,6},{8,9},{9,8},{10,11... | collective-permute-start | bytes 1671176 | tf_op jit(solution)/shard_map/ppermute | solution.py:42
  62.3 15.3 %collective-permute-start.13 = (bf16[544,512]{1,0:T(8,128)(2,1)}, bf16[544,512]{1,0:T(8,128)(2,1)}, u32[]{:S(2)}, u32[]{:S(2)}) collective-permute-start(bf16[544,512]{1,0:T(8,128)(2,1)} %collective-permute-done.5.refs_6_), channel_id=1, source_target_pairs={{0,1},{1,0},{2,3},{3,2},{4,5},{5,4},{6,7},{7,6},{8,9},{9,8},{10,11... | collective-permute-start | bytes 1671176 | tf_op jit(solution)/shard_map/ppermute | solution.py:42
  67.9 0.8 copy-start.1
  68.7 8.9 %collective-permute-start.14 = (bf16[544,512]{1,0:T(8,128)(2,1)}, bf16[544,512]{1,0:T(8,128)(2,1)}, u32[]{:S(2)}, u32[]{:S(2)}) collective-permute-start(bf16[544,512]{1,0:T(8,128)(2,1)} %collective-permute-done.6.refs_7_), channel_id=1, source_target_pairs={{0,1},{1,0},{2,3},{3,2},{4,5},{5,4},{6,7},{7,6},{8,9},{9,8},{10,11... | collective-permute-start | bytes 1671176 | tf_op jit(solution)/shard_map/ppermute | solution.py:42
  71.3 1.1 copy-start.4
  72.3 1.1 copy-start.6
  73.4 1.1 copy-start.8
  74.4 2.0 %copy-start.2 = (bf16[2048,128]{1,0:T(8,128)(2,1)S(1)}, bf16[2048,128]{1,0:T(8,128)(2,1)}, u32[]{:S(2)}) copy-start(bf16[2048,128]{1,0:T(8,128)(2,1)} %copy-done.1) | copy-start | bytes 1572868
  76.5 1.1 copy-start.10
  76.5 1.2 copy-start.12
  76.5 1.4 %copy-start.14 = (bf16[544,512]{1,0:T(8,128)(2,1)S(1)}, bf16[544,512]{1,0:T(8,128)(2,1)}, u32[]{:S(2)}) copy-start(bf16[544,512]{1,0:T(8,128)(2,1)} %copy-done.13) | copy-start | bytes 1671172
  83.5 9.3 %collective-permute-start.22 = (bf16[2048,128]{1,0:T(8,128)(2,1)S(1)}, bf16[2048,128]{1,0:T(8,128)(2,1)S(1)}, u32[]{:S(2)}, u32[]{:S(2)}) collective-permute-start(bf16[2048,128]{1,0:T(8,128)(2,1)S(1)} %get-tuple-element.18), channel_id=1, source_target_pairs={{0,14},{1,3},{2,0},{3,5},{4,2},{5,7},{6,4},{7,9},{8,6},{9,11},{10,... | collective-permute-start | bytes 1572872 | tf_op jit(solution)/shard_map/ppermute | solution.py:31
  83.6 14.8 %collective-permute-start.26 = (bf16[2048,128]{1,0:T(8,128)(2,1)S(1)}, bf16[2048,128]{1,0:T(8,128)(2,1)S(1)}, u32[]{:S(2)}, u32[]{:S(2)}) collective-permute-start(bf16[2048,128]{1,0:T(8,128)(2,1)S(1)} %get-tuple-element.22), channel_id=1, source_target_pairs={{0,14},{1,3},{2,0},{3,5},{4,2},{5,7},{6,4},{7,9},{8,6},{9,11},{10,... | collective-permute-start | bytes 1572872 | tf_op jit(solution)/shard_map/ppermute | solution.py:31
  93.0 11.1 %collective-permute-start.23 = (bf16[2048,128]{1,0:T(8,128)(2,1)S(1)}, bf16[2048,128]{1,0:T(8,128)(2,1)S(1)}, u32[]{:S(2)}, u32[]{:S(2)}) collective-permute-start(bf16[2048,128]{1,0:T(8,128)(2,1)S(1)} %add_convert_fusion.4), channel_id=1, source_target_pairs={{0,14},{1,3},{2,0},{3,5},{4,2},{5,7},{6,4},{7,9},{8,6},{9,11},{10,... | collective-permute-start | bytes 1572872 | tf_op jit(solution)/shard_map/ppermute | solution.py:31
  98.6 11.1 %collective-permute-start.27 = (bf16[2048,128]{1,0:T(8,128)(2,1)S(1)}, bf16[2048,128]{1,0:T(8,128)(2,1)S(1)}, u32[]{:S(2)}, u32[]{:S(2)}) collective-permute-start(bf16[2048,128]{1,0:T(8,128)(2,1)S(1)} %add_convert_fusion.1), channel_id=1, source_target_pairs={{0,14},{1,3},{2,0},{3,5},{4,2},{5,7},{6,4},{7,9},{8,6},{9,11},{10,... | collective-permute-start | bytes 1572872 | tf_op jit(solution)/shard_map/ppermute | solution.py:31
  103.2 6.7 %copy-start = (bf16[2048,128]{1,0:T(8,128)(2,1)S(1)}, bf16[2048,128]{1,0:T(8,128)(2,1)}, u32[]{:S(2)}) copy-start(bf16[2048,128]{1,0:T(8,128)(2,1)} %norm.1.refs_1_) | copy-start | bytes 1572868
  104.2 11.1 %collective-permute-start.24 = (bf16[2048,128]{1,0:T(8,128)(2,1)S(1)}, bf16[2048,128]{1,0:T(8,128)(2,1)S(1)}, u32[]{:S(2)}, u32[]{:S(2)}) collective-permute-start(bf16[2048,128]{1,0:T(8,128)(2,1)S(1)} %add_convert_fusion.3), channel_id=1, source_target_pairs={{0,14},{1,3},{2,0},{3,5},{4,2},{5,7},{6,4},{7,9},{8,6},{9,11},{10,... | collective-permute-start | bytes 1572872 | tf_op jit(solution)/shard_map/ppermute | solution.py:31
  109.8 11.1 %collective-permute-start.28 = (bf16[2048,128]{1,0:T(8,128)(2,1)S(1)}, bf16[2048,128]{1,0:T(8,128)(2,1)S(1)}, u32[]{:S(2)}, u32[]{:S(2)}) collective-permute-start(bf16[2048,128]{1,0:T(8,128)(2,1)S(1)} %add_convert_fusion), channel_id=1, source_target_pairs={{0,14},{1,3},{2,0},{3,5},{4,2},{5,7},{6,4},{7,9},{8,6},{9,11},{10,... | collective-permute-start | bytes 1572872 | tf_op jit(solution)/shard_map/ppermute | solution.py:31
  115.4 11.1 %collective-permute-start.25 = (bf16[2048,128]{1,0:T(8,128)(2,1)S(1)}, bf16[2048,128]{1,0:T(8,128)(2,1)S(1)}, u32[]{:S(2)}, u32[]{:S(2)}) collective-permute-start(bf16[2048,128]{1,0:T(8,128)(2,1)S(1)} %add_convert_fusion.2), channel_id=1, source_target_pairs={{0,14},{1,3},{2,0},{3,5},{4,2},{5,7},{6,4},{7,9},{8,6},{9,11},{10,... | collective-permute-start | bytes 1572872 | tf_op jit(solution)/shard_map/ppermute | solution.py:31
  120.9 5.6 %collective-permute-start.29 = (bf16[2048,128]{1,0:T(8,128)(2,1)S(1)}, bf16[2048,128]{1,0:T(8,128)(2,1)S(1)}, u32[]{:S(2)}, u32[]{:S(2)}) collective-permute-start(bf16[2048,128]{1,0:T(8,128)(2,1)S(1)} %collective-permute-done.28), channel_id=1, source_target_pairs={{0,1},{1,0},{2,3},{3,2},{4,5},{5,4},{6,7},{7,6},{8,9},{9,8},{10,11... | collective-permute-start | bytes 1572872 | tf_op jit(solution)/shard_map/ppermute | solution.py:42

commit v4 on v3

--- a/solution.py
+++ b/solution.py
@@ -111,48 +111,56 @@
     )(gate, upper, down)
 
 
-def spread_body(blocks, *halves):
+def spread_body(blocks, whole, *halves):
     n = halves[0].shape[0]
     for i, out in enumerate(halves):
         for k in range(4):
-            out[:, LANES * k : LANES * (k + 1)] = blocks[k, n * i : n * (i + 1)]
+            part = blocks[k, n * i : n * (i + 1)]
+            out[:, LANES * k : LANES * (k + 1)] = part
+            whole[n * i : n * (i + 1), LANES * k : LANES * (k + 1)] = part
 
 
 def spread(blocks):
     return pl.pallas_call(
         spread_body,
-        out_shape=[jax.ShapeDtypeStruct((blocks.shape[1] // 2, 4 * LANES), bf16)] * 2,
+        out_shape=[jax.ShapeDtypeStruct((blocks.shape[1] // n, 4 * LANES), bf16) for n in (1, 2, 2)],
         in_specs=[WHOLE],
-        out_specs=[WHOLE] * 2,
+        out_specs=[WHOLE] * 3,
         compiler_params=SMALL,
         name="spread",
     )(blocks)
 
 
-def hold_body(place_ref, *refs):
-    blocks, out, sems = refs[:8], refs[8], refs[9]
-    at, half = place_ref[0], blocks[0].shape[0]
+PARTS = ((0, None), (3, 0), (3, 1), (1, 0), (1, 1), (2, 0), (2, 1))
+
+
+def hold_body(parts, place_ref, *refs):
+    n = len(parts)
+    blocks, out, sems = refs[:n], refs[-2], refs[-1]
+    half, at = out.shape[1] // 2, place_ref[0]
     copies = []
-    for i, b in enumerate(blocks):
-        end = out.at[(at + (0, 3, 1, 2)[i // 2]) % 4, half * (i % 2) : half * (i % 2 + 1)]
-        copies.append(pltpu.make_async_copy(b, end, sems.at[i]))
+    for i, (by, h) in enumerate(parts):
+        end = out.at[(at + by) % 4] if h is None else out.at[(at + by) % 4, half * h : half * (h + 1)]
+        copies.append(pltpu.make_async_copy(blocks[i], end, sems.at[i]))
     for c in copies:
         c.start()
     for c in copies:
         c.wait()
 
 
-def hold(place, blocks):
-    half, width = blocks[0].shape
-    return pl.pallas_call(
-        hold_body,
-        out_shape=jax.ShapeDtypeStruct((4, 2 * half, width), bf16),
-        in_specs=[pl.BlockSpec(memory_space=pltpu.SMEM)] + [pl.BlockSpec(memory_space=pltpu.HBM)] * 8,
+def hold(place, parts, blocks, shape, so_far=None):
+    n = len(parts)
+    more = [] if so_far is None else [so_far]
+    return pl.pallas_call(
+        functools.partial(hold_body, parts),
+        out_shape=jax.ShapeDtypeStruct(shape, bf16),
+        in_specs=[pl.BlockSpec(memory_space=pltpu.SMEM)] + [pl.BlockSpec(memory_space=pltpu.HBM)] * n + [WHOLE] * len(more),
         out_specs=WHOLE,
-        scratch_shapes=[pltpu.SemaphoreType.DMA((8,))],
+        input_output_aliases={n + 1: 0} if more else {},
+        scratch_shapes=[pltpu.SemaphoreType.DMA((n,))],
         compiler_params=SMALL,
         name="hold",
-    )(place, *blocks)
+    )(place, *blocks, *more)
 
 
 def order(core, b, w):
@@ -178,18 +186,27 @@
 
 
 def finish_body(n, units, core_ref, *refs):
-    pieces, weights, first, outs, turned = refs[:n], refs[n : n + 2], refs[n + 2], refs[n + 3 : 2 * n + 3], refs[2 * n + 3]
+    pieces, weights, first = refs[:n], refs[n : n + 2], refs[n + 2]
+    outs, turned, held = refs[n + 3 : 2 * n + 3], refs[2 * n + 3], refs[2 * n + 4]
     core, m = core_ref[0], pieces[0].shape[1]
-    hidden = first[...], half_hidden(core, 1, units, pieces, weights[1], turned)
-    for b in range(turned.shape[0] // LANES):
-        part = 0.0
-        for w in (0, 1):
-            at = order(core, b, w)
-            lanes = pl.ds(pl.multiple_of(at % 4 * LANES, LANES), LANES)
-            tiles = [weights[w][at // 4, r : r + LANES, lanes] for r in range(2 * units, weights[w].shape[1], LANES)]
-            part += jnp.dot(jnp.concatenate(tiles, axis=1)[:, :units], hidden[w], preferred_element_type=f32)
-        for i in range(n):
-            outs[i][LANES * b : LANES * (b + 1), :] = part[:, m * i : m * (i + 1)].astype(outs[i].dtype)
+    hidden = first, held
+    held[...] = half_hidden(core, 1, units, pieces, weights[1], turned)
+
+    def four(group, carry):
+        for j in range(4):
+            b = group * 4 + j
+            part = 0.0
+            for w in (0, 1):
+                at = order(core, b, w)
+                lanes = pl.ds(pl.multiple_of(at % 4 * LANES, LANES), LANES)
+                tiles = [weights[w][at // 4, r : r + LANES, lanes] for r in range(2 * units, weights[w].shape[1], LANES)]
+                part += jnp.dot(jnp.concatenate(tiles, axis=1)[:, :units], hidden[w][...], preferred_element_type=f32)
+            rows = pl.ds(pl.multiple_of(b * LANES, LANES), LANES)
+            for i in range(n):
+                outs[i][rows, :] = part[:, m * i : m * (i + 1)].astype(outs[i].dtype)
+        return carry
+
+    lax.fori_loop(0, turned.shape[0] // LANES // 4, four, 0)
 
 
 def call(body, units, core, pieces, rest, out_shape):
@@ -199,7 +216,7 @@
         out_shape=out_shape,
         in_specs=[pl.BlockSpec(memory_space=pltpu.SMEM)] + [WHOLE] * (n + len(rest)),
         out_specs=jax.tree.map(lambda _: WHOLE, out_shape),
-        scratch_shapes=[pltpu.VMEM((features, n * m), bf16)],
+        scratch_shapes=[pltpu.VMEM((features, n * m), bf16), pltpu.VMEM((units, n * m), bf16)],
         compiler_params=pltpu.CompilerParams(vmem_limit_bytes=18 << 20),
     )(core, *pieces, *rest)
 
@@ -240,30 +257,37 @@
             mate[d] = onward(mate[d - 1], 1)
 
     rows = from_four(pack(gate_weight.T, up_weight.T, down_weight), ROWS)
-    top, bottom = spread(rows)
+    here, top, bottom = spread(rows)
     before_top = along_column(top, 1)
     after_bottom = along_column(bottom, -1)
     before_bottom = along_column(bottom, 1)
     after_top = along_column(top, -1)
     far_top = along_column(before_top, 1)
     far_bottom = along_column(after_bottom, -1)
-    blocks = top, bottom, before_top, before_bottom, after_top, after_bottom, far_top, far_bottom
+    blocks = here, before_top, before_bottom, after_top, after_bottom, far_top, far_bottom
     others = []
     for b in blocks:
         others.append(swap(b))
     row, column = lax.axis_index("y").astype(jnp.int32)[None], lax.axis_index("x").astype(jnp.int32)[None]
     first = core == 0
-    columns = hold(jnp.where(first, row, column), blocks)
-    weights = columns, hold(jnp.where(first, column, row), others)
+    shape = (4, *here.shape)
+
+    def held(place, blocks):
+        most = hold(place, PARTS[:5], blocks[:5], shape)
+        return hold(place, PARTS[5:], blocks[5:], shape, most)
+
+    columns = held(jnp.where(first, row, column), blocks)
+    weights = columns, held(jnp.where(first, column, row), others)
 
     units = down_weight.shape[0]
-    groups = [(own[4], mate[3]), (own[3], mate[2]), (own[2], mate[1]), (own[1], own[0])]
+    groups = [(own[4], mate[3]), (own[3], mate[2]), (own[2], mate[1]), (own[1],), (own[0],)]
     firsts = []
     for g in groups:
         firsts.append(begin(units, core, g, columns))
-    dtypes = [bf16, f32, f32, f32]
-    shares = [finish(units, core, g, weights, f, t) for g, f, t in zip(groups, firsts, dtypes)]
-    (own4, mate3), (own3, mate2), (own2, mate1), (own1, own0) = shares
+    shares = []
+    for i, (g, f) in enumerate(zip(groups, firsts)):
+        shares.append(finish(units, core, g, weights, f, f32 if i else bf16))
+    (own4, mate3), (own3, mate2), (own2, mate1), (own1,), (own0,) = shares
 
     def send(x):
         return onward(x.astype(bf16), -1)

time: 128 us -> 129 us (level)
  the two profiles are of different devices: /device:TPU:1 before, /device:TPU:2 now
where the time goes in v4:
time: 129 us; the launch traced here: 128 us
  waiting for transfers between devices  53 us (41%)
  starting transfers between devices  31.2 us (24%)
  Pallas kernels  30.9 us (24%)
  local copies, waits for them, and re-layouts  12 us (9%)
    ppermute x14, waiting for transfers between devices, onward(): return lax.ppermute(x, ('z', 'c'), pairs)  47 us
    pallas_call x10, Pallas kernels, call(): pl.pallas_call(functools.partial(body, n, units), out_shape=out_shape, in...  18.1 us
    unnamed x38, local copies, waits for them, and re-layouts  12 us
    ppermute x6, starting transfers between devices, along_column(): return lax.ppermute(x, ('y', 'x', 'c'), pairs)  11.9 us
    ppermute x14, starting transfers between devices, onward(): return lax.ppermute(x, ('z', 'c'), pairs)  7.88 us
    all_to_all x1, starting transfers between devices, from_four(): lax.all_to_all(copies, AXES, 0, 0, axis_index_groups=groups, tiled=True)  6.46 us
    ppermute x6, waiting for transfers between devices, along_column(): return lax.ppermute(x, ('y', 'x', 'c'), pairs)  6.03 us
    pallas_call x4, Pallas kernels, hold(): pl.pallas_call(functools.partial(hold_body, parts), out_shape=jax.ShapeDt...  5.61 us
  transfers between devices with their start and end apart: 30, of which 15 were waited for; matrix products, arithmetic and copies ran while one was open for 1% of the time, Pallas kernels for 18%

profile of v4, /device:TPU:2, one launch (start us, length us, event | category | flops | bytes accessed | tf_op | source)
XLA Modules:
  0.0 128.1 jit_solution(12881293723661188447)
XLA Ops:
  0.0 2.1 %pack.1 = bf16[4,1088,128]{2,1,0:T(8,128)(2,1)} custom-call(bf16[352,128]{1,0:T(8,128)(2,1)} %bitcast.6, bf16[352,128]{1,0:T(8,128)(2,1)} %bitcast.7, bf16[352,128]{1,0:T(8,128)(2,1)} %down_in.1), custom_call_target="tpu_custom_call" | custom-call | tf_op jit(solution)/shard_map/pack/pallas_call | solution.py:103
  2.1 6.5 %all-to-all-start = ((bf16[4,1088,128]{2,1,0:T(8,128)(2,1)}), bf16[4,1088,128]{2,1,0:T(8,128)(2,1)}, u32[]{:S(2)}, u32[]{:S(2)}) async-start(bf16[4,1088,128]{2,1,0:T(8,128)(2,1)} %pack.1), calls=%async_computation | async-start | bytes 2228224 | tf_op jit(solution)/shard_map/all_to_all | solution.py:46
  8.6 2.2 %norm.1.refs_0_ = bf16[2048,128]{1,0:T(8,128)(2,1)} custom-call(bf16[128,2048]{1,0:T(8,128)(2,1)} %tokens_in.1, f32[1,2048]{1,0:T(1,128)} %bitcast.8), custom_call_target="tpu_custom_call" | custom-call | tf_op jit(solution)/shard_map/norm/pallas_call | solution.py:61
  11.2 2.9 %collective-permute-start.17 = (bf16[2048,128]{1,0:T(8,128)(2,1)}, bf16[2048,128]{1,0:T(8,128)(2,1)S(1)}, u32[]{:S(2)}, u32[]{:S(2)}) collective-permute-start(bf16[2048,128]{1,0:T(8,128)(2,1)} %norm.1.refs_0_), channel_id=1, source_target_pairs={{0,1},{1,0},{2,3},{3,2},{4,5},{5,4},{6,7},{7,6},{8,9},{9,8},{10,11... | collective-permute-start | bytes 1572872 | tf_op jit(solution)/shard_map/ppermute | solution.py:42
  14.1 8.4 %collective-permute-done.13.refs_0_ = bf16[2048,128]{1,0:T(8,128)(2,1)S(1)} collective-permute-done((bf16[2048,128]{1,0:T(8,128)(2,1)}, bf16[2048,128]{1,0:T(8,128)(2,1)S(1)}, u32[]{:S(2)}, u32[]{:S(2)}) %collective-permute-start.13) | collective-permute-done | bytes 524320 | tf_op jit(solution)/shard_map/ppermute | solution.py:31
  22.5 1.7 %spread.1 = (bf16[1088,512]{1,0:T(8,128)(2,1)S(1)}, bf16[544,512]{1,0:T(8,128)(2,1)S(1)}, bf16[544,512]{1,0:T(8,128)(2,1)S(1)}) custom-call(bf16[4,1088,128]{2,1,0:T(8,128)(2,1)} %all-to-all-done.blocks), custom_call_target="tpu_custom_call" | custom-call | tf_op jit(solution)/shard_map/spread/pallas_call | solution.py:124
  24.3 1.0 collective-permute-start.8
  25.2 1.0 copy-done.5
  26.3 1.7 %collective-permute-start = (bf16[544,512]{1,0:T(8,128)(2,1)S(1)}, bf16[544,512]{1,0:T(8,128)(2,1)S(1)}, u32[]{:S(2)}, u32[]{:S(2)}) collective-permute-start(bf16[544,512]{1,0:T(8,128)(2,1)S(1)} %get-tuple-element.14), channel_id=1, source_target_pairs={{0,64},{16,80},{32,96},{48,112},{64,128},{80,144},{96,160},{112,17... | collective-permute-start | bytes 1671176 | tf_op jit(solution)/shard_map/ppermute | solution.py:38
  28.0 1.5 %collective-permute-start.2 = (bf16[544,512]{1,0:T(8,128)(2,1)S(1)}, bf16[544,512]{1,0:T(8,128)(2,1)}, u32[]{:S(2)}, u32[]{:S(2)}) collective-permute-start(bf16[544,512]{1,0:T(8,128)(2,1)S(1)} %get-tuple-element.15), channel_id=1, source_target_pairs={{0,192},{16,208},{32,224},{48,240},{64,0},{80,16},{96,32},{112,48}... | collective-permute-start | bytes 1671176 | tf_op jit(solution)/shard_map/ppermute | solution.py:38
  29.5 3.4 %collective-permute-done.14.refs_0_ = bf16[2048,128]{1,0:T(8,128)(2,1)S(1)} collective-permute-done((bf16[2048,128]{1,0:T(8,128)(2,1)S(1)}, bf16[2048,128]{1,0:T(8,128)(2,1)S(1)}, u32[]{:S(2)}, u32[]{:S(2)}) %collective-permute-start.14) | collective-permute-done | bytes 524320 | tf_op jit(solution)/shard_map/ppermute | solution.py:31
  32.9 1.6 %collective-permute-start.4 = (bf16[544,512]{1,0:T(8,128)(2,1)S(1)}, bf16[544,512]{1,0:T(8,128)(2,1)S(1)}, u32[]{:S(2)}, u32[]{:S(2)}) collective-permute-start(bf16[544,512]{1,0:T(8,128)(2,1)S(1)} %get-tuple-element.15), channel_id=1, source_target_pairs={{0,64},{16,80},{32,96},{48,112},{64,128},{80,144},{96,160},{112,17... | collective-permute-start | bytes 1671176 | tf_op jit(solution)/shard_map/ppermute | solution.py:38
  34.5 4.0 %collective-permute-done.18.refs_1_ = bf16[2048,128]{1,0:T(8,128)(2,1)S(1)} collective-permute-done((bf16[2048,128]{1,0:T(8,128)(2,1)S(1)}, bf16[2048,128]{1,0:T(8,128)(2,1)S(1)}, u32[]{:S(2)}, u32[]{:S(2)}) %collective-permute-start.18) | collective-permute-done | bytes 524320 | tf_op jit(solution)/shard_map/ppermute | solution.py:31
  38.5 3.0 %collective-permute-start.5 = (bf16[544,512]{1,0:T(8,128)(2,1)S(1)}, bf16[544,512]{1,0:T(8,128)(2,1)S(1)}, u32[]{:S(2)}, u32[]{:S(2)}) collective-permute-start(bf16[544,512]{1,0:T(8,128)(2,1)S(1)} %get-tuple-element.14), channel_id=1, source_target_pairs={{0,192},{16,208},{32,224},{48,240},{64,0},{80,16},{96,32},{112,48}... | collective-permute-start | bytes 1671176 | tf_op jit(solution)/shard_map/ppermute | solution.py:38
  42.2 1.4 %collective-permute-done.4.refs_2_ = bf16[544,512]{1,0:T(8,128)(2,1)S(1)} collective-permute-done((bf16[544,512]{1,0:T(8,128)(2,1)S(1)}, bf16[544,512]{1,0:T(8,128)(2,1)S(1)}, u32[]{:S(2)}, u32[]{:S(2)}) %collective-permute-start.4) | collective-permute-done | bytes 557088 | tf_op jit(solution)/shard_map/ppermute | solution.py:38
  44.0 4.6 %collective-permute-done.5.refs_3_ = bf16[544,512]{1,0:T(8,128)(2,1)S(1)} collective-permute-done((bf16[544,512]{1,0:T(8,128)(2,1)S(1)}, bf16[544,512]{1,0:T(8,128)(2,1)S(1)}, u32[]{:S(2)}, u32[]{:S(2)}) %collective-permute-start.5) | collective-permute-done | bytes 557088 | tf_op jit(solution)/shard_map/ppermute | solution.py:38
  48.6 3.7 %collective-permute-start.3 = (bf16[544,512]{1,0:T(8,128)(2,1)}, bf16[544,512]{1,0:T(8,128)(2,1)}, u32[]{:S(2)}, u32[]{:S(2)}) collective-permute-start(bf16[544,512]{1,0:T(8,128)(2,1)} %collective-permute-done.2.refs_4_), channel_id=1, source_target_pairs={{0,192},{16,208},{32,224},{48,240},{64,0},{80,16},{96,32},{112,48}... | collective-permute-start | bytes 1671176 | tf_op jit(solution)/shard_map/ppermute | solution.py:38
  53.1 4.4 %collective-permute-done.19.refs_1_ = bf16[2048,128]{1,0:T(8,128)(2,1)S(1)} collective-permute-done((bf16[2048,128]{1,0:T(8,128)(2,1)S(1)}, bf16[2048,128]{1,0:T(8,128)(2,1)S(1)}, u32[]{:S(2)}, u32[]{:S(2)}) %collective-permute-start.19) | collective-permute-done | bytes 524320 | tf_op jit(solution)/shard_map/ppermute | solution.py:31
  58.4 1.0 copy-done.3
  63.9 1.2 copy-done.6
  65.1 1.1 copy-done.8
  66.2 1.1 copy-done.10
  67.2 1.1 copy-done.12
  68.3 1.5 %hold.4.refs_2_ = bf16[4,1088,512]{2,1,0:T(8,128)(2,1)S(1)} custom-call(s32[1]{0:T(128)S(6)} %select_n.7.place_ref, bf16[1088,512]{1,0:T(8,128)(2,1)S(1)} %copy-done.6, bf16[544,512]{1,0:T(8,128)(2,1)S(1)} %copy-done.8, bf16[544,512]{1,0:T(8,128)(2,1)S(1)} %copy-done.10, bf16[544,512]{1,0:T(8,128)(2,1)S(1)} %copy-done.12, ...), custom_call_target="tpu_custom_call" | custom-call | tf_op jit(solution)/shard_map/hold/pallas_call | solution.py:154
  69.8 1.4 %hold.5.refs_1_.refs_2_ = bf16[4,1088,512]{2,1,0:T(8,128)(2,1)S(1)} custom-call(s32[1]{0:T(128)S(6)} %select_n.7.place_ref, bf16[544,512]{1,0:T(8,128)(2,1)} %collective-permute-done.1.refs_0_, bf16[544,512]{1,0:T(8,128)(2,1)} %collective-permute-done.3.refs_1_, bf16[4,1088,512]{2,1,0:T(8,128)(2,1)S(1)} %hold.4.refs_2_), custom_call_target="tpu_custom_call", output_to_operand_aliasing={{}: (3, {})} | custom-call | tf_op jit(solution)/shard_map/hold/pallas_call | solution.py:154
  71.8 1.5 %hold.6.refs_2_ = bf16[4,1088,512]{2,1,0:T(8,128)(2,1)S(1)} custom-call(s32[1]{0:T(128)S(6)} %select_n.8.place_ref, bf16[1088,512]{1,0:T(8,128)(2,1)S(1)} %copy-done.4, bf16[544,512]{1,0:T(8,128)(2,1)S(1)} %copy-done.14, bf16[544,512]{1,0:T(8,128)(2,1)S(1)} %copy-done.16, bf16[544,512]{1,0:T(8,128)(2,1)S(1)} %copy-done.18, ...), custom_call_target="tpu_custom_call" | custom-call | tf_op jit(solution)/shard_map/hold/pallas_call | solution.py:154
  73.4 5.6 %collective-permute-done.20.refs_1_ = bf16[2048,128]{1,0:T(8,128)(2,1)S(1)} collective-permute-done((bf16[2048,128]{1,0:T(8,128)(2,1)S(1)}, bf16[2048,128]{1,0:T(8,128)(2,1)S(1)}, u32[]{:S(2)}, u32[]{:S(2)}) %collective-permute-start.20) | collective-permute-done | bytes 524320 | tf_op jit(solution)/shard_map/ppermute | solution.py:31
  79.0 1.0 shard_map.57.refs_4_
  80.0 1.2 hold.7.refs_2_.refs_3_
  81.3 2.8 %shard_map.58 = (bf16[2048,128]{1,0:T(8,128)(2,1)S(1)}, bf16[2048,128]{1,0:T(8,128)(2,1)S(1)}) custom-call(s32[1]{0:T(128)} %bitcast.core_ref, bf16[2048,128]{1,0:T(8,128)(2,1)S(1)} %collective-permute-done.16.refs_0_, bf16[2048,128]{1,0:T(8,128)(2,1)S(1)} %collective-permute-done.20.refs_1_, bf16[4,1088,512]{2,1,0:T(8,128)(2,1)S(1)} %hold.5.refs_1_.refs_2_, ...), custom_call_target="tpu_custom_call" | custom-call | tf_op jit(solution)/shard_map/pallas_call | solution.py:214
  84.3 1.0 shard_map.59.refs_4_
  85.3 2.8 %shard_map.60 = (f32[2048,128]{1,0:T(8,128)S(1)}, f32[2048,128]{1,0:T(8,128)S(1)}) custom-call(s32[1]{0:T(128)} %bitcast.core_ref, bf16[2048,128]{1,0:T(8,128)(2,1)S(1)} %collective-permute-done.15.refs_0_, bf16[2048,128]{1,0:T(8,128)(2,1)S(1)} %collective-permute-done.19.refs_1_, bf16[4,1088,512]{2,1,0:T(8,128)(2,1)S(1)} %hold.5.refs_1_.refs_2_, ...), custom_call_target="tpu_custom_call" | custom-call | tf_op jit(solution)/shard_map/pallas_call | solution.py:214
  88.1 5.3 %collective-permute-done.21 = bf16[2048,128]{1,0:T(8,128)(2,1)S(1)} collective-permute-done((bf16[2048,128]{1,0:T(8,128)(2,1)S(1)}, bf16[2048,128]{1,0:T(8,128)(2,1)S(1)}, u32[]{:S(2)}, u32[]{:S(2)}) %collective-permute-start.21) | collective-permute-done | bytes 524320 | tf_op jit(solution)/shard_map/ppermute | solution.py:31
  93.5 1.3 %collective-permute-start.22 = (bf16[2048,128]{1,0:T(8,128)(2,1)S(1)}, bf16[2048,128]{1,0:T(8,128)(2,1)S(1)}, u32[]{:S(2)}, u32[]{:S(2)}) collective-permute-start(bf16[2048,128]{1,0:T(8,128)(2,1)S(1)} %add_convert_fusion.4), channel_id=1, source_target_pairs={{0,14},{1,3},{2,0},{3,5},{4,2},{5,7},{6,4},{7,9},{8,6},{9,11},{10,... | collective-permute-start | bytes 1572872 | tf_op jit(solution)/shard_map/ppermute | solution.py:31
  94.8 4.2 %collective-permute-done.25 = bf16[2048,128]{1,0:T(8,128)(2,1)S(1)} collective-permute-done((bf16[2048,128]{1,0:T(8,128)(2,1)S(1)}, bf16[2048,128]{1,0:T(8,128)(2,1)S(1)}, u32[]{:S(2)}, u32[]{:S(2)}) %collective-permute-start.25) | collective-permute-done | bytes 524320 | tf_op jit(solution)/shard_map/ppermute | solution.py:31
  99.1 1.5 %collective-permute-start.26 = (bf16[2048,128]{1,0:T(8,128)(2,1)S(1)}, bf16[2048,128]{1,0:T(8,128)(2,1)S(1)}, u32[]{:S(2)}, u32[]{:S(2)}) collective-permute-start(bf16[2048,128]{1,0:T(8,128)(2,1)S(1)} %add_convert_fusion.1), channel_id=1, source_target_pairs={{0,14},{1,3},{2,0},{3,5},{4,2},{5,7},{6,4},{7,9},{8,6},{9,11},{10,... | collective-permute-start | bytes 1572872 | tf_op jit(solution)/shard_map/ppermute | solution.py:31
  100.6 1.0 shard_map.61.refs_4_
  101.6 2.8 %shard_map.62 = (f32[2048,128]{1,0:T(8,128)S(1)}, f32[2048,128]{1,0:T(8,128)S(1)}) custom-call(s32[1]{0:T(128)} %bitcast.core_ref, bf16[2048,128]{1,0:T(8,128)(2,1)S(1)} %collective-permute-done.14.refs_0_, bf16[2048,128]{1,0:T(8,128)(2,1)S(1)} %collective-permute-done.18.refs_1_, bf16[4,1088,512]{2,1,0:T(8,128)(2,1)S(1)} %hold.5.refs_1_.refs_2_, ...), custom_call_target="tpu_custom_call" | custom-call | tf_op jit(solution)/shard_map/pallas_call | solution.py:214
  104.7 1.3 %collective-permute-start.23 = (bf16[2048,128]{1,0:T(8,128)(2,1)S(1)}, bf16[2048,128]{1,0:T(8,128)(2,1)S(1)}, u32[]{:S(2)}, u32[]{:S(2)}) collective-permute-start(bf16[2048,128]{1,0:T(8,128)(2,1)S(1)} %add_convert_fusion.3), channel_id=1, source_target_pairs={{0,14},{1,3},{2,0},{3,5},{4,2},{5,7},{6,4},{7,9},{8,6},{9,11},{10,... | collective-permute-start | bytes 1572872 | tf_op jit(solution)/shard_map/ppermute | solution.py:31
  106.0 4.2 %collective-permute-done.26 = bf16[2048,128]{1,0:T(8,128)(2,1)S(1)} collective-permute-done((bf16[2048,128]{1,0:T(8,128)(2,1)S(1)}, bf16[2048,128]{1,0:T(8,128)(2,1)S(1)}, u32[]{:S(2)}, u32[]{:S(2)}) %collective-permute-start.26) | collective-permute-done | bytes 524320 | tf_op jit(solution)/shard_map/ppermute | solution.py:31
  110.3 1.3 %collective-permute-start.27 = (bf16[2048,128]{1,0:T(8,128)(2,1)S(1)}, bf16[2048,128]{1,0:T(8,128)(2,1)S(1)}, u32[]{:S(2)}, u32[]{:S(2)}) collective-permute-start(bf16[2048,128]{1,0:T(8,128)(2,1)S(1)} %add_convert_fusion), channel_id=1, source_target_pairs={{0,14},{1,3},{2,0},{3,5},{4,2},{5,7},{6,4},{7,9},{8,6},{9,11},{10,... | collective-permute-start | bytes 1572872 | tf_op jit(solution)/shard_map/ppermute | solution.py:31
  112.6 2.4 %shard_map.64 = f32[2048,128]{1,0:T(8,128)S(1)} custom-call(s32[1]{0:T(128)} %bitcast.core_ref, bf16[2048,128]{1,0:T(8,128)(2,1)S(1)} %copy-done.2, bf16[4,1088,512]{2,1,0:T(8,128)(2,1)S(1)} %hold.5.refs_1_.refs_2_, bf16[4,1088,512]{2,1,0:T(8,128)(2,1)S(1)} %hold.7.refs_2_.refs_3_, bf16[352,128]{1,0:T(8,128)(2,1)S(1)} %shard_map.63.refs_3_), custom_call_target="tpu_custom_call" | custom-call | tf_op jit(solution)/shard_map/pallas_call | solution.py:214
  116.0 1.3 %collective-permute-start.24 = (bf16[2048,128]{1,0:T(8,128)(2,1)S(1)}, bf16[2048,128]{1,0:T(8,128)(2,1)S(1)}, u32[]{:S(2)}, u32[]{:S(2)}) collective-permute-start(bf16[2048,128]{1,0:T(8,128)(2,1)S(1)} %add_convert_fusion.2), channel_id=1, source_target_pairs={{0,14},{1,3},{2,0},{3,5},{4,2},{5,7},{6,4},{7,9},{8,6},{9,11},{10,... | collective-permute-start | bytes 1572872 | tf_op jit(solution)/shard_map/ppermute | solution.py:31
  117.3 4.2 %collective-permute-done.27 = bf16[2048,128]{1,0:T(8,128)(2,1)S(1)} collective-permute-done((bf16[2048,128]{1,0:T(8,128)(2,1)S(1)}, bf16[2048,128]{1,0:T(8,128)(2,1)S(1)}, u32[]{:S(2)}, u32[]{:S(2)}) %collective-permute-start.27) | collective-permute-done | bytes 524320 | tf_op jit(solution)/shard_map/ppermute | solution.py:31
  121.5 1.0 shard_map.55.refs_3_
  122.4 2.4 %shard_map.56.own = f32[2048,128]{1,0:T(8,128)S(1)} custom-call(s32[1]{0:T(128)} %bitcast.core_ref, bf16[2048,128]{1,0:T(8,128)(2,1)S(1)} %copy-done, bf16[4,1088,512]{2,1,0:T(8,128)(2,1)S(1)} %hold.5.refs_1_.refs_2_, bf16[4,1088,512]{2,1,0:T(8,128)(2,1)S(1)} %hold.7.refs_2_.refs_3_, bf16[352,128]{1,0:T(8,128)(2,1)S(1)} %shard_map.55.refs_3_), custom_call_target="tpu_custom_call" | custom-call | tf_op jit(solution)/shard_map/pallas_call | solution.py:214
  124.9 2.2 %collective-permute-done.24.first = bf16[2048,128]{1,0:T(8,128)(2,1)S(1)} collective-permute-done((bf16[2048,128]{1,0:T(8,128)(2,1)S(1)}, bf16[2048,128]{1,0:T(8,128)(2,1)S(1)}, u32[]{:S(2)}, u32[]{:S(2)}) %collective-permute-start.24) | collective-permute-done | bytes 524320 | tf_op jit(solution)/shard_map/ppermute | solution.py:31
  127.1 1.1 close.1
  (73 shorter events, 11.0 us)
Async XLA Ops:
  2.1 20.4 %all-to-all-start = ((bf16[4,1088,128]{2,1,0:T(8,128)(2,1)}), bf16[4,1088,128]{2,1,0:T(8,128)(2,1)}, u32[]{:S(2)}, u32[]{:S(2)}) async-start(bf16[4,1088,128]{2,1,0:T(8,128)(2,1)} %pack.1), calls=%async_computation | async-start | bytes 2228224 | tf_op jit(solution)/shard_map/all_to_all | solution.py:46
  10.8 11.7 %collective-permute-start.13 = (bf16[2048,128]{1,0:T(8,128)(2,1)}, bf16[2048,128]{1,0:T(8,128)(2,1)S(1)}, u32[]{:S(2)}, u32[]{:S(2)}) collective-permute-start(bf16[2048,128]{1,0:T(8,128)(2,1)} %norm.1.refs_0_), channel_id=1, source_target_pairs={{0,2},{1,15},{2,4},{3,1},{4,6},{5,3},{6,8},{7,5},{8,10},{9,7},{10,... | collective-permute-start | bytes 1572872 | tf_op jit(solution)/shard_map/ppermute | solution.py:31
  11.2 15.1 %collective-permute-start.17 = (bf16[2048,128]{1,0:T(8,128)(2,1)}, bf16[2048,128]{1,0:T(8,128)(2,1)S(1)}, u32[]{:S(2)}, u32[]{:S(2)}) collective-permute-start(bf16[2048,128]{1,0:T(8,128)(2,1)} %norm.1.refs_0_), channel_id=1, source_target_pairs={{0,1},{1,0},{2,3},{3,2},{4,5},{5,4},{6,7},{7,6},{8,9},{9,8},{10,11... | collective-permute-start | bytes 1572872 | tf_op jit(solution)/shard_map/ppermute | solution.py:42
  22.5 19.0 %copy-start.1 = (bf16[2048,128]{1,0:T(8,128)(2,1)}, bf16[2048,128]{1,0:T(8,128)(2,1)S(1)}, u32[]{:S(2)}) copy-start(bf16[2048,128]{1,0:T(8,128)(2,1)S(1)} %collective-permute-done.13.refs_0_) | copy-start | bytes 1572868
  22.5 10.4 %collective-permute-start.14 = (bf16[2048,128]{1,0:T(8,128)(2,1)S(1)}, bf16[2048,128]{1,0:T(8,128)(2,1)S(1)}, u32[]{:S(2)}, u32[]{:S(2)}) collective-permute-start(bf16[2048,128]{1,0:T(8,128)(2,1)S(1)} %collective-permute-done.13.refs_0_), channel_id=1, source_target_pairs={{0,2},{1,15},{2,4},{3,1},{4,6},{5,3},{6,8},{7,5},{8,10},{9,7},{10,... | collective-permute-start | bytes 1572872 | tf_op jit(solution)/shard_map/ppermute | solution.py:31
  24.3 34.1 %collective-permute-start.8 = (bf16[1088,512]{1,0:T(8,128)(2,1)S(1)}, bf16[1088,512]{1,0:T(8,128)(2,1)S(1)}, u32[]{:S(2)}, u32[]{:S(2)}) collective-permute-start(bf16[1088,512]{1,0:T(8,128)(2,1)S(1)} %get-tuple-element.16.refs_0_), channel_id=1, source_target_pairs={{0,1},{1,0},{2,3},{3,2},{4,5},{5,4},{6,7},{7,6},{8,9},{9,8},{10,11... | collective-permute-start | bytes 3342344 | tf_op jit(solution)/shard_map/ppermute | solution.py:42
  25.2 1.0 copy-start.5
  26.3 12.3 %collective-permute-start.18 = (bf16[2048,128]{1,0:T(8,128)(2,1)S(1)}, bf16[2048,128]{1,0:T(8,128)(2,1)S(1)}, u32[]{:S(2)}, u32[]{:S(2)}) collective-permute-start(bf16[2048,128]{1,0:T(8,128)(2,1)S(1)} %collective-permute-done.17), channel_id=1, source_target_pairs={{0,2},{1,15},{2,4},{3,1},{4,6},{5,3},{6,8},{7,5},{8,10},{9,7},{10,... | collective-permute-start | bytes 1572872 | tf_op jit(solution)/shard_map/ppermute | solution.py:31
  26.3 15.3 %collective-permute-start = (bf16[544,512]{1,0:T(8,128)(2,1)S(1)}, bf16[544,512]{1,0:T(8,128)(2,1)S(1)}, u32[]{:S(2)}, u32[]{:S(2)}) collective-permute-start(bf16[544,512]{1,0:T(8,128)(2,1)S(1)} %get-tuple-element.14), channel_id=1, source_target_pairs={{0,64},{16,80},{32,96},{48,112},{64,128},{80,144},{96,160},{112,17... | collective-permute-start | bytes 1671176 | tf_op jit(solution)/shard_map/ppermute | solution.py:38
  28.0 13.6 %collective-permute-start.2 = (bf16[544,512]{1,0:T(8,128)(2,1)S(1)}, bf16[544,512]{1,0:T(8,128)(2,1)}, u32[]{:S(2)}, u32[]{:S(2)}) collective-permute-start(bf16[544,512]{1,0:T(8,128)(2,1)S(1)} %get-tuple-element.15), channel_id=1, source_target_pairs={{0,192},{16,208},{32,224},{48,240},{64,0},{80,16},{96,32},{112,48}... | collective-permute-start | bytes 1671176 | tf_op jit(solution)/shard_map/ppermute | solution.py:38
  32.9 10.7 %collective-permute-start.4 = (bf16[544,512]{1,0:T(8,128)(2,1)S(1)}, bf16[544,512]{1,0:T(8,128)(2,1)S(1)}, u32[]{:S(2)}, u32[]{:S(2)}) collective-permute-start(bf16[544,512]{1,0:T(8,128)(2,1)S(1)} %get-tuple-element.15), channel_id=1, source_target_pairs={{0,64},{16,80},{32,96},{48,112},{64,128},{80,144},{96,160},{112,17... | collective-permute-start | bytes 1671176 | tf_op jit(solution)/shard_map/ppermute | solution.py:38
  38.5 10.1 %collective-permute-start.5 = (bf16[544,512]{1,0:T(8,128)(2,1)S(1)}, bf16[544,512]{1,0:T(8,128)(2,1)S(1)}, u32[]{:S(2)}, u32[]{:S(2)}) collective-permute-start(bf16[544,512]{1,0:T(8,128)(2,1)S(1)} %get-tuple-element.14), channel_id=1, source_target_pairs={{0,192},{16,208},{32,224},{48,240},{64,0},{80,16},{96,32},{112,48}... | collective-permute-start | bytes 1671176 | tf_op jit(solution)/shard_map/ppermute | solution.py:38
  41.5 10.7 %collective-permute-start.15 = (bf16[2048,128]{1,0:T(8,128)(2,1)S(1)}, bf16[2048,128]{1,0:T(8,128)(2,1)S(1)}, u32[]{:S(2)}, u32[]{:S(2)}) collective-permute-start(bf16[2048,128]{1,0:T(8,128)(2,1)S(1)} %collective-permute-done.14.refs_0_), channel_id=1, source_target_pairs={{0,2},{1,15},{2,4},{3,1},{4,6},{5,3},{6,8},{7,5},{8,10},{9,7},{10,... | collective-permute-start | bytes 1572872 | tf_op jit(solution)/shard_map/ppermute | solution.py:31
  41.6 16.0 %collective-permute-start.19 = (bf16[2048,128]{1,0:T(8,128)(2,1)S(1)}, bf16[2048,128]{1,0:T(8,128)(2,1)S(1)}, u32[]{:S(2)}, u32[]{:S(2)}) collective-permute-start(bf16[2048,128]{1,0:T(8,128)(2,1)S(1)} %collective-permute-done.18.refs_1_), channel_id=1, source_target_pairs={{0,2},{1,15},{2,4},{3,1},{4,6},{5,3},{6,8},{7,5},{8,10},{9,7},{10,... | collective-permute-start | bytes 1572872 | tf_op jit(solution)/shard_map/ppermute | solution.py:31
  43.6 17.0 %collective-permute-start.1 = (bf16[544,512]{1,0:T(8,128)(2,1)S(1)}, bf16[544,512]{1,0:T(8,128)(2,1)}, u32[]{:S(2)}, u32[]{:S(2)}) collective-permute-start(bf16[544,512]{1,0:T(8,128)(2,1)S(1)} %collective-permute-done.refs_1_), channel_id=1, source_target_pairs={{0,64},{16,80},{32,96},{48,112},{64,128},{80,144},{96,160},{112,17... | collective-permute-start | bytes 1671176 | tf_op jit(solution)/shard_map/ppermute | solution.py:38
  48.6 12.1 %collective-permute-start.3 = (bf16[544,512]{1,0:T(8,128)(2,1)}, bf16[544,512]{1,0:T(8,128)(2,1)}, u32[]{:S(2)}, u32[]{:S(2)}) collective-permute-start(bf16[544,512]{1,0:T(8,128)(2,1)} %collective-permute-done.2.refs_4_), channel_id=1, source_target_pairs={{0,192},{16,208},{32,224},{48,240},{64,0},{80,16},{96,32},{112,48}... | collective-permute-start | bytes 1671176 | tf_op jit(solution)/shard_map/ppermute | solution.py:38
  52.3 8.9 %collective-permute-start.9 = (bf16[544,512]{1,0:T(8,128)(2,1)S(1)}, bf16[544,512]{1,0:T(8,128)(2,1)S(1)}, u32[]{:S(2)}, u32[]{:S(2)}) collective-permute-start(bf16[544,512]{1,0:T(8,128)(2,1)S(1)} %collective-permute-done.refs_1_), channel_id=1, source_target_pairs={{0,1},{1,0},{2,3},{3,2},{4,5},{5,4},{6,7},{7,6},{8,9},{9,8},{10,11... | collective-permute-start | bytes 1671176 | tf_op jit(solution)/shard_map/ppermute | solution.py:42
  52.3 0.8 copy-start.7
  57.6 4.6 %collective-permute-start.10 = (bf16[544,512]{1,0:T(8,128)(2,1)S(1)}, bf16[544,512]{1,0:T(8,128)(2,1)S(1)}, u32[]{:S(2)}, u32[]{:S(2)}) collective-permute-start(bf16[544,512]{1,0:T(8,128)(2,1)S(1)} %collective-permute-done.4.refs_2_), channel_id=1, source_target_pairs={{0,1},{1,0},{2,3},{3,2},{4,5},{5,4},{6,7},{7,6},{8,9},{9,8},{10,11... | collective-permute-start | bytes 1671176 | tf_op jit(solution)/shard_map/ppermute | solution.py:42
  58.4 1.0 copy-start.3
  59.4 3.6 %collective-permute-start.11 = (bf16[544,512]{1,0:T(8,128)(2,1)S(1)}, bf16[544,512]{1,0:T(8,128)(2,1)S(1)}, u32[]{:S(2)}, u32[]{:S(2)}) collective-permute-start(bf16[544,512]{1,0:T(8,128)(2,1)S(1)} %collective-permute-done.5.refs_3_), channel_id=1, source_target_pairs={{0,1},{1,0},{2,3},{3,2},{4,5},{5,4},{6,7},{7,6},{8,9},{9,8},{10,11... | collective-permute-start | bytes 1671176 | tf_op jit(solution)/shard_map/ppermute | solution.py:42
  59.9 0.8 copy-start.11
  60.7 10.5 %collective-permute-start.12 = (bf16[544,512]{1,0:T(8,128)(2,1)}, bf16[544,512]{1,0:T(8,128)(2,1)}, u32[]{:S(2)}, u32[]{:S(2)}) collective-permute-start(bf16[544,512]{1,0:T(8,128)(2,1)} %collective-permute-done.2.refs_4_), channel_id=1, source_target_pairs={{0,1},{1,0},{2,3},{3,2},{4,5},{5,4},{6,7},{7,6},{8,9},{9,8},{10,11... | collective-permute-start | bytes 1671176 | tf_op jit(solution)/shard_map/ppermute | solution.py:42
  60.7 19.3 %collective-permute-start.6 = (bf16[544,512]{1,0:T(8,128)(2,1)}, bf16[544,512]{1,0:T(8,128)(2,1)}, u32[]{:S(2)}, u32[]{:S(2)}) collective-permute-start(bf16[544,512]{1,0:T(8,128)(2,1)} %collective-permute-done.1.refs_0_), channel_id=1, source_target_pairs={{0,1},{1,0},{2,3},{3,2},{4,5},{5,4},{6,7},{7,6},{8,9},{9,8},{10,11... | collective-permute-start | bytes 1671176 | tf_op jit(solution)/shard_map/ppermute | solution.py:42
  61.2 0.9 copy-start.13
  62.1 18.0 %collective-permute-start.7 = (bf16[544,512]{1,0:T(8,128)(2,1)}, bf16[544,512]{1,0:T(8,128)(2,1)}, u32[]{:S(2)}, u32[]{:S(2)}) collective-permute-start(bf16[544,512]{1,0:T(8,128)(2,1)} %collective-permute-done.3.refs_1_), channel_id=1, source_target_pairs={{0,1},{1,0},{2,3},{3,2},{4,5},{5,4},{6,7},{7,6},{8,9},{9,8},{10,11... | collective-permute-start | bytes 1671176 | tf_op jit(solution)/shard_map/ppermute | solution.py:42
  62.2 0.9 copy-start.15
  63.0 10.4 %collective-permute-start.16 = (bf16[2048,128]{1,0:T(8,128)(2,1)S(1)}, bf16[2048,128]{1,0:T(8,128)(2,1)S(1)}, u32[]{:S(2)}, u32[]{:S(2)}) collective-permute-start(bf16[2048,128]{1,0:T(8,128)(2,1)S(1)} %collective-permute-done.15.refs_0_), channel_id=1, source_target_pairs={{0,2},{1,15},{2,4},{3,1},{4,6},{5,3},{6,8},{7,5},{8,10},{9,7},{10,... | collective-permute-start | bytes 1572872 | tf_op jit(solution)/shard_map/ppermute | solution.py:31
  63.0 0.8 copy-start.17
  63.9 15.2 %collective-permute-start.20 = (bf16[2048,128]{1,0:T(8,128)(2,1)S(1)}, bf16[2048,128]{1,0:T(8,128)(2,1)S(1)}, u32[]{:S(2)}, u32[]{:S(2)}) collective-permute-start(bf16[2048,128]{1,0:T(8,128)(2,1)S(1)} %collective-permute-done.19.refs_1_), channel_id=1, source_target_pairs={{0,2},{1,15},{2,4},{3,1},{4,6},{5,3},{6,8},{7,5},{8,10},{9,7},{10,... | collective-permute-start | bytes 1572872 | tf_op jit(solution)/shard_map/ppermute | solution.py:31
  63.9 1.2 copy-start.6
  65.1 1.1 copy-start.8
  66.2 1.1 copy-start.10
  67.2 1.1 copy-start.12
  69.8 1.6 %copy-start.4 = (bf16[1088,512]{1,0:T(8,128)(2,1)S(1)}, bf16[1088,512]{1,0:T(8,128)(2,1)}, u32[]{:S(2)}) copy-start(bf16[1088,512]{1,0:T(8,128)(2,1)} %copy-done.3) | copy-start | bytes 3342340
  69.8 1.7 %copy-start.14 = (bf16[544,512]{1,0:T(8,128)(2,1)S(1)}, bf16[544,512]{1,0:T(8,128)(2,1)}, u32[]{:S(2)}) copy-start(bf16[544,512]{1,0:T(8,128)(2,1)} %copy-done.13) | copy-start | bytes 1671172
  69.8 1.9 %copy-start.16 = (bf16[544,512]{1,0:T(8,128)(2,1)S(1)}, bf16[544,512]{1,0:T(8,128)(2,1)}, u32[]{:S(2)}) copy-start(bf16[544,512]{1,0:T(8,128)(2,1)} %copy-done.15) | copy-start | bytes 1671172
  69.8 2.0 %copy-start.18 = (bf16[544,512]{1,0:T(8,128)(2,1)S(1)}, bf16[544,512]{1,0:T(8,128)(2,1)}, u32[]{:S(2)}) copy-start(bf16[544,512]{1,0:T(8,128)(2,1)} %copy-done.17) | copy-start | bytes 1671172
  84.1 9.3 %collective-permute-start.21 = (bf16[2048,128]{1,0:T(8,128)(2,1)S(1)}, bf16[2048,128]{1,0:T(8,128)(2,1)S(1)}, u32[]{:S(2)}, u32[]{:S(2)}) collective-permute-start(bf16[2048,128]{1,0:T(8,128)(2,1)S(1)} %get-tuple-element.17), channel_id=1, source_target_pairs={{0,14},{1,3},{2,0},{3,5},{4,2},{5,7},{6,4},{7,9},{8,6},{9,11},{10,... | collective-permute-start | bytes 1572872 | tf_op jit(solution)/shard_map/ppermute | solution.py:31
  84.2 14.8 %collective-permute-start.25 = (bf16[2048,128]{1,0:T(8,128)(2,1)S(1)}, bf16[2048,128]{1,0:T(8,128)(2,1)S(1)}, u32[]{:S(2)}, u32[]{:S(2)}) collective-permute-start(bf16[2048,128]{1,0:T(8,128)(2,1)S(1)} %get-tuple-element.20), channel_id=1, source_target_pairs={{0,14},{1,3},{2,0},{3,5},{4,2},{5,7},{6,4},{7,9},{8,6},{9,11},{10,... | collective-permute-start | bytes 1572872 | tf_op jit(solution)/shard_map/ppermute | solution.py:31
  93.5 11.1 %collective-permute-start.22 = (bf16[2048,128]{1,0:T(8,128)(2,1)S(1)}, bf16[2048,128]{1,0:T(8,128)(2,1)S(1)}, u32[]{:S(2)}, u32[]{:S(2)}) collective-permute-start(bf16[2048,128]{1,0:T(8,128)(2,1)S(1)} %add_convert_fusion.4), channel_id=1, source_target_pairs={{0,14},{1,3},{2,0},{3,5},{4,2},{5,7},{6,4},{7,9},{8,6},{9,11},{10,... | collective-permute-start | bytes 1572872 | tf_op jit(solution)/shard_map/ppermute | solution.py:31
  99.1 11.1 %collective-permute-start.26 = (bf16[2048,128]{1,0:T(8,128)(2,1)S(1)}, bf16[2048,128]{1,0:T(8,128)(2,1)S(1)}, u32[]{:S(2)}, u32[]{:S(2)}) collective-permute-start(bf16[2048,128]{1,0:T(8,128)(2,1)S(1)} %add_convert_fusion.1), channel_id=1, source_target_pairs={{0,14},{1,3},{2,0},{3,5},{4,2},{5,7},{6,4},{7,9},{8,6},{9,11},{10,... | collective-permute-start | bytes 1572872 | tf_op jit(solution)/shard_map/ppermute | solution.py:31
  104.4 7.2 %copy-start.2 = (bf16[2048,128]{1,0:T(8,128)(2,1)S(1)}, bf16[2048,128]{1,0:T(8,128)(2,1)}, u32[]{:S(2)}) copy-start(bf16[2048,128]{1,0:T(8,128)(2,1)} %copy-done.1) | copy-start | bytes 1572868
  104.7 11.1 %collective-permute-start.23 = (bf16[2048,128]{1,0:T(8,128)(2,1)S(1)}, bf16[2048,128]{1,0:T(8,128)(2,1)S(1)}, u32[]{:S(2)}, u32[]{:S(2)}) collective-permute-start(bf16[2048,128]{1,0:T(8,128)(2,1)S(1)} %add_convert_fusion.3), channel_id=1, source_target_pairs={{0,14},{1,3},{2,0},{3,5},{4,2},{5,7},{6,4},{7,9},{8,6},{9,11},{10,... | collective-permute-start | bytes 1572872 | tf_op jit(solution)/shard_map/ppermute | solution.py:31
  110.3 11.1 %collective-permute-start.27 = (bf16[2048,128]{1,0:T(8,128)(2,1)S(1)}, bf16[2048,128]{1,0:T(8,128)(2,1)S(1)}, u32[]{:S(2)}, u32[]{:S(2)}) collective-permute-start(bf16[2048,128]{1,0:T(8,128)(2,1)S(1)} %add_convert_fusion), channel_id=1, source_target_pairs={{0,14},{1,3},{2,0},{3,5},{4,2},{5,7},{6,4},{7,9},{8,6},{9,11},{10,... | collective-permute-start | bytes 1572872 | tf_op jit(solution)/shard_map/ppermute | solution.py:31
  112.6 8.8 %copy-start = (bf16[2048,128]{1,0:T(8,128)(2,1)S(1)}, bf16[2048,128]{1,0:T(8,128)(2,1)}, u32[]{:S(2)}) copy-start(bf16[2048,128]{1,0:T(8,128)(2,1)} %norm.1.refs_0_) | copy-start | bytes 1572868
  116.0 11.1 %collective-permute-start.24 = (bf16[2048,128]{1,0:T(8,128)(2,1)S(1)}, bf16[2048,128]{1,0:T(8,128)(2,1)S(1)}, u32[]{:S(2)}, u32[]{:S(2)}) collective-permute-start(bf16[2048,128]{1,0:T(8,128)(2,1)S(1)} %add_convert_fusion.2), channel_id=1, source_target_pairs={{0,14},{1,3},{2,0},{3,5},{4,2},{5,7},{6,4},{7,9},{8,6},{9,11},{10,... | collective-permute-start | bytes 1572872 | tf_op jit(solution)/shard_map/ppermute | solution.py:31
  121.4 5.6 %collective-permute-start.28 = (bf16[2048,128]{1,0:T(8,128)(2,1)S(1)}, bf16[2048,128]{1,0:T(8,128)(2,1)S(1)}, u32[]{:S(2)}, u32[]{:S(2)}) collective-permute-start(bf16[2048,128]{1,0:T(8,128)(2,1)S(1)} %collective-permute-done.27), channel_id=1, source_target_pairs={{0,1},{1,0},{2,3},{3,2},{4,5},{5,4},{6,7},{7,6},{8,9},{9,8},{10,11... | collective-permute-start | bytes 1572872 | tf_op jit(solution)/shard_map/ppermute | solution.py:42
  (1 other events, 0.8 us)
